TPU v7x, 128 devices: a whole 4x4x4 slice. The times are simulated.
128 devices in a mesh: sp: 32 (over z, y, core), tp: 4 (over x).
Axes of the slice: x: 4, y: 4, z: 4, core: 2. Of those that a mesh axis runs over, the one named last changes fastest.
Arguments:
- resid_in: bfloat16 [12288, 2048], P('sp'), may hold values from -6 to 6
- cotangent: bfloat16 [12288, 2048], P('sp'), may hold values from -2 to 2
- norm_gain: float32 [2048], replicated, may hold values from 0.1 to 1.9
- routes: int32 [12288, 2], P('sp'), may hold values from 0 to 31, all different within a row; in each aligned block of 384 rows (0 to 383, 384 to 767, ...) at most 48 rows name the same one
- route_weights: float32 [12288, 2], P('sp'), may hold values from 0.1 to 1
- gate_weight: bfloat16 [32, 2048, 1024], P('sp', None, 'tp'), may hold values from -0.125 to 0.125
- up_weight: bfloat16 [32, 2048, 1024], P('sp', None, 'tp'), may hold values from -0.125 to 0.125
- down_weight: bfloat16 [32, 1024, 2048], P('sp', 'tp'), may hold values from -0.1875 to 0.1875
- out_weight: bfloat16 [2048, 1024], P(None, 'tp'), may hold values from -0.1875 to 0.1875
- gate_b: bfloat16 [12288, 1024], P('sp', 'tp'), may hold values from -6 to 6
- gate_c: bfloat16 [12288, 1024], P('sp', 'tp'), may hold values from -6 to 6
- values_u: bfloat16 [12288, 1024], P('sp', 'tp'), may hold values from -6 to 6
- taps: float32 [3, 1024], P(None, 'tp'), may hold values from -3.5 to 3.5
Outputs:
- grad_gate_weight: float32 [32, 2048, 1024], P('sp', None, 'tp')
- grad_up_weight: float32 [32, 2048, 1024], P('sp', None, 'tp')
- grad_down_weight: float32 [32, 1024, 2048], P('sp', 'tp')
- grad_resid: bfloat16 [12288, 2048], P('sp')
- grad_out_weight: float32 [2048, 1024], P('sp', 'tp')
- grad_gate_b: bfloat16 [12288, 1024], P('sp', 'tp')
- grad_gate_c: bfloat16 [12288, 1024], P('sp', 'tp')
- grad_values: bfloat16 [12288, 1024], P('sp', 'tp')
Inputs may be any that keep to these rules, and one draw needn't show every extreme that they name: `routes`: A row's 2 experts differ. In the rows of one index of sp (384 tokens) no expert is named more than 48 times, a bound that some block reaches.
All inputs are finite; a program needn't handle non-finite values.
Results may differ from a plain program's by a relative error of at most 0.024.
Values may be sent and summed in bfloat16 or wider, within the bound.
No kernel may reach another device: no remote copies, remote signals or barrier semaphores. Data moves between devices by JAX's collectives and lax.ppermute only.
A program may use at most 128 MiB of HBM per device.

v0:
```python
import jax
import jax.numpy as jnp
from jax import lax
from jax.experimental import pallas as pl
from jax.experimental.pallas import tpu as pltpu
from jax.sharding import PartitionSpec as P

norm_eps = 1e-06
direct_width = 128
f32 = jnp.float32
bf16 = jnp.bfloat16


def passed_along(array, axis, by):
    size = lax.axis_size(axis)
    pairs = [(i, i + by) for i in range(size) if 0 <= i + by < size]
    return lax.ppermute(array, axis, pairs)


def turned(array, by):
    size = lax.axis_size("tp")
    return lax.ppermute(array, "tp", [(i, (i + by) % size) for i in range(size)])


def exchanged(array):
    return lax.all_to_all(array, "sp", split_axis=0, concat_axis=0, tiled=True)


def ring_gather(piece):
    half = piece.shape[0] // 2
    prev = turned(piece, 1)
    nxt = turned(piece, -1)
    far_top = turned(prev[:half], 1)
    far_low = turned(nxt[half:], -1)
    return prev, nxt, far_top, far_low


def placed_columns(lane, pieces, width):
    piece, (prev, nxt, far_top, far_low) = pieces
    half = piece.shape[0] // 2
    size = piece.shape[1]
    lanes = width // size
    whole = jnp.zeros((piece.shape[0], width), piece.dtype)
    whole = lax.dynamic_update_slice(whole, piece, (0, lane * size))
    whole = lax.dynamic_update_slice(whole, prev, (0, ((lane + lanes - 1) % lanes) * size))
    whole = lax.dynamic_update_slice(whole, nxt, (0, ((lane + 1) % lanes) * size))
    far = ((lane + 2) % lanes) * size
    whole = lax.dynamic_update_slice(whole, far_top, (0, far))
    return lax.dynamic_update_slice(whole, far_low, (half, far))


def lane_gather(piece):
    others = []
    for way in (1, -1, 2):
        others.append(turned(piece, way))
    return piece, *others


lane_steps = (0, -1, 1, 2)


def finish_kernel(lane_ref, *refs):
    wide_refs, narrow_refs, direct_refs = refs[:4], refs[4:8], refs[8:12]
    cot_ref, resid_ref, gain_ref, out_ref, grad_ref = refs[12:]
    width = grad_ref.shape[1]
    quarter = width // 4
    wide = wide_refs[0].shape[1]
    for step, wide_ref, narrow_ref in zip(lane_steps, wide_refs, narrow_refs):
        start = ((lane_ref[0] + (4 + step)) % 4) * quarter
        grad_ref[:, pl.ds(pl.multiple_of(start, 128), wide)] = wide_ref[...].astype(f32)
        grad_ref[:, pl.ds(pl.multiple_of(start + wide, 128), direct_width)] = narrow_ref[
            ...
        ].astype(f32)
    direct = sum(ref[...].astype(f32) for ref in direct_refs)
    for place in range(4):
        end = (place + 1) * quarter
        grad_ref[:, end - direct_width : end] = direct[
            :, place * direct_width : (place + 1) * direct_width
        ]
    resid = resid_ref[...].astype(f32)
    inv_rms = lax.rsqrt(jnp.mean(resid * resid, axis=1, keepdims=True) + norm_eps)
    scaled = grad_ref[...] * gain_ref[...]
    inner = jnp.mean(scaled * resid, axis=1, keepdims=True)
    out_ref[...] = (
        cot_ref[...].astype(f32) + inv_rms * scaled - resid * (inv_rms**3 * inner)
    ).astype(bf16)


def finish(lane, pieces, cotangent, resid_in, norm_gain):
    tokens, width = cotangent.shape
    block = 64

    def rows(array):
        return pl.BlockSpec((block, array.shape[1]), lambda i, _: (i, 0))

    gain = norm_gain.reshape(1, width)
    return pl.pallas_call(
        finish_kernel,
        grid_spec=pltpu.PrefetchScalarGridSpec(
            num_scalar_prefetch=1,
            grid=(tokens // block,),
            in_specs=[rows(x) for x in (*pieces, cotangent, resid_in)]
            + [pl.BlockSpec((1, width), lambda i, _: (0, 0))],
            out_specs=pl.BlockSpec((block, width), lambda i, _: (i, 0)),
            scratch_shapes=[pltpu.VMEM((block, width), f32)],
        ),
        out_shape=jax.ShapeDtypeStruct((tokens, width), bf16),
    )(lane.reshape(1), *pieces, cotangent, resid_in, gain)


def weighted_kernel(chooser_ref, cot_ref, weight_ref, out_ref):
    rows = jnp.dot(chooser_ref[...], cot_ref[...], preferred_element_type=f32)
    out_ref[...] = (rows * weight_ref[...]).astype(bf16)


def weighted_rows(chooser, cotangent, slot_weight):
    slots, tokens = chooser.shape
    width = cotangent.shape[1]
    block, part = 256, 512
    return pl.pallas_call(
        weighted_kernel,
        grid=(width // part, slots // block),
        in_specs=[
            pl.BlockSpec((block, tokens), lambda j, i: (i, 0)),
            pl.BlockSpec((tokens, part), lambda j, i: (0, j)),
            pl.BlockSpec((block, 1), lambda j, i: (i, 0)),
        ],
        out_specs=pl.BlockSpec((block, part), lambda j, i: (i, j)),
        out_shape=jax.ShapeDtypeStruct((slots, width), bf16),
    )(chooser, cotangent, slot_weight)


along_last = (((1,), (1,)), ((), ()))


def expert_kernel(lane_ref, gate_ref, up_ref, cot_ref, down_ref, gmat_ref, umat_ref, *outs):
    hidden_ref, dgate_ref, dup_ref, own_ref, direct_ref = outs[:5]
    further_refs = (outs[5:8], outs[8:11], outs[11:14])
    quarter = gmat_ref.shape[0] // 4
    dhidden = lax.dot_general(
        cot_ref[...], down_ref[...], along_last, preferred_element_type=f32
    )
    gate_pre = gate_ref[...]
    up_pre = up_ref[...]
    logistic = jax.nn.sigmoid(gate_pre)
    activated = gate_pre * logistic
    hidden_ref[...] = (activated * up_pre).astype(bf16)
    dgate = (dhidden * up_pre * logistic * (1.0 + gate_pre * (1.0 - logistic))).astype(bf16)
    dup = (dhidden * activated).astype(bf16)
    dgate_ref[...] = dgate
    dup_ref[...] = dup
    for further in range(4):
        place = (lane_ref[0] + further) % 4
        at = pl.ds(pl.multiple_of(place * quarter, 128), quarter)
        part = lax.dot_general(
            dgate, gmat_ref[at, :], along_last, preferred_element_type=f32
        ) + lax.dot_general(dup, umat_ref[at, :], along_last, preferred_element_type=f32)
        part = part.astype(bf16)
        direct_ref[:, pl.ds(pl.multiple_of(place * direct_width, 128), direct_width)] = part[
            :, quarter - direct_width :
        ]
        if further == 0:
            own_ref[...] = part[:, : quarter - direct_width]
        else:
            for i, ref in enumerate(further_refs[further - 1]):
                ref[...] = part[:, i * direct_width : (i + 1) * direct_width]


def expert_grads(lane, gate_pre, up_pre, entry_cots, down_mat, gate_mat, up_mat):
    slots, width = entry_cots.shape
    inner = gate_pre.shape[1]
    quarter = width // 4
    block = 256

    def rows(size):
        return pl.BlockSpec((block, size), lambda i, _: (i, 0))

    def whole(array):
        return pl.BlockSpec(array.shape, lambda i, _: (0, 0))

    sizes = [inner] * 3 + [quarter - direct_width, 4 * direct_width] + [direct_width] * 9
    return pl.pallas_call(
        expert_kernel,
        grid_spec=pltpu.PrefetchScalarGridSpec(
            num_scalar_prefetch=1,
            grid=(slots // block,),
            in_specs=[rows(inner), rows(inner), rows(width)]
            + [whole(x) for x in (down_mat, gate_mat, up_mat)],
            out_specs=[rows(size) for size in sizes],
        ),
        out_shape=[jax.ShapeDtypeStruct((slots, size), bf16) for size in sizes],
    )(lane.reshape(1), gate_pre, up_pre, entry_cots, down_mat, gate_mat, up_mat)


def on_device(
    resid_in,
    cotangent,
    norm_gain,
    routes,
    route_weights,
    gate_weight,
    up_weight,
    down_weight,
    out_weight,
    gate_b,
    gate_c,
    values_u,
    taps,
):
    token_count, model_width = resid_in.shape
    groups = lax.axis_size("sp")
    lanes = lax.axis_size("tp")
    lane = lax.axis_index("tp")
    expert_total = gate_weight.shape[0] * groups
    capacity = 4 * token_count // expert_total
    slots = expert_total * capacity
    quarter = model_width // lanes
    gate_mat, up_mat, down_mat = gate_weight[0], up_weight[0], down_weight[0]

    expert_ids = jnp.arange(expert_total, dtype=jnp.int32)[:, None]
    first = routes[:, 0][None, :] == expert_ids
    second = routes[:, 1][None, :] == expert_ids
    named = first | second
    order = jnp.arange(token_count, dtype=jnp.int32)
    earlier_mask = (order[:, None] < order[None, :]).astype(bf16)
    rank = jnp.dot(named.astype(bf16), earlier_mask, preferred_element_type=f32).astype(jnp.int32)
    rank = jnp.where(named, rank, -1)
    in_slot = rank[:, None, :] == jnp.arange(capacity, dtype=jnp.int32)[None, :, None]
    weight_of = jnp.where(first, route_weights[:, 0][None, :], 0.0) + jnp.where(
        second, route_weights[:, 1][None, :], 0.0
    )
    slot_weight = jnp.sum(jnp.where(in_slot, weight_of[:, None, :], 0.0), axis=2).reshape(slots, 1)
    chooser = in_slot.astype(bf16).reshape(slots, token_count)
    spread = (jnp.arange(slots, dtype=jnp.int32) // capacity)[None, :] == expert_ids
    slot_ranks = jnp.einsum(
        "et,es->ts", rank.astype(bf16), spread.astype(bf16), preferred_element_type=f32
    )
    slot_order = (jnp.arange(slots, dtype=jnp.int32) % capacity).astype(f32)
    token_chooser = (slot_ranks == slot_order[None, :]).astype(bf16)

    resid_wide = resid_in.astype(f32)
    inv_rms = lax.rsqrt(jnp.mean(resid_wide * resid_wide, axis=1, keepdims=True) + norm_eps)
    resid_part = lax.dynamic_slice_in_dim(resid_in, lane * quarter, quarter, axis=1)
    gain_part = lax.dynamic_slice_in_dim(norm_gain, lane * quarter, quarter, axis=0)
    normed_part = (resid_part.astype(f32) * inv_rms * gain_part).astype(bf16)
    sent_rows = jnp.dot(chooser, normed_part, preferred_element_type=f32).astype(bf16)
    got_part = exchanged(sent_rows.reshape(groups, capacity, quarter)).reshape(slots, quarter)
    sent_cots = weighted_rows(chooser, cotangent, slot_weight)
    entry_cots = exchanged(sent_cots.reshape(groups, capacity, model_width)).reshape(
        slots, model_width
    )
    entry_rows = placed_columns(lane, (got_part, ring_gather(got_part)), model_width)

    mixed = gate_c.astype(f32) * values_u.astype(f32)
    earlier = passed_along(mixed[-2:], "sp", 1)

    gate_pre = jnp.dot(entry_rows, gate_mat, preferred_element_type=f32)
    up_pre = jnp.dot(entry_rows, up_mat, preferred_element_type=f32)
    hidden, dgate, dup, own, direct, *others = expert_grads(
        lane, gate_pre, up_pre, entry_cots, down_mat, gate_mat, up_mat
    )
    a_ahead, b_ahead, c_ahead, a_far, b_far, c_far, a_behind, b_behind, c_behind = others

    def back(array):
        return exchanged(array.reshape(groups, capacity, -1)).reshape(slots, -1)

    def per_token(array):
        return jnp.dot(token_chooser, array, preferred_element_type=f32).astype(bf16)

    def plus(*arrays):
        return sum(array.astype(f32) for array in arrays).astype(bf16)

    a_far = turned(a_far, 1)
    b_far = turned(b_far, -1)
    a_next = turned(a_behind, -1)
    b_prev = turned(b_ahead, 1)
    direct = per_token(back(direct))
    a_prev = turned(plus(a_ahead, a_far), 1)
    b_next = turned(plus(b_behind, b_far), -1)
    c_far, c_behind, a_far = lax.optimization_barrier((c_far, c_behind, a_far))
    c_far = turned(c_far, 1)
    c_next = turned(c_behind, -1)
    c_prev = turned(plus(c_ahead, c_far), 1)
    pair = 2 * direct_width
    wide = jnp.concatenate(
        [
            plus(own[:, :direct_width], a_prev, a_next),
            plus(own[:, direct_width:pair], b_prev, b_next),
        ],
        axis=1,
    )
    own_last = own[:, pair:]
    wide, direct, own_last, hidden = lax.optimization_barrier((wide, direct, own_last, hidden))
    grad_down = jnp.einsum("rf,rd->fd", hidden, entry_cots, preferred_element_type=f32)
    direct_parts = lane_gather(direct)
    wide = per_token(back(wide))
    narrow = plus(own_last, c_prev, c_next)
    narrow, wide = lax.optimization_barrier((narrow, wide))
    wide_parts = lane_gather(wide)
    narrow_parts = lane_gather(per_token(back(narrow)))
    pieces = (*wide_parts, *narrow_parts, *direct_parts)
    grad_resid = finish(lane, pieces, cotangent, resid_in, norm_gain)

    extended = jnp.concatenate([earlier, mixed], axis=0)
    conv = (
        taps[0] * extended[:token_count]
        + taps[1] * extended[1 : token_count + 1]
        + taps[2] * extended[2 : token_count + 2]
    )
    merged = (gate_b.astype(f32) * conv).astype(bf16)
    out_parts = jnp.einsum("td,tc->dc", grad_resid, merged, preferred_element_type=f32).astype(bf16)
    out_tiles = exchanged(out_parts.reshape(groups, model_width // groups, -1))
    grad_out_weight = jnp.sum(out_tiles.astype(f32), axis=0)
    dgate, out_parts = lax.optimization_barrier((dgate, out_parts))
    grad_gate = jnp.einsum("rd,rf->df", entry_rows, dgate, preferred_element_type=f32)
    late_resid, grad_gate, dup = lax.optimization_barrier((grad_resid, grad_gate, dup))
    grad_up = jnp.einsum("rd,rf->df", entry_rows, dup, preferred_element_type=f32)
    dmerged = jnp.dot(late_resid, out_weight, preferred_element_type=f32)
    grad_gate_b = (dmerged * conv).astype(bf16)
    dconv = dmerged * gate_b.astype(f32)
    later = passed_along(dconv[:2], "sp", -1)
    extended_grad = jnp.concatenate([dconv, later], axis=0)
    dmixed = (
        taps[2] * extended_grad[:token_count]
        + taps[1] * extended_grad[1 : token_count + 1]
        + taps[0] * extended_grad[2 : token_count + 2]
    )
    grad_gate_c = (dmixed * values_u.astype(f32)).astype(bf16)
    grad_values = (dmixed * gate_c.astype(f32)).astype(bf16)
    return (
        grad_gate[None],
        grad_up[None],
        grad_down[None],
        grad_resid,
        grad_out_weight,
        grad_gate_b,
        grad_gate_c,
        grad_values,
    )


def solution(mesh):
    placed = (
        P("sp", None),
        P("sp", None),
        P(),
        P("sp", None),
        P("sp", None),
        P("sp", None, "tp"),
        P("sp", None, "tp"),
        P("sp", "tp", None),
        P(None, "tp"),
        P("sp", "tp"),
        P("sp", "tp"),
        P("sp", "tp"),
        P(None, "tp"),
    )

    return jax.shard_map(
        on_device,
        mesh=mesh,
        in_specs=placed,
        out_specs=(
            P("sp", None, "tp"),
            P("sp", None, "tp"),
            P("sp", "tp", None),
            P("sp", None),
            P("sp", "tp"),
            P("sp", "tp"),
            P("sp", "tp"),
            P("sp", "tp"),
        ),
        check_vma=False,
    )
```

profile of v0, /device:TPU:1, one launch (start us, length us, event | category | flops | bytes accessed | tf_op | source)
XLA Modules:
  0.0 294.8 jit_solution(5842921378186005267)
XLA Ops:
  5.8 3.2 %convolution_convert_fusion = bf16[1536,512]{1,0:T(8,128)(2,1)} fusion(pred[1536,384]{1,0:T(32,128)(4,1)S(1)} %get-tuple-element.71, f32[512]{0:T(512)S(1)} %dynamic_slice.7, f32[384]{0:T(512)S(1)} %add_rsqrt_fusion, bf16[384,2048]{1,0:T(8,128)(2,1)} %refs_13_.1, s32[]{:T(128)S(6)} %select_n.73), kind=kOutput, calls=%fused_computation.1 | convolution fusion | flops 605552640 | bytes 2559492 | tf_op jit(solution)/shard_map/dot_general | solution.py:246
  9.1 9.6 %all-to-all-start = ((bf16[32,48,512]{2,1,0:T(8,128)(2,1)}), bf16[32,48,512]{2,1,0:T(8,128)(2,1)S(1)}, u32[]{:S(2)}, u32[]{:S(2)}) async-start(bf16[32,48,512]{2,1,0:T(8,128)(2,1)} %bitcast.55), calls=%async_computation | async-start | bytes 3145728 | tf_op jit(solution)/shard_map/all_to_all | solution.py:26
  20.3 18.9 %shard_map.188 = bf16[1536,2048]{1,0:T(8,128)(2,1)} custom-call(bf16[1536,384]{1,0:T(8,128)(2,1)} %get-tuple-element.70.chooser_ref, bf16[384,2048]{1,0:T(8,128)(2,1)} %refs_12_.1, f32[1536,1]{1,0:T(8,128)} %reshape.179.weight_ref), custom_call_target="tpu_custom_call" | custom-call | tf_op jit(solution)/shard_map/pallas_call | solution.py:120
  40.8 6.4 %all-to-all-start.1 = ((bf16[32,48,2048]{2,1,0:T(8,128)(2,1)}), bf16[32,48,2048]{2,1,0:T(8,128)(2,1)}, u32[]{:S(2)}, u32[]{:S(2)}) async-start(bf16[32,48,2048]{2,1,0:T(8,128)(2,1)} %bitcast.50), calls=%async_computation.1 | async-start | bytes 12582912 | tf_op jit(solution)/shard_map/all_to_all | solution.py:26
  50.0 34.2 %collective-permute-done = bf16[1536,512]{1,0:T(8,128)(2,1)} collective-permute-done((bf16[1536,512]{1,0:T(8,128)(2,1)S(1)}, bf16[1536,512]{1,0:T(8,128)(2,1)}, u32[]{:S(2)}, u32[]{:S(2)}) %collective-permute-start) | collective-permute-done | bytes 1572896 | tf_op jit(solution)/shard_map/ppermute | solution.py:22
  86.7 2.7 collective-permute-start.3
  93.8 10.8 %collective-permute-done.2 = bf16[768,512]{1,0:T(8,128)(2,1)S(1)} collective-permute-done((bf16[768,512]{1,0:T(8,128)(2,1)S(1)}, bf16[768,512]{1,0:T(8,128)(2,1)S(1)}, u32[]{:S(2)}, u32[]{:S(2)}) %collective-permute-start.2) | collective-permute-done | bytes 786464 | tf_op jit(solution)/shard_map/ppermute | solution.py:22
  104.9 3.2 %fusion.33.up_ref = f32[1536,256]{1,0:T(8,128)} fusion(bf16[1536,2048]{1,0:T(8,128)(2,1)S(1)} %constant_dynamic-update-slice_fusion.4, bf16[1,2048,256]{2,1,0:T(8,128)(2,1)S(1)} %copy-done.6), kind=kOutput, calls=%fused_computation.84 | convolution fusion | flops 1610612736 | bytes 8912896 | tf_op jit(solution)/shard_map/dot_general | solution.py:258
  108.1 3.0 %fusion.35.gate_ref = f32[1536,256]{1,0:T(8,128)} fusion(bf16[1536,2048]{1,0:T(8,128)(2,1)S(1)} %constant_dynamic-update-slice_fusion.4, bf16[1,2048,256]{2,1,0:T(8,128)(2,1)S(1)} %copy-done.5), kind=kOutput, calls=%fused_computation.86 | convolution fusion | flops 1610612736 | bytes 8912896 | tf_op jit(solution)/shard_map/dot_general | solution.py:257
  111.1 9.5 %all-to-all-done.1 = bf16[32,48,2048]{2,1,0:T(8,128)(2,1)} async-done(((bf16[32,48,2048]{2,1,0:T(8,128)(2,1)}), bf16[32,48,2048]{2,1,0:T(8,128)(2,1)}, u32[]{:S(2)}, u32[]{:S(2)}) %all-to-all-start.1) | async-done | bytes 6291488 | tf_op jit(solution)/shard_map/all_to_all | solution.py:26
  120.6 13.6 %shard_map.189 = (bf16[1536,256]{1,0:T(8,128)(2,1)}, bf16[1536,256]{1,0:T(8,128)(2,1)}, bf16[1536,256]{1,0:T(8,128)(2,1)}, bf16[1536,384]{1,0:T(8,128)(2,1)}, bf...) custom-call(s32[1]{0:T(128)} %bitcast.lane_ref, ...), custom_call_target="tpu_custom_call" | custom-call | tf_op jit(solution)/shard_map/pallas_call | solution.py:182
  134.2 2.7 collective-permute-start.8
  138.3 2.7 collective-permute-start.6
  141.0 9.4 %all-to-all-start.2 = ((bf16[32,48,512]{2,1,0:T(8,128)(2,1)}), bf16[32,48,512]{2,1,0:T(8,128)(2,1)S(1)}, u32[]{:S(2)}, u32[]{:S(2)}) async-start(bf16[32,48,512]{2,1,0:T(8,128)(2,1)} %bitcast.9), calls=%async_computation.2 | async-start | bytes 3145728 | tf_op jit(solution)/shard_map/all_to_all | solution.py:26
  152.8 3.0 %collective-permute-start.9 = (bf16[1536,128]{1,0:T(8,128)(2,1)S(1)}, bf16[1536,128]{1,0:T(8,128)(2,1)S(1)}, u32[]{:S(2)}, u32[]{:S(2)}) collective-permute-start(bf16[1536,128]{1,0:T(8,128)(2,1)S(1)} %add_convert_fusion.3), channel_id=1, source_target_pairs={{0,3},{1,0},{2,1},{3,2},{4,7},{5,4},{6,5},{7,6},{8,11},{9,8},{10,9... | collective-permute-start | bytes 1179656 | tf_op jit(solution)/shard_map/ppermute | solution.py:22
  157.1 10.2 %collective-permute-done.10 = bf16[1536,128]{1,0:T(8,128)(2,1)S(1)} collective-permute-done((bf16[1536,128]{1,0:T(8,128)(2,1)}, bf16[1536,128]{1,0:T(8,128)(2,1)S(1)}, u32[]{:S(2)}, u32[]{:S(2)}) %collective-permute-start.10) | collective-permute-done | bytes 393248 | tf_op jit(solution)/shard_map/ppermute | solution.py:22
  169.6 6.1 %collective-permute-done.5 = bf16[1536,128]{1,0:T(8,128)(2,1)S(1)} collective-permute-done((bf16[1536,128]{1,0:T(8,128)(2,1)S(1)}, bf16[1536,128]{1,0:T(8,128)(2,1)S(1)}, u32[]{:S(2)}, u32[]{:S(2)}) %collective-permute-start.5) | collective-permute-done | bytes 393248 | tf_op jit(solution)/shard_map/ppermute | solution.py:22
  180.7 9.7 %all-to-all-start.3 = ((bf16[32,48,256]{2,1,0:T(8,128)(2,1)}), bf16[32,48,256]{2,1,0:T(8,128)(2,1)S(1)}, u32[]{:S(2)}, u32[]{:S(2)}) async-start(bf16[32,48,256]{2,1,0:T(8,128)(2,1)} %bitcast.11), calls=%async_computation.3 | async-start | bytes 1572864 | tf_op jit(solution)/shard_map/all_to_all | solution.py:26
  190.5 3.5 %collective-permute-start.22 = (f32[2,256]{1,0:T(2,128)S(1)}, f32[2,256]{1,0:T(2,128)S(1)}, u32[]{:S(2)}, u32[]{:S(2)}) collective-permute-start(f32[2,256]{1,0:T(2,128)S(1)} %slice.77), channel_id=1, source_target_pairs={{0,4},{4,8},{8,12},{12,16},{16,20},{20,24},{24,28},{28,32},{32,36}... | collective-permute-start | bytes 6152 | tf_op jit(solution)/shard_map/ppermute | solution.py:17
  196.1 8.6 %all-to-all-done.3 = bf16[32,48,256]{2,1,0:T(8,128)(2,1)S(1)} async-done(((bf16[32,48,256]{2,1,0:T(8,128)(2,1)}), bf16[32,48,256]{2,1,0:T(8,128)(2,1)S(1)}, u32[]{:S(2)}, u32[]{:S(2)}) %all-to-all-start.3) | async-done | bytes 786464 | tf_op jit(solution)/shard_map/all_to_all | solution.py:26
  208.1 4.0 %all-to-all-start.4 = ((bf16[32,48,128]{2,1,0:T(8,128)(2,1)}), bf16[32,48,128]{2,1,0:T(8,128)(2,1)S(1)}, u32[]{:S(2)}, u32[]{:S(2)}) async-start(bf16[32,48,128]{2,1,0:T(8,128)(2,1)} %bitcast.13), calls=%async_computation.4 | async-start | bytes 786432 | tf_op jit(solution)/shard_map/all_to_all | solution.py:26
  217.8 4.6 %all-to-all-done.4 = bf16[32,48,128]{2,1,0:T(8,128)(2,1)S(1)} async-done(((bf16[32,48,128]{2,1,0:T(8,128)(2,1)}), bf16[32,48,128]{2,1,0:T(8,128)(2,1)S(1)}, u32[]{:S(2)}, u32[]{:S(2)}) %all-to-all-start.4) | async-done | bytes 393248 | tf_op jit(solution)/shard_map/all_to_all | solution.py:26
  223.9 8.5 %collective-permute-done.19.refs_9_ = bf16[384,512]{1,0:T(8,128)(2,1)} collective-permute-done((bf16[384,512]{1,0:T(8,128)(2,1)}, bf16[384,512]{1,0:T(8,128)(2,1)}, u32[]{:S(2)}, u32[]{:S(2)}) %collective-permute-start.19) | collective-permute-done | bytes 393248 | tf_op jit(solution)/shard_map/ppermute | solution.py:22
  232.5 2.7 collective-permute-start.17
  236.9 5.9 %convolution_bitcast_fusion = f32[1,256,2048]{2,1,0:T(8,128)} fusion(bf16[1536,256]{1,0:T(8,128)(2,1)S(1)} %copy-done.3, bf16[1536,2048]{1,0:T(8,128)(2,1)} %bitcast.7.cot_ref), kind=kOutput, calls=%fused_computation.3 | convolution fusion | flops 1610612736 | bytes 9175040 | tf_op jit(solution)/shard_map/rf,rd->fd/dot_general | solution.py:294
  244.7 6.5 %shard_map.190 = bf16[384,2048]{1,0:T(8,128)(2,1)} custom-call(s32[1]{0:T(128)} %bitcast.lane_ref, bf16[384,256]{1,0:T(8,128)(2,1)} %convolution_convert_fusion.3.refs_0_, bf16[384,256]{1,0:T(8,128)(2,1)} %copy-done.13, bf16[384,256]{1,0:T(8,128)(2,1)} %collective-permute-done.14.refs_2_, bf16[384,256]{1,0:T(8,128)(2,1)} %copy-done.14, ...), custom_call_target="tpu_custom_call" | custom-call | tf_op jit(solution)/shard_map/pallas_call | solution.py:97
  251.2 3.2 %convolution_convert_fusion.1 = bf16[2048,256]{1,0:T(8,128)(2,1)} fusion(bf16[384,2048]{1,0:T(8,128)(2,1)} %shard_map.190, f32[384,256]{1,0:T(8,128)S(1)} %fusion.8, bf16[384,256]{1,0:T(8,128)(2,1)S(1)} %copy-done.12), kind=kOutput, calls=%fused_computation.5 | convolution fusion | flops 403472384 | bytes 3211264 | tf_op jit(solution)/shard_map/td,tc->dc/dot_general | solution.py:311
  254.4 6.1 %fusion.40 = f32[2048,256]{1,0:T(8,128)} fusion(bf16[1536,2048]{1,0:T(8,128)(2,1)} %copy-done.2, bf16[1536,256]{1,0:T(8,128)(2,1)S(1)} %copy-done.20), kind=kOutput, calls=%fused_computation.90 | convolution fusion | flops 1610612736 | bytes 9175040 | tf_op jit(solution)/shard_map/rd,rf->df/dot_general | solution.py:315
  261.8 7.8 %collective-permute-start.23 = (f32[2,256]{1,0:T(2,128)S(1)}, f32[2,256]{1,0:T(2,128)S(1)}, u32[]{:S(2)}, u32[]{:S(2)}) collective-permute-start(f32[2,256]{1,0:T(2,128)S(1)} %slice.80), channel_id=1, source_target_pairs={{4,0},{8,4},{12,8},{16,12},{20,16},{24,20},{28,24},{32,28},{36,32}... | collective-permute-start | bytes 6152 | tf_op jit(solution)/shard_map/ppermute | solution.py:17
  269.7 7.3 %all-to-all-start.5 = ((bf16[32,64,256]{2,1,0:T(8,128)(2,1)}), bf16[32,64,256]{2,1,0:T(8,128)(2,1)S(1)}, u32[]{:S(2)}, u32[]{:S(2)}) async-start(bf16[32,64,256]{2,1,0:T(8,128)(2,1)} %bitcast.22), calls=%async_computation.5 | async-start | bytes 2097152 | tf_op jit(solution)/shard_map/all_to_all | solution.py:26
  277.0 6.2 %convolution_bitcast_fusion.1 = f32[1,2048,256]{2,1,0:T(8,128)} fusion(bf16[1536,2048]{1,0:T(8,128)(2,1)} %copy-done.2, bf16[1536,256]{1,0:T(8,128)(2,1)} %get-tuple-element.57), kind=kOutput, calls=%fused_computation.4 | convolution fusion | flops 1610612736 | bytes 9175040 | tf_op jit(solution)/shard_map/rd,rf->df/dot_general | solution.py:317
  284.7 9.3 %all-to-all-done.5 = bf16[32,64,256]{2,1,0:T(8,128)(2,1)S(1)} async-done(((bf16[32,64,256]{2,1,0:T(8,128)(2,1)}), bf16[32,64,256]{2,1,0:T(8,128)(2,1)S(1)}, u32[]{:S(2)}, u32[]{:S(2)}) %all-to-all-start.5) | async-done | bytes 1048608 | tf_op jit(solution)/shard_map/all_to_all | solution.py:26
  (121 shorter events, 50.4 us)
Async XLA Ops:
  0.6 259.9 %copy-start = (bf16[2048,256]{1,0:T(8,128)(2,1)S(1)}, bf16[2048,256]{1,0:T(8,128)(2,1)}, u32[]{:S(2)}) copy-start(bf16[2048,256]{1,0:T(8,128)(2,1)} %param.21) | copy-start | bytes 3145732
  9.1 31.8 %all-to-all-start = ((bf16[32,48,512]{2,1,0:T(8,128)(2,1)}), bf16[32,48,512]{2,1,0:T(8,128)(2,1)S(1)}, u32[]{:S(2)}, u32[]{:S(2)}) async-start(bf16[32,48,512]{2,1,0:T(8,128)(2,1)} %bitcast.55), calls=%async_computation | async-start | bytes 3145728 | tf_op jit(solution)/shard_map/all_to_all | solution.py:26
  40.8 79.8 %all-to-all-start.1 = ((bf16[32,48,2048]{2,1,0:T(8,128)(2,1)}), bf16[32,48,2048]{2,1,0:T(8,128)(2,1)}, u32[]{:S(2)}, u32[]{:S(2)}) async-start(bf16[32,48,2048]{2,1,0:T(8,128)(2,1)} %bitcast.50), calls=%async_computation.1 | async-start | bytes 12582912 | tf_op jit(solution)/shard_map/all_to_all | solution.py:26
  47.3 36.9 %collective-permute-start = (bf16[1536,512]{1,0:T(8,128)(2,1)S(1)}, bf16[1536,512]{1,0:T(8,128)(2,1)}, u32[]{:S(2)}, u32[]{:S(2)}) collective-permute-start(bf16[1536,512]{1,0:T(8,128)(2,1)S(1)} %bitcast.51), channel_id=1, source_target_pairs={{0,1},{1,2},{2,3},{3,0},{4,5},{5,6},{6,7},{7,4},{8,9},{9,10},{10,1... | collective-permute-start | bytes 4718600 | tf_op jit(solution)/shard_map/ppermute | solution.py:22
  48.6 36.9 %collective-permute-start.1 = (bf16[1536,512]{1,0:T(8,128)(2,1)S(1)}, bf16[1536,512]{1,0:T(8,128)(2,1)}, u32[]{:S(2)}, u32[]{:S(2)}) collective-permute-start(bf16[1536,512]{1,0:T(8,128)(2,1)S(1)} %bitcast.52), channel_id=1, source_target_pairs={{0,3},{1,0},{2,1},{3,2},{4,7},{5,4},{6,5},{7,6},{8,11},{9,8},{10,9... | collective-permute-start | bytes 4718600 | tf_op jit(solution)/shard_map/ppermute | solution.py:22
  85.4 19.2 %collective-permute-start.2 = (bf16[768,512]{1,0:T(8,128)(2,1)S(1)}, bf16[768,512]{1,0:T(8,128)(2,1)S(1)}, u32[]{:S(2)}, u32[]{:S(2)}) collective-permute-start(bf16[768,512]{1,0:T(8,128)(2,1)S(1)} %slice.75), channel_id=1, source_target_pairs={{0,1},{1,2},{2,3},{3,0},{4,5},{5,6},{6,7},{7,4},{8,9},{9,10},{10,1... | collective-permute-start | bytes 2359304 | tf_op jit(solution)/shard_map/ppermute | solution.py:22
  86.7 18.1 %collective-permute-start.3 = (bf16[768,512]{1,0:T(8,128)(2,1)S(1)}, bf16[768,512]{1,0:T(8,128)(2,1)S(1)}, u32[]{:S(2)}, u32[]{:S(2)}) collective-permute-start(bf16[768,512]{1,0:T(8,128)(2,1)S(1)} %slice.76), channel_id=1, source_target_pairs={{0,3},{1,0},{2,1},{3,2},{4,7},{5,4},{6,5},{7,6},{8,11},{9,8},{10,9... | collective-permute-start | bytes 2359304 | tf_op jit(solution)/shard_map/ppermute | solution.py:22
  134.2 17.3 %collective-permute-start.8 = (bf16[1536,128]{1,0:T(8,128)(2,1)}, bf16[1536,128]{1,0:T(8,128)(2,1)}, u32[]{:S(2)}, u32[]{:S(2)}) collective-permute-start(bf16[1536,128]{1,0:T(8,128)(2,1)} %get-tuple-element.40), channel_id=1, source_target_pairs={{0,3},{1,0},{2,1},{3,2},{4,7},{5,4},{6,5},{7,6},{8,11},{9,8},{10,9... | collective-permute-start | bytes 1179656 | tf_op jit(solution)/shard_map/ppermute | solution.py:22
  138.3 17.6 %collective-permute-start.4 = (bf16[1536,128]{1,0:T(8,128)(2,1)}, bf16[1536,128]{1,0:T(8,128)(2,1)}, u32[]{:S(2)}, u32[]{:S(2)}) collective-permute-start(bf16[1536,128]{1,0:T(8,128)(2,1)} %get-tuple-element.36), channel_id=1, source_target_pairs={{0,1},{1,2},{2,3},{3,0},{4,5},{5,6},{6,7},{7,4},{8,9},{9,10},{10,1... | collective-permute-start | bytes 1179656 | tf_op jit(solution)/shard_map/ppermute | solution.py:22
  138.3 29.9 %collective-permute-start.6 = (bf16[1536,128]{1,0:T(8,128)(2,1)}, bf16[1536,128]{1,0:T(8,128)(2,1)S(1)}, u32[]{:S(2)}, u32[]{:S(2)}) collective-permute-start(bf16[1536,128]{1,0:T(8,128)(2,1)} %get-tuple-element.37), channel_id=1, source_target_pairs={{0,3},{1,0},{2,1},{3,2},{4,7},{5,4},{6,5},{7,6},{8,11},{9,8},{10,9... | collective-permute-start | bytes 1179656 | tf_op jit(solution)/shard_map/ppermute | solution.py:22
  140.9 28.7 %collective-permute-start.7 = (bf16[1536,128]{1,0:T(8,128)(2,1)}, bf16[1536,128]{1,0:T(8,128)(2,1)}, u32[]{:S(2)}, u32[]{:S(2)}) collective-permute-start(bf16[1536,128]{1,0:T(8,128)(2,1)} %get-tuple-element.38), channel_id=1, source_target_pairs={{0,1},{1,2},{2,3},{3,0},{4,5},{5,6},{6,7},{7,4},{8,9},{9,10},{10,1... | collective-permute-start | bytes 1179656 | tf_op jit(solution)/shard_map/ppermute | solution.py:22
  141.0 37.1 %all-to-all-start.2 = ((bf16[32,48,512]{2,1,0:T(8,128)(2,1)}), bf16[32,48,512]{2,1,0:T(8,128)(2,1)S(1)}, u32[]{:S(2)}, u32[]{:S(2)}) async-start(bf16[32,48,512]{2,1,0:T(8,128)(2,1)} %bitcast.9), calls=%async_computation.2 | async-start | bytes 3145728 | tf_op jit(solution)/shard_map/all_to_all | solution.py:26
  152.8 16.8 %collective-permute-start.9 = (bf16[1536,128]{1,0:T(8,128)(2,1)S(1)}, bf16[1536,128]{1,0:T(8,128)(2,1)S(1)}, u32[]{:S(2)}, u32[]{:S(2)}) collective-permute-start(bf16[1536,128]{1,0:T(8,128)(2,1)S(1)} %add_convert_fusion.3), channel_id=1, source_target_pairs={{0,3},{1,0},{2,1},{3,2},{4,7},{5,4},{6,5},{7,6},{8,11},{9,8},{10,9... | collective-permute-start | bytes 1179656 | tf_op jit(solution)/shard_map/ppermute | solution.py:22
  155.8 11.5 %collective-permute-start.10 = (bf16[1536,128]{1,0:T(8,128)(2,1)}, bf16[1536,128]{1,0:T(8,128)(2,1)S(1)}, u32[]{:S(2)}, u32[]{:S(2)}) collective-permute-start(bf16[1536,128]{1,0:T(8,128)(2,1)} %get-tuple-element.47), channel_id=1, source_target_pairs={{0,1},{1,2},{2,3},{3,0},{4,5},{5,6},{6,7},{7,4},{8,9},{9,10},{10,1... | collective-permute-start | bytes 1179656 | tf_op jit(solution)/shard_map/ppermute | solution.py:22
  157.1 18.7 %collective-permute-start.5 = (bf16[1536,128]{1,0:T(8,128)(2,1)S(1)}, bf16[1536,128]{1,0:T(8,128)(2,1)S(1)}, u32[]{:S(2)}, u32[]{:S(2)}) collective-permute-start(bf16[1536,128]{1,0:T(8,128)(2,1)S(1)} %add_convert_fusion.5), channel_id=1, source_target_pairs={{0,1},{1,2},{2,3},{3,0},{4,5},{5,6},{6,7},{7,4},{8,9},{9,10},{10,1... | collective-permute-start | bytes 1179656 | tf_op jit(solution)/shard_map/ppermute | solution.py:22
  167.3 26.8 %collective-permute-start.12 = (bf16[1536,128]{1,0:T(8,128)(2,1)}, bf16[1536,128]{1,0:T(8,128)(2,1)}, u32[]{:S(2)}, u32[]{:S(2)}) collective-permute-start(bf16[1536,128]{1,0:T(8,128)(2,1)} %get-tuple-element.48), channel_id=1, source_target_pairs={{0,3},{1,0},{2,1},{3,2},{4,7},{5,4},{6,5},{7,6},{8,11},{9,8},{10,9... | collective-permute-start | bytes 1179656 | tf_op jit(solution)/shard_map/ppermute | solution.py:22
  168.2 25.9 %collective-permute-start.11 = (bf16[1536,128]{1,0:T(8,128)(2,1)}, bf16[1536,128]{1,0:T(8,128)(2,1)}, u32[]{:S(2)}, u32[]{:S(2)}) collective-permute-start(bf16[1536,128]{1,0:T(8,128)(2,1)} %add_convert_fusion.1), channel_id=1, source_target_pairs={{0,1},{1,2},{2,3},{3,0},{4,5},{5,6},{6,7},{7,4},{8,9},{9,10},{10,1... | collective-permute-start | bytes 1179656 | tf_op jit(solution)/shard_map/ppermute | solution.py:22
  180.7 24.0 %all-to-all-start.3 = ((bf16[32,48,256]{2,1,0:T(8,128)(2,1)}), bf16[32,48,256]{2,1,0:T(8,128)(2,1)S(1)}, u32[]{:S(2)}, u32[]{:S(2)}) async-start(bf16[32,48,256]{2,1,0:T(8,128)(2,1)} %bitcast.11), calls=%async_computation.3 | async-start | bytes 1572864 | tf_op jit(solution)/shard_map/all_to_all | solution.py:26
  190.5 24.4 %collective-permute-start.22 = (f32[2,256]{1,0:T(2,128)S(1)}, f32[2,256]{1,0:T(2,128)S(1)}, u32[]{:S(2)}, u32[]{:S(2)}) collective-permute-start(f32[2,256]{1,0:T(2,128)S(1)} %slice.77), channel_id=1, source_target_pairs={{0,4},{4,8},{8,12},{12,16},{16,20},{20,24},{24,28},{28,32},{32,36}... | collective-permute-start | bytes 6152 | tf_op jit(solution)/shard_map/ppermute | solution.py:17
  205.5 31.4 %copy-start.3 = (bf16[1536,256]{1,0:T(8,128)(2,1)S(1)}, bf16[1536,256]{1,0:T(8,128)(2,1)}, u32[]{:S(2)}) copy-start(bf16[1536,256]{1,0:T(8,128)(2,1)} %get-tuple-element.58) | copy-start | bytes 2359300
  208.1 14.3 %all-to-all-start.4 = ((bf16[32,48,128]{2,1,0:T(8,128)(2,1)}), bf16[32,48,128]{2,1,0:T(8,128)(2,1)S(1)}, u32[]{:S(2)}, u32[]{:S(2)}) async-start(bf16[32,48,128]{2,1,0:T(8,128)(2,1)} %bitcast.13), calls=%async_computation.4 | async-start | bytes 786432 | tf_op jit(solution)/shard_map/all_to_all | solution.py:26
  212.1 20.3 %collective-permute-start.19 = (bf16[384,512]{1,0:T(8,128)(2,1)}, bf16[384,512]{1,0:T(8,128)(2,1)}, u32[]{:S(2)}, u32[]{:S(2)}) collective-permute-start(bf16[384,512]{1,0:T(8,128)(2,1)} %convolution_convert_fusion.2.refs_8_), channel_id=1, source_target_pairs={{0,1},{1,2},{2,3},{3,0},{4,5},{5,6},{6,7},{7,4},{8,9},{9,10},{10,1... | collective-permute-start | bytes 1179656 | tf_op jit(solution)/shard_map/ppermute | solution.py:22
  212.2 20.3 %collective-permute-start.20 = (bf16[384,512]{1,0:T(8,128)(2,1)}, bf16[384,512]{1,0:T(8,128)(2,1)}, u32[]{:S(2)}, u32[]{:S(2)}) collective-permute-start(bf16[384,512]{1,0:T(8,128)(2,1)} %convolution_convert_fusion.2.refs_8_), channel_id=1, source_target_pairs={{0,3},{1,0},{2,1},{3,2},{4,7},{5,4},{6,5},{7,6},{8,11},{9,8},{10,9... | collective-permute-start | bytes 1179656 | tf_op jit(solution)/shard_map/ppermute | solution.py:22
  214.9 17.6 %collective-permute-start.21 = (bf16[384,512]{1,0:T(8,128)(2,1)}, bf16[384,512]{1,0:T(8,128)(2,1)}, u32[]{:S(2)}, u32[]{:S(2)}) collective-permute-start(bf16[384,512]{1,0:T(8,128)(2,1)} %convolution_convert_fusion.2.refs_8_), channel_id=1, source_target_pairs={{0,2},{1,3},{2,0},{3,1},{4,6},{5,7},{6,4},{7,5},{8,10},{9,11},{10,... | collective-permute-start | bytes 1179656 | tf_op jit(solution)/shard_map/ppermute | solution.py:22
  215.0 21.6 %collective-permute-start.13 = (bf16[384,256]{1,0:T(8,128)(2,1)}, bf16[384,256]{1,0:T(8,128)(2,1)S(1)}, u32[]{:S(2)}, u32[]{:S(2)}) collective-permute-start(bf16[384,256]{1,0:T(8,128)(2,1)} %convolution_convert_fusion.3.refs_0_), channel_id=1, source_target_pairs={{0,1},{1,2},{2,3},{3,0},{4,5},{5,6},{6,7},{7,4},{8,9},{9,10},{10,1... | collective-permute-start | bytes 589832 | tf_op jit(solution)/shard_map/ppermute | solution.py:22
  215.7 27.2 %collective-permute-start.14 = (bf16[384,256]{1,0:T(8,128)(2,1)}, bf16[384,256]{1,0:T(8,128)(2,1)}, u32[]{:S(2)}, u32[]{:S(2)}) collective-permute-start(bf16[384,256]{1,0:T(8,128)(2,1)} %convolution_convert_fusion.3.refs_0_), channel_id=1, source_target_pairs={{0,3},{1,0},{2,1},{3,2},{4,7},{5,4},{6,5},{7,6},{8,11},{9,8},{10,9... | collective-permute-start | bytes 589832 | tf_op jit(solution)/shard_map/ppermute | solution.py:22
  232.5 10.4 %collective-permute-start.15 = (bf16[384,256]{1,0:T(8,128)(2,1)}, bf16[384,256]{1,0:T(8,128)(2,1)S(1)}, u32[]{:S(2)}, u32[]{:S(2)}) collective-permute-start(bf16[384,256]{1,0:T(8,128)(2,1)} %convolution_convert_fusion.3.refs_0_), channel_id=1, source_target_pairs={{0,2},{1,3},{2,0},{3,1},{4,6},{5,7},{6,4},{7,5},{8,10},{9,11},{10,... | collective-permute-start | bytes 589832 | tf_op jit(solution)/shard_map/ppermute | solution.py:22
  232.5 11.5 %collective-permute-start.16 = (bf16[384,128]{1,0:T(8,128)(2,1)S(1)}, bf16[384,128]{1,0:T(8,128)(2,1)S(1)}, u32[]{:S(2)}, u32[]{:S(2)}) collective-permute-start(bf16[384,128]{1,0:T(8,128)(2,1)S(1)} %convolution_convert_fusion.4.refs_4_), channel_id=1, source_target_pairs={{0,1},{1,2},{2,3},{3,0},{4,5},{5,6},{6,7},{7,4},{8,9},{9,10},{10,1... | collective-permute-start | bytes 294920 | tf_op jit(solution)/shard_map/ppermute | solution.py:22
  232.5 11.5 %collective-permute-start.17 = (bf16[384,128]{1,0:T(8,128)(2,1)S(1)}, bf16[384,128]{1,0:T(8,128)(2,1)S(1)}, u32[]{:S(2)}, u32[]{:S(2)}) collective-permute-start(bf16[384,128]{1,0:T(8,128)(2,1)S(1)} %convolution_convert_fusion.4.refs_4_), channel_id=1, source_target_pairs={{0,3},{1,0},{2,1},{3,2},{4,7},{5,4},{6,5},{7,6},{8,11},{9,8},{10,9... | collective-permute-start | bytes 294920 | tf_op jit(solution)/shard_map/ppermute | solution.py:22
  236.6 7.4 %collective-permute-start.18 = (bf16[384,128]{1,0:T(8,128)(2,1)S(1)}, bf16[384,128]{1,0:T(8,128)(2,1)S(1)}, u32[]{:S(2)}, u32[]{:S(2)}) collective-permute-start(bf16[384,128]{1,0:T(8,128)(2,1)S(1)} %convolution_convert_fusion.4.refs_4_), channel_id=1, source_target_pairs={{0,2},{1,3},{2,0},{3,1},{4,6},{5,7},{6,4},{7,5},{8,10},{9,11},{10,... | collective-permute-start | bytes 294920 | tf_op jit(solution)/shard_map/ppermute | solution.py:22
  261.8 21.3 %collective-permute-start.23 = (f32[2,256]{1,0:T(2,128)S(1)}, f32[2,256]{1,0:T(2,128)S(1)}, u32[]{:S(2)}, u32[]{:S(2)}) collective-permute-start(f32[2,256]{1,0:T(2,128)S(1)} %slice.80), channel_id=1, source_target_pairs={{4,0},{8,4},{12,8},{16,12},{20,16},{24,20},{28,24},{32,28},{36,32}... | collective-permute-start | bytes 6152 | tf_op jit(solution)/shard_map/ppermute | solution.py:17
  269.7 24.3 %all-to-all-start.5 = ((bf16[32,64,256]{2,1,0:T(8,128)(2,1)}), bf16[32,64,256]{2,1,0:T(8,128)(2,1)S(1)}, u32[]{:S(2)}, u32[]{:S(2)}) async-start(bf16[32,64,256]{2,1,0:T(8,128)(2,1)} %bitcast.22), calls=%async_computation.5 | async-start | bytes 2097152 | tf_op jit(solution)/shard_map/all_to_all | solution.py:26
  (19 other events, 164.0 us)
where the time goes:
time: 297 us; the launch traced here: 295 us
  waiting for transfers between devices  106 us (36%)
  starting transfers between devices  81.9 us (28%)
  matrix products  40.3 us (14%)
  Pallas kernels  38.9 us (13%)
  other arithmetic  13.7 us (5%)
  local copies, waits for them, and re-layouts  12.7 us (4%)
    ppermute x22, waiting for transfers between devices, turned(): lax.ppermute(array, 'tp', [(i, (i + by) % size) for i in range(size)])  72.3 us
    all_to_all x6, starting transfers between devices, exchanged(): return lax.all_to_all(array, 'sp', split_axis=0, concat_axis=0, tiled=True)  46.5 us
    all_to_all x6, waiting for transfers between devices, exchanged(): return lax.all_to_all(array, 'sp', split_axis=0, concat_axis=0, tiled=True)  33.7 us
    ppermute x22, starting transfers between devices, turned(): lax.ppermute(array, 'tp', [(i, (i + by) % size) for i in range(size)])  24 us
    pallas_call x1, Pallas kernels, weighted_rows(): pl.pallas_call(weighted_kernel, grid=(width // part, slots // block), in_...  18.9 us
    pallas_call x1, Pallas kernels, expert_grads(): pl.pallas_call(expert_kernel, grid_spec=pltpu.PrefetchScalarGridSpec(num_...  13.6 us
    ppermute x2, starting transfers between devices, passed_along(): return lax.ppermute(array, axis, pairs)  11.4 us
    dot_general x3, matrix products, per_token(): jnp.dot(token_chooser, array, preferred_element_type=f32).astype(bf16)  6.73 us
  transfers between devices with their start and end apart: 30, of which 12 were waited for; matrix products, arithmetic and copies ran while one was open for 15% of the time, Pallas kernels for 6%

commit v1 on v0

--- a/solution.py
+++ b/solution.py
@@ -88,7 +88,7 @@
 
 def finish(lane, pieces, cotangent, resid_in, norm_gain):
     tokens, width = cotangent.shape
-    block = 64
+    block = 128
 
     def rows(array):
         return pl.BlockSpec((block, array.shape[1]), lambda i, _: (i, 0))
@@ -108,34 +108,150 @@
     )(lane.reshape(1), *pieces, cotangent, resid_in, gain)
 
 
-def weighted_kernel(chooser_ref, cot_ref, weight_ref, out_ref):
-    rows = jnp.dot(chooser_ref[...], cot_ref[...], preferred_element_type=f32)
-    out_ref[...] = (rows * weight_ref[...]).astype(bf16)
-
-
-def weighted_rows(chooser, cotangent, slot_weight):
+along_last = (((1,), (1,)), ((), ()))
+
+
+def slot_pattern(block, at, count, capacity):
+    slot = lax.broadcasted_iota(jnp.int32, (block, count), 0) + at
+    low = lax.broadcasted_iota(jnp.int32, (block, count), 1) * capacity
+    return ((slot >= low) & (slot < low + capacity)).astype(f32).astype(bf16)
+
+
+def rows_kernel(lane_ref, routes_ref, share_ref, resid_ref, gain_ref, *refs):
+    sent_ref, chooser_ref, rank_ref, high_ref, low_ref, normed_ref, turn_ref = refs
+    tokens, quarter = normed_ref.shape
+    experts = rank_ref.shape[1]
+    block = chooser_ref.shape[0]
+    capacity = 4 * tokens // experts
+    step = pl.program_id(0)
+
+    @pl.when(step == 0)
+    def _():
+        at = pl.ds(pl.multiple_of(lane_ref[0] * quarter, 128), quarter)
+        some = 64
+
+        def normalise(i, carry):
+            rows = pl.ds(pl.multiple_of(i * some, some), some)
+            wide = resid_ref[rows, :].astype(f32)
+            inv_rms = lax.rsqrt(jnp.mean(wide * wide, axis=1, keepdims=True) + norm_eps)
+            part = resid_ref[rows, at].astype(f32)
+            normed_ref[rows, :] = (part * inv_rms * gain_ref[:, at]).astype(bf16)
+            return carry
+
+        lax.fori_loop(0, tokens // some, normalise, 0)
+        ids = lax.broadcasted_iota(jnp.int32, (experts, tokens), 0)
+        first = ids == routes_ref[0:1, :]
+        second = ids == routes_ref[1:2, :]
+        named = (first | second).astype(f32)
+        share = jnp.where(first, share_ref[0:1, :], 0.0) + jnp.where(second, share_ref[1:2, :], 0.0)
+        down = lax.broadcasted_iota(jnp.int32, (tokens, tokens), 0)
+        over = lax.broadcasted_iota(jnp.int32, (tokens, tokens), 1)
+        before = (down < over).astype(f32).astype(bf16)
+        same = (over == down).astype(f32).astype(bf16)
+        rank = jnp.dot(named.astype(bf16), before, preferred_element_type=f32)
+        rank = jnp.where(named > 0.0, rank, -1.0).astype(bf16)
+        turn_ref[...] = rank
+        rank_ref[...] = lax.dot_general(
+            same, rank, along_last, preferred_element_type=f32
+        ).astype(bf16)
+        high = share.astype(bf16)
+        high_ref[...] = high
+        low_ref[...] = (share - high.astype(f32)).astype(bf16)
+
+    pattern = slot_pattern(block, step * block, experts, capacity)
+    ranks = jnp.dot(pattern, turn_ref[...], preferred_element_type=f32)
+    slot = lax.broadcasted_iota(jnp.int32, (block, 1), 0) + step * block
+    wanted = lax.rem(slot, capacity).astype(f32)
+    chooser = (ranks == wanted).astype(f32).astype(bf16)
+    chooser_ref[...] = chooser
+    sent_ref[...] = jnp.dot(chooser, normed_ref[...], preferred_element_type=f32).astype(bf16)
+
+
+slot_block = 256
+
+
+def chosen_rows(lane, routes, route_weights, resid_in, norm_gain, experts):
+    tokens, width = resid_in.shape
+    quarter = width // 4
+    slots = 4 * tokens
+
+    def whole(*shape):
+        return pl.BlockSpec(shape, lambda i, _: (0, 0))
+
+    return pl.pallas_call(
+        rows_kernel,
+        grid_spec=pltpu.PrefetchScalarGridSpec(
+            num_scalar_prefetch=1,
+            grid=(slots // slot_block,),
+            in_specs=[whole(2, tokens), whole(2, tokens), whole(tokens, width), whole(1, width)],
+            out_specs=[
+                pl.BlockSpec((slot_block, quarter), lambda i, _: (i, 0)),
+                pl.BlockSpec((slot_block, tokens), lambda i, _: (i, 0)),
+                whole(tokens, experts),
+                whole(experts, tokens),
+                whole(experts, tokens),
+            ],
+            scratch_shapes=[pltpu.VMEM((tokens, quarter), bf16), pltpu.VMEM((experts, tokens), bf16)],
+        ),
+        out_shape=[
+            jax.ShapeDtypeStruct((slots, quarter), bf16),
+            jax.ShapeDtypeStruct((slots, tokens), bf16),
+            jax.ShapeDtypeStruct((tokens, experts), bf16),
+            jax.ShapeDtypeStruct((experts, tokens), bf16),
+            jax.ShapeDtypeStruct((experts, tokens), bf16),
+        ],
+    )(lane.reshape(1), routes.T, route_weights.T, resid_in, norm_gain.reshape(1, width))
+
+
+def weighted_kernel(chooser_ref, cot_ref, rank_ref, high_ref, low_ref, out_ref, token_ref):
+    tokens, experts = rank_ref.shape
+    block = chooser_ref.shape[0]
+    capacity = 4 * tokens // experts
+    at = pl.program_id(0) * block
+    pattern = slot_pattern(block, at, experts, capacity)
+    share = jnp.dot(pattern, high_ref[...], preferred_element_type=f32) + jnp.dot(
+        pattern, low_ref[...], preferred_element_type=f32
+    )
+    chooser = chooser_ref[...]
+    share = jnp.sum(share * chooser.astype(f32), axis=1, keepdims=True)
+    width = out_ref.shape[1]
+    part = 512
+    for i in range(width // part):
+        rows = jnp.dot(
+            chooser, cot_ref[:, i * part : (i + 1) * part], preferred_element_type=f32
+        )
+        out_ref[:, i * part : (i + 1) * part] = (rows * share).astype(bf16)
+    ranks = lax.dot_general(rank_ref[...], pattern, along_last, preferred_element_type=f32)
+    slot = lax.broadcasted_iota(jnp.int32, (1, block), 1) + at
+    token_ref[...] = (ranks == lax.rem(slot, capacity).astype(f32)).astype(f32).astype(bf16)
+
+
+def weighted_rows(chooser, cotangent, rank, high, low):
     slots, tokens = chooser.shape
     width = cotangent.shape[1]
-    block, part = 256, 512
+
+    def whole(array):
+        return pl.BlockSpec(array.shape, lambda i: (0, 0))
+
     return pl.pallas_call(
         weighted_kernel,
-        grid=(width // part, slots // block),
-        in_specs=[
-            pl.BlockSpec((block, tokens), lambda j, i: (i, 0)),
-            pl.BlockSpec((tokens, part), lambda j, i: (0, j)),
-            pl.BlockSpec((block, 1), lambda j, i: (i, 0)),
+        grid=(slots // slot_block,),
+        in_specs=[pl.BlockSpec((slot_block, tokens), lambda i: (i, 0))]
+        + [whole(x) for x in (cotangent, rank, high, low)],
+        out_specs=[
+            pl.BlockSpec((slot_block, width), lambda i: (i, 0)),
+            pl.BlockSpec((tokens, slot_block), lambda i: (0, i)),
         ],
-        out_specs=pl.BlockSpec((block, part), lambda j, i: (i, j)),
-        out_shape=jax.ShapeDtypeStruct((slots, width), bf16),
-    )(chooser, cotangent, slot_weight)
-
-
-along_last = (((1,), (1,)), ((), ()))
+        out_shape=[
+            jax.ShapeDtypeStruct((slots, width), bf16),
+            jax.ShapeDtypeStruct((tokens, slots), bf16),
+        ],
+    )(chooser, cotangent, rank, high, low)
 
 
 def expert_kernel(lane_ref, gate_ref, up_ref, cot_ref, down_ref, gmat_ref, umat_ref, *outs):
-    hidden_ref, dgate_ref, dup_ref, own_ref, direct_ref = outs[:5]
-    further_refs = (outs[5:8], outs[8:11], outs[11:14])
+    hidden_ref, dgate_ref, dup_ref, direct_ref = outs[:4]
+    further_refs = (outs[4:7], outs[7:10], outs[10:13], outs[13:16])
     quarter = gmat_ref.shape[0] // 4
     dhidden = lax.dot_general(
         cot_ref[...], down_ref[...], along_last, preferred_element_type=f32
@@ -159,17 +275,13 @@
         direct_ref[:, pl.ds(pl.multiple_of(place * direct_width, 128), direct_width)] = part[
             :, quarter - direct_width :
         ]
-        if further == 0:
-            own_ref[...] = part[:, : quarter - direct_width]
-        else:
-            for i, ref in enumerate(further_refs[further - 1]):
-                ref[...] = part[:, i * direct_width : (i + 1) * direct_width]
+        for i, ref in enumerate(further_refs[further]):
+            ref[...] = part[:, i * direct_width : (i + 1) * direct_width]
 
 
 def expert_grads(lane, gate_pre, up_pre, entry_cots, down_mat, gate_mat, up_mat):
     slots, width = entry_cots.shape
     inner = gate_pre.shape[1]
-    quarter = width // 4
     block = 256
 
     def rows(size):
@@ -178,7 +290,7 @@
     def whole(array):
         return pl.BlockSpec(array.shape, lambda i, _: (0, 0))
 
-    sizes = [inner] * 3 + [quarter - direct_width, 4 * direct_width] + [direct_width] * 9
+    sizes = [inner] * 3 + [4 * direct_width] + [direct_width] * 12
     return pl.pallas_call(
         expert_kernel,
         grid_spec=pltpu.PrefetchScalarGridSpec(
@@ -217,38 +329,13 @@
     quarter = model_width // lanes
     gate_mat, up_mat, down_mat = gate_weight[0], up_weight[0], down_weight[0]
 
-    expert_ids = jnp.arange(expert_total, dtype=jnp.int32)[:, None]
-    first = routes[:, 0][None, :] == expert_ids
-    second = routes[:, 1][None, :] == expert_ids
-    named = first | second
-    order = jnp.arange(token_count, dtype=jnp.int32)
-    earlier_mask = (order[:, None] < order[None, :]).astype(bf16)
-    rank = jnp.dot(named.astype(bf16), earlier_mask, preferred_element_type=f32).astype(jnp.int32)
-    rank = jnp.where(named, rank, -1)
-    in_slot = rank[:, None, :] == jnp.arange(capacity, dtype=jnp.int32)[None, :, None]
-    weight_of = jnp.where(first, route_weights[:, 0][None, :], 0.0) + jnp.where(
-        second, route_weights[:, 1][None, :], 0.0
-    )
-    slot_weight = jnp.sum(jnp.where(in_slot, weight_of[:, None, :], 0.0), axis=2).reshape(slots, 1)
-    chooser = in_slot.astype(bf16).reshape(slots, token_count)
-    spread = (jnp.arange(slots, dtype=jnp.int32) // capacity)[None, :] == expert_ids
-    slot_ranks = jnp.einsum(
-        "et,es->ts", rank.astype(bf16), spread.astype(bf16), preferred_element_type=f32
-    )
-    slot_order = (jnp.arange(slots, dtype=jnp.int32) % capacity).astype(f32)
-    token_chooser = (slot_ranks == slot_order[None, :]).astype(bf16)
-
-    resid_wide = resid_in.astype(f32)
-    inv_rms = lax.rsqrt(jnp.mean(resid_wide * resid_wide, axis=1, keepdims=True) + norm_eps)
-    resid_part = lax.dynamic_slice_in_dim(resid_in, lane * quarter, quarter, axis=1)
-    gain_part = lax.dynamic_slice_in_dim(norm_gain, lane * quarter, quarter, axis=0)
-    normed_part = (resid_part.astype(f32) * inv_rms * gain_part).astype(bf16)
-    sent_rows = jnp.dot(chooser, normed_part, preferred_element_type=f32).astype(bf16)
+    sent_rows, chooser, rank, high, low = chosen_rows(
+        lane, routes, route_weights, resid_in, norm_gain, expert_total
+    )
     got_part = exchanged(sent_rows.reshape(groups, capacity, quarter)).reshape(slots, quarter)
-    sent_cots = weighted_rows(chooser, cotangent, slot_weight)
-    entry_cots = exchanged(sent_cots.reshape(groups, capacity, model_width)).reshape(
-        slots, model_width
-    )
+    sent_cots, token_chooser = weighted_rows(chooser, cotangent, rank, high, low)
+    entry_cots = exchanged(sent_cots.reshape(groups, capacity, model_width))
+    entry_cots = entry_cots.reshape(slots, model_width)
     entry_rows = placed_columns(lane, (got_part, ring_gather(got_part)), model_width)
 
     mixed = gate_c.astype(f32) * values_u.astype(f32)
@@ -256,10 +343,11 @@
 
     gate_pre = jnp.dot(entry_rows, gate_mat, preferred_element_type=f32)
     up_pre = jnp.dot(entry_rows, up_mat, preferred_element_type=f32)
-    hidden, dgate, dup, own, direct, *others = expert_grads(
+    hidden, dgate, dup, direct, *others = expert_grads(
         lane, gate_pre, up_pre, entry_cots, down_mat, gate_mat, up_mat
     )
-    a_ahead, b_ahead, c_ahead, a_far, b_far, c_far, a_behind, b_behind, c_behind = others
+    a_own, b_own, c_own, a_ahead, b_ahead, c_ahead = others[:6]
+    a_far, b_far, c_far, a_behind, b_behind, c_behind = others[6:]
 
     def back(array):
         return exchanged(array.reshape(groups, capacity, -1)).reshape(slots, -1)
@@ -272,32 +360,23 @@
 
     a_far = turned(a_far, 1)
     b_far = turned(b_far, -1)
+    direct = back(direct)
+    c_ahead, direct = lax.optimization_barrier((c_ahead, direct))
     a_next = turned(a_behind, -1)
     b_prev = turned(b_ahead, 1)
-    direct = per_token(back(direct))
     a_prev = turned(plus(a_ahead, a_far), 1)
     b_next = turned(plus(b_behind, b_far), -1)
-    c_far, c_behind, a_far = lax.optimization_barrier((c_far, c_behind, a_far))
     c_far = turned(c_far, 1)
     c_next = turned(c_behind, -1)
+    grad_down = jnp.einsum("rf,rd->fd", hidden, entry_cots, preferred_element_type=f32)
+    wide = jnp.concatenate([plus(a_own, a_prev, a_next), plus(b_own, b_prev, b_next)], axis=1)
+    c_own, wide = lax.optimization_barrier((c_own, wide))
+    wide = back(wide)
+    direct_parts = lane_gather(per_token(direct))
     c_prev = turned(plus(c_ahead, c_far), 1)
-    pair = 2 * direct_width
-    wide = jnp.concatenate(
-        [
-            plus(own[:, :direct_width], a_prev, a_next),
-            plus(own[:, direct_width:pair], b_prev, b_next),
-        ],
-        axis=1,
-    )
-    own_last = own[:, pair:]
-    wide, direct, own_last, hidden = lax.optimization_barrier((wide, direct, own_last, hidden))
-    grad_down = jnp.einsum("rf,rd->fd", hidden, entry_cots, preferred_element_type=f32)
-    direct_parts = lane_gather(direct)
-    wide = per_token(back(wide))
-    narrow = plus(own_last, c_prev, c_next)
-    narrow, wide = lax.optimization_barrier((narrow, wide))
-    wide_parts = lane_gather(wide)
-    narrow_parts = lane_gather(per_token(back(narrow)))
+    narrow = back(plus(c_own, c_prev, c_next))
+    wide_parts = lane_gather(per_token(wide))
+    narrow_parts = lane_gather(per_token(narrow))
     pieces = (*wide_parts, *narrow_parts, *direct_parts)
     grad_resid = finish(lane, pieces, cotangent, resid_in, norm_gain)
 

time: 297 us -> 303 us (1.020)
  waiting for transfers between devices: 106 us -> 123 us
  starting transfers between devices: 81.9 us -> 86.8 us
  matrix products: 40.3 us -> 35.5 us
  Pallas kernels: 38.9 us -> 34.5 us
  local copies, waits for them, and re-layouts: 12.7 us -> 8.37 us
    ppermute x22, waiting for transfers between devices: 72.3 us -> 93.7 us  [turned(): lax.ppermute(array, 'tp', [(i, (i + by) % size) for i in range(size)])]
    all_to_all x6, waiting for transfers between devices: 33.7 us -> 24.6 us  [exchanged(): return lax.all_to_all(array, 'sp', split_axis=0, concat_axis=0, tiled=True)]
    all_to_all x6, starting transfers between devices: 46.5 us -> 53.1 us  [exchanged(): return lax.all_to_all(array, 'sp', split_axis=0, concat_axis=0, tiled=True)]
    dot_general x3 -> x0, matrix products: 4.71 us -> none  [the longest x1 3.23 us: on_device(): jnp.dot(chooser, normed_part, preferred_element_type=f32).astype(bf16)]
    ppermute x2, waiting for transfers between devices: 0.01 us -> 4.34 us  [passed_along(): return lax.ppermute(array, axis, pairs)]
    pallas_call x1 -> x2, Pallas kernels: 18.9 us -> 15.1 us  [the longest x1 8.58 us: weighted_rows(): pl.pallas_call(weighted_kernel, grid=(slots // slot_block,), in_specs=[pl...]
    ppermute x2, starting transfers between devices: 11.4 us -> 8.15 us  [passed_along(): return lax.ppermute(array, axis, pairs)]
    convert_element_type x5 -> x6, other arithmetic: 6.63 us -> 7.91 us  [plus(): return sum((array.astype(f32) for array in arrays)).astype(bf16)]
  transfers between devices with their start and end apart: 30 -> 30, of which waited for: 12 -> 14; matrix products, arithmetic and copies ran while one was open for 15% -> 15% of each run, Pallas kernels for 6% -> 3%
where the time goes in v1:
time: 303 us; the launch traced here: 302 us
  waiting for transfers between devices  123 us (41%)
  starting transfers between devices  86.8 us (29%)
  matrix products  35.5 us (12%)
  Pallas kernels  34.5 us (11%)
  other arithmetic  12.6 us (4%)
  local copies, waits for them, and re-layouts  8.37 us (3%)
    ppermute x22, waiting for transfers between devices, turned(): lax.ppermute(array, 'tp', [(i, (i + by) % size) for i in range(size)])  93.7 us
    all_to_all x6, starting transfers between devices, exchanged(): return lax.all_to_all(array, 'sp', split_axis=0, concat_axis=0, tiled=True)  53.1 us
    ppermute x22, starting transfers between devices, turned(): lax.ppermute(array, 'tp', [(i, (i + by) % size) for i in range(size)])  25.6 us
    all_to_all x6, waiting for transfers between devices, exchanged(): return lax.all_to_all(array, 'sp', split_axis=0, concat_axis=0, tiled=True)  24.6 us
    pallas_call x1, Pallas kernels, expert_grads(): pl.pallas_call(expert_kernel, grid_spec=pltpu.PrefetchScalarGridSpec(num_...  13.6 us
    pallas_call x1, Pallas kernels, weighted_rows(): pl.pallas_call(weighted_kernel, grid=(slots // slot_block,), in_specs=[pl...  8.58 us
    ppermute x2, starting transfers between devices, passed_along(): return lax.ppermute(array, axis, pairs)  8.15 us
    convert_element_type x6, other arithmetic, plus(): return sum((array.astype(f32) for array in arrays)).astype(bf16)  7.91 us
  transfers between devices with their start and end apart: 30, of which 14 were waited for; matrix products, arithmetic and copies ran while one was open for 15% of the time, Pallas kernels for 3%

profile of v1, /device:TPU:1, one launch (start us, length us, event | category | flops | bytes accessed | tf_op | source)
XLA Modules:
  0.0 301.6 jit_solution(8909976915629383091)
XLA Ops:
  0.7 6.5 %shard_map.188 = (bf16[1536,512]{1,0:T(8,128)(2,1)}, bf16[1536,384]{1,0:T(8,128)(2,1)}, bf16[384,32]{1,0:T(8,128)(2,1)}, bf16[32,384]{1,0:T(8,128)(2,1)}, bf16[32,384]{1,0:T(8,128)(2,1)}) custom-call(s32[1]{0:T(128)} %bitcast.lane_ref, s32[2,384]{1,0:T(2,128)} %bitcast.67, f32[2,384]{1,0:T(2,128)} %bitcast.68, bf16[384,2048]{1,0:T(8,128)(2,1)} %refs_13_.1, ...), custom_call_target="tpu_custom_call" | custom-call | tf_op jit(solution)/shard_map/pallas_call | solution.py:181
  7.2 9.6 %all-to-all-start = ((bf16[32,48,512]{2,1,0:T(8,128)(2,1)}), bf16[32,48,512]{2,1,0:T(8,128)(2,1)S(1)}, u32[]{:S(2)}, u32[]{:S(2)}) async-start(bf16[32,48,512]{2,1,0:T(8,128)(2,1)} %bitcast.53), calls=%async_computation | async-start | bytes 3145728 | tf_op jit(solution)/shard_map/all_to_all | solution.py:26
  16.8 8.6 %shard_map.189 = (bf16[1536,2048]{1,0:T(8,128)(2,1)}, bf16[384,1536]{1,0:T(8,128)(2,1)}) custom-call(bf16[1536,384]{1,0:T(8,128)(2,1)} %get-tuple-element.39.chooser_ref, bf16[384,2048]{1,0:T(8,128)(2,1)} %refs_12_.1, bf16[384,32]{1,0:T(8,128)(2,1)} %get-tuple-element.40.rank_ref, bf16[32,384]{1,0:T(8,128)(2,1)} %get-tuple-element.41.high_ref, ...), custom_call_target="tpu_custom_call" | custom-call | tf_op jit(solution)/shard_map/pallas_call | solution.py:236
  25.4 13.6 %all-to-all-done = bf16[32,48,512]{2,1,0:T(8,128)(2,1)S(1)} async-done(((bf16[32,48,512]{2,1,0:T(8,128)(2,1)}), bf16[32,48,512]{2,1,0:T(8,128)(2,1)S(1)}, u32[]{:S(2)}, u32[]{:S(2)}) %all-to-all-start) | async-done | bytes 1572896 | tf_op jit(solution)/shard_map/all_to_all | solution.py:26
  39.0 6.5 %all-to-all-start.1 = ((bf16[32,48,2048]{2,1,0:T(8,128)(2,1)}), bf16[32,48,2048]{2,1,0:T(8,128)(2,1)}, u32[]{:S(2)}, u32[]{:S(2)}) async-start(bf16[32,48,2048]{2,1,0:T(8,128)(2,1)} %bitcast.47), calls=%async_computation.1 | async-start | bytes 12582912 | tf_op jit(solution)/shard_map/all_to_all | solution.py:26
  48.2 34.2 %collective-permute-done = bf16[1536,512]{1,0:T(8,128)(2,1)} collective-permute-done((bf16[1536,512]{1,0:T(8,128)(2,1)S(1)}, bf16[1536,512]{1,0:T(8,128)(2,1)}, u32[]{:S(2)}, u32[]{:S(2)}) %collective-permute-start) | collective-permute-done | bytes 1572896 | tf_op jit(solution)/shard_map/ppermute | solution.py:22
  84.8 2.7 collective-permute-start.3
  92.0 10.8 %collective-permute-done.2 = bf16[768,512]{1,0:T(8,128)(2,1)S(1)} collective-permute-done((bf16[768,512]{1,0:T(8,128)(2,1)S(1)}, bf16[768,512]{1,0:T(8,128)(2,1)S(1)}, u32[]{:S(2)}, u32[]{:S(2)}) %collective-permute-start.2) | collective-permute-done | bytes 786464 | tf_op jit(solution)/shard_map/ppermute | solution.py:22
  103.1 3.2 %fusion.16.gate_ref = f32[1536,256]{1,0:T(8,128)} fusion(bf16[1536,2048]{1,0:T(8,128)(2,1)S(1)} %constant_dynamic-update-slice_fusion.4, bf16[1,2048,256]{2,1,0:T(8,128)(2,1)S(1)} %copy-done.7), kind=kOutput, calls=%fused_computation.46 | convolution fusion | flops 1610612736 | bytes 8912896 | tf_op jit(solution)/shard_map/dot_general | solution.py:344
  106.3 3.0 fusion.14.up_ref
  109.3 9.5 %all-to-all-done.1 = bf16[32,48,2048]{2,1,0:T(8,128)(2,1)} async-done(((bf16[32,48,2048]{2,1,0:T(8,128)(2,1)}), bf16[32,48,2048]{2,1,0:T(8,128)(2,1)}, u32[]{:S(2)}, u32[]{:S(2)}) %all-to-all-start.1) | async-done | bytes 6291488 | tf_op jit(solution)/shard_map/all_to_all | solution.py:26
  118.8 13.6 %shard_map.190 = (bf16[1536,256]{1,0:T(8,128)(2,1)}, bf16[1536,256]{1,0:T(8,128)(2,1)}, bf16[1536,256]{1,0:T(8,128)(2,1)}, bf16[1536,512]{1,0:T(8,128)(2,1)}, bf...) custom-call(s32[1]{0:T(128)} %bitcast.lane_ref, ...), custom_call_target="tpu_custom_call" | custom-call | tf_op jit(solution)/shard_map/pallas_call | solution.py:294
  135.0 5.8 %collective-permute-start.22 = (f32[2,256]{1,0:T(2,128)S(1)}, f32[2,256]{1,0:T(2,128)S(1)}, u32[]{:S(2)}, u32[]{:S(2)}) collective-permute-start(f32[2,256]{1,0:T(2,128)S(1)} %slice.49), channel_id=1, source_target_pairs={{0,4},{4,8},{8,12},{12,16},{16,20},{20,24},{24,28},{28,32},{32,36}... | collective-permute-start | bytes 6152 | tf_op jit(solution)/shard_map/ppermute | solution.py:17
  143.6 6.3 %all-to-all-start.3 = ((bf16[32,48,512]{2,1,0:T(8,128)(2,1)}), bf16[32,48,512]{2,1,0:T(8,128)(2,1)S(1)}, u32[]{:S(2)}, u32[]{:S(2)}) async-start(bf16[32,48,512]{2,1,0:T(8,128)(2,1)} %bitcast.52), calls=%async_computation.3 | async-start | bytes 3145728 | tf_op jit(solution)/shard_map/all_to_all | solution.py:26
  149.9 2.9 collective-permute-start.15
  154.1 6.7 %collective-permute-done.4 = bf16[1536,128]{1,0:T(8,128)(2,1)} collective-permute-done((bf16[1536,128]{1,0:T(8,128)(2,1)}, bf16[1536,128]{1,0:T(8,128)(2,1)}, u32[]{:S(2)}, u32[]{:S(2)}) %collective-permute-start.4) | collective-permute-done | bytes 393248 | tf_op jit(solution)/shard_map/ppermute | solution.py:22
  163.5 6.4 %collective-permute-done.9 = bf16[1536,128]{1,0:T(8,128)(2,1)S(1)} collective-permute-done((bf16[1536,128]{1,0:T(8,128)(2,1)S(1)}, bf16[1536,128]{1,0:T(8,128)(2,1)S(1)}, u32[]{:S(2)}, u32[]{:S(2)}) %collective-permute-start.9) | collective-permute-done | bytes 393248 | tf_op jit(solution)/shard_map/ppermute | solution.py:22
  171.6 9.4 %collective-permute-done.5 = bf16[1536,128]{1,0:T(8,128)(2,1)S(1)} collective-permute-done((bf16[1536,128]{1,0:T(8,128)(2,1)S(1)}, bf16[1536,128]{1,0:T(8,128)(2,1)S(1)}, u32[]{:S(2)}, u32[]{:S(2)}) %collective-permute-start.5) | collective-permute-done | bytes 393248 | tf_op jit(solution)/shard_map/ppermute | solution.py:22
  183.2 9.1 %all-to-all-start.2 = ((bf16[32,48,256]{2,1,0:T(8,128)(2,1)}), bf16[32,48,256]{2,1,0:T(8,128)(2,1)}, u32[]{:S(2)}, u32[]{:S(2)}) async-start(bf16[32,48,256]{2,1,0:T(8,128)(2,1)} %bitcast.11), calls=%async_computation.2 | async-start | bytes 1572864 | tf_op jit(solution)/shard_map/all_to_all | solution.py:26
  193.7 11.5 %collective-permute-done.14 = bf16[1536,128]{1,0:T(8,128)(2,1)S(1)} collective-permute-done((bf16[1536,128]{1,0:T(8,128)(2,1)S(1)}, bf16[1536,128]{1,0:T(8,128)(2,1)S(1)}, u32[]{:S(2)}, u32[]{:S(2)}) %collective-permute-start.14) | collective-permute-done | bytes 393248 | tf_op jit(solution)/shard_map/ppermute | solution.py:22
  207.2 8.0 %all-to-all-start.4 = ((bf16[32,48,128]{2,1,0:T(8,128)(2,1)}), bf16[32,48,128]{2,1,0:T(8,128)(2,1)S(1)}, u32[]{:S(2)}, u32[]{:S(2)}) async-start(bf16[32,48,128]{2,1,0:T(8,128)(2,1)} %bitcast.15), calls=%async_computation.4 | async-start | bytes 786432 | tf_op jit(solution)/shard_map/all_to_all | solution.py:26
  215.3 2.9 convolution_convert_fusion.1.refs_8_
  218.2 2.7 collective-permute-start.20
  223.1 2.7 collective-permute-start.11
  227.6 11.0 %collective-permute-done.10.refs_1_ = bf16[384,256]{1,0:T(8,128)(2,1)} collective-permute-done((bf16[384,256]{1,0:T(8,128)(2,1)}, bf16[384,256]{1,0:T(8,128)(2,1)}, u32[]{:S(2)}, u32[]{:S(2)}) %collective-permute-start.10) | collective-permute-done | bytes 196640 | tf_op jit(solution)/shard_map/ppermute | solution.py:22
  243.0 5.9 %convolution_bitcast_fusion = f32[1,256,2048]{2,1,0:T(8,128)} fusion(bf16[1536,256]{1,0:T(8,128)(2,1)S(1)} %copy-done.3, bf16[1536,2048]{1,0:T(8,128)(2,1)} %bitcast.9.cot_ref), kind=kOutput, calls=%fused_computation | convolution fusion | flops 1610612736 | bytes 9175040 | tf_op jit(solution)/shard_map/rf,rd->fd/dot_general | solution.py:371
  254.0 5.7 %shard_map.191 = bf16[384,2048]{1,0:T(8,128)(2,1)} custom-call(s32[1]{0:T(128)} %bitcast.lane_ref, bf16[384,256]{1,0:T(8,128)(2,1)} %convolution_convert_fusion.2.refs_0_, bf16[384,256]{1,0:T(8,128)(2,1)} %collective-permute-done.10.refs_1_, bf16[384,256]{1,0:T(8,128)(2,1)} %collective-permute-done.11.refs_2_, ...), custom_call_target="tpu_custom_call" | custom-call | tf_op jit(solution)/shard_map/pallas_call | solution.py:97
  259.7 3.2 %convolution_convert_fusion = bf16[2048,256]{1,0:T(8,128)(2,1)} fusion(bf16[384,2048]{1,0:T(8,128)(2,1)} %shard_map.191, f32[384,256]{1,0:T(8,128)S(1)} %fusion.7, bf16[384,256]{1,0:T(8,128)(2,1)S(1)} %copy-done.20), kind=kOutput, calls=%fused_computation.2 | convolution fusion | flops 403472384 | bytes 3211264 | tf_op jit(solution)/shard_map/td,tc->dc/dot_general | solution.py:390
  263.0 6.0 %fusion.20 = f32[2048,256]{1,0:T(8,128)} fusion(bf16[1536,2048]{1,0:T(8,128)(2,1)} %copy-done.2, bf16[1536,256]{1,0:T(8,128)(2,1)S(1)} %copy-done.26), kind=kOutput, calls=%fused_computation.49 | convolution fusion | flops 1610612736 | bytes 9175040 | tf_op jit(solution)/shard_map/rd,rf->df/dot_general | solution.py:394
  269.0 13.6 %all-to-all-start.5 = ((bf16[32,64,256]{2,1,0:T(8,128)(2,1)}), bf16[32,64,256]{2,1,0:T(8,128)(2,1)}, u32[]{:S(2)}, u32[]{:S(2)}) async-start(bf16[32,64,256]{2,1,0:T(8,128)(2,1)} %bitcast.58), calls=%async_computation.5 | async-start | bytes 2097152 | tf_op jit(solution)/shard_map/all_to_all | solution.py:26
  286.2 6.0 %convolution_bitcast_fusion.1 = f32[1,2048,256]{2,1,0:T(8,128)} fusion(bf16[1536,2048]{1,0:T(8,128)(2,1)} %copy-done.2, bf16[1536,256]{1,0:T(8,128)(2,1)S(1)} %copy-done.25), kind=kOutput, calls=%fused_computation.1 | convolution fusion | flops 1610612736 | bytes 9175040 | tf_op jit(solution)/shard_map/rd,rf->df/dot_general | solution.py:396
  292.2 4.3 %collective-permute-done.23 = f32[2,256]{1,0:T(2,128)S(1)} collective-permute-done((f32[2,256]{1,0:T(2,128)S(1)}, f32[2,256]{1,0:T(2,128)S(1)}, u32[]{:S(2)}, u32[]{:S(2)}) %collective-permute-start.23) | collective-permute-done | bytes 2080 | tf_op jit(solution)/shard_map/ppermute | solution.py:17
  (119 shorter events, 48.5 us)
Async XLA Ops:
  0.6 281.9 %copy-start = (bf16[2048,256]{1,0:T(8,128)(2,1)S(1)}, bf16[2048,256]{1,0:T(8,128)(2,1)}, u32[]{:S(2)}) copy-start(bf16[2048,256]{1,0:T(8,128)(2,1)} %param.21) | copy-start | bytes 3145732
  7.2 31.8 %all-to-all-start = ((bf16[32,48,512]{2,1,0:T(8,128)(2,1)}), bf16[32,48,512]{2,1,0:T(8,128)(2,1)S(1)}, u32[]{:S(2)}, u32[]{:S(2)}) async-start(bf16[32,48,512]{2,1,0:T(8,128)(2,1)} %bitcast.53), calls=%async_computation | async-start | bytes 3145728 | tf_op jit(solution)/shard_map/all_to_all | solution.py:26
  39.0 79.8 %all-to-all-start.1 = ((bf16[32,48,2048]{2,1,0:T(8,128)(2,1)}), bf16[32,48,2048]{2,1,0:T(8,128)(2,1)}, u32[]{:S(2)}, u32[]{:S(2)}) async-start(bf16[32,48,2048]{2,1,0:T(8,128)(2,1)} %bitcast.47), calls=%async_computation.1 | async-start | bytes 12582912 | tf_op jit(solution)/shard_map/all_to_all | solution.py:26
  45.5 36.9 %collective-permute-start = (bf16[1536,512]{1,0:T(8,128)(2,1)S(1)}, bf16[1536,512]{1,0:T(8,128)(2,1)}, u32[]{:S(2)}, u32[]{:S(2)}) collective-permute-start(bf16[1536,512]{1,0:T(8,128)(2,1)S(1)} %bitcast.48), channel_id=1, source_target_pairs={{0,1},{1,2},{2,3},{3,0},{4,5},{5,6},{6,7},{7,4},{8,9},{9,10},{10,1... | collective-permute-start | bytes 4718600 | tf_op jit(solution)/shard_map/ppermute | solution.py:22
  46.7 36.9 %collective-permute-start.1 = (bf16[1536,512]{1,0:T(8,128)(2,1)S(1)}, bf16[1536,512]{1,0:T(8,128)(2,1)}, u32[]{:S(2)}, u32[]{:S(2)}) collective-permute-start(bf16[1536,512]{1,0:T(8,128)(2,1)S(1)} %bitcast.49), channel_id=1, source_target_pairs={{0,3},{1,0},{2,1},{3,2},{4,7},{5,4},{6,5},{7,6},{8,11},{9,8},{10,9... | collective-permute-start | bytes 4718600 | tf_op jit(solution)/shard_map/ppermute | solution.py:22
  83.6 19.2 %collective-permute-start.2 = (bf16[768,512]{1,0:T(8,128)(2,1)S(1)}, bf16[768,512]{1,0:T(8,128)(2,1)S(1)}, u32[]{:S(2)}, u32[]{:S(2)}) collective-permute-start(bf16[768,512]{1,0:T(8,128)(2,1)S(1)} %slice.47), channel_id=1, source_target_pairs={{0,1},{1,2},{2,3},{3,0},{4,5},{5,6},{6,7},{7,4},{8,9},{9,10},{10,1... | collective-permute-start | bytes 2359304 | tf_op jit(solution)/shard_map/ppermute | solution.py:22
  84.8 18.1 %collective-permute-start.3 = (bf16[768,512]{1,0:T(8,128)(2,1)S(1)}, bf16[768,512]{1,0:T(8,128)(2,1)S(1)}, u32[]{:S(2)}, u32[]{:S(2)}) collective-permute-start(bf16[768,512]{1,0:T(8,128)(2,1)S(1)} %slice.48), channel_id=1, source_target_pairs={{0,3},{1,0},{2,1},{3,2},{4,7},{5,4},{6,5},{7,6},{8,11},{9,8},{10,9... | collective-permute-start | bytes 2359304 | tf_op jit(solution)/shard_map/ppermute | solution.py:22
  132.4 17.5 %collective-permute-start.8 = (bf16[1536,128]{1,0:T(8,128)(2,1)}, bf16[1536,128]{1,0:T(8,128)(2,1)}, u32[]{:S(2)}, u32[]{:S(2)}) collective-permute-start(bf16[1536,128]{1,0:T(8,128)(2,1)} %get-tuple-element.54), channel_id=1, source_target_pairs={{0,3},{1,0},{2,1},{3,2},{4,7},{5,4},{6,5},{7,6},{8,11},{9,8},{10,9... | collective-permute-start | bytes 1179656 | tf_op jit(solution)/shard_map/ppermute | solution.py:22
  135.0 58.5 %collective-permute-start.22 = (f32[2,256]{1,0:T(2,128)S(1)}, f32[2,256]{1,0:T(2,128)S(1)}, u32[]{:S(2)}, u32[]{:S(2)}) collective-permute-start(f32[2,256]{1,0:T(2,128)S(1)} %slice.49), channel_id=1, source_target_pairs={{0,4},{4,8},{8,12},{12,16},{16,20},{20,24},{24,28},{28,32},{32,36}... | collective-permute-start | bytes 6152 | tf_op jit(solution)/shard_map/ppermute | solution.py:17
  140.8 21.2 %collective-permute-start.7 = (bf16[1536,128]{1,0:T(8,128)(2,1)}, bf16[1536,128]{1,0:T(8,128)(2,1)}, u32[]{:S(2)}, u32[]{:S(2)}) collective-permute-start(bf16[1536,128]{1,0:T(8,128)(2,1)} %get-tuple-element.52), channel_id=1, source_target_pairs={{0,1},{1,2},{2,3},{3,0},{4,5},{5,6},{6,7},{7,4},{8,9},{9,10},{10,1... | collective-permute-start | bytes 1179656 | tf_op jit(solution)/shard_map/ppermute | solution.py:22
  140.9 30.7 %collective-permute-start.6 = (bf16[1536,128]{1,0:T(8,128)(2,1)}, bf16[1536,128]{1,0:T(8,128)(2,1)}, u32[]{:S(2)}, u32[]{:S(2)}) collective-permute-start(bf16[1536,128]{1,0:T(8,128)(2,1)} %get-tuple-element.50), channel_id=1, source_target_pairs={{0,3},{1,0},{2,1},{3,2},{4,7},{5,4},{6,5},{7,6},{8,11},{9,8},{10,9... | collective-permute-start | bytes 1179656 | tf_op jit(solution)/shard_map/ppermute | solution.py:22
  143.6 17.2 %collective-permute-start.4 = (bf16[1536,128]{1,0:T(8,128)(2,1)}, bf16[1536,128]{1,0:T(8,128)(2,1)}, u32[]{:S(2)}, u32[]{:S(2)}) collective-permute-start(bf16[1536,128]{1,0:T(8,128)(2,1)} %get-tuple-element.49), channel_id=1, source_target_pairs={{0,1},{1,2},{2,3},{3,0},{4,5},{5,6},{6,7},{7,4},{8,9},{9,10},{10,1... | collective-permute-start | bytes 1179656 | tf_op jit(solution)/shard_map/ppermute | solution.py:22
  143.6 39.6 %all-to-all-start.3 = ((bf16[32,48,512]{2,1,0:T(8,128)(2,1)}), bf16[32,48,512]{2,1,0:T(8,128)(2,1)S(1)}, u32[]{:S(2)}, u32[]{:S(2)}) async-start(bf16[32,48,512]{2,1,0:T(8,128)(2,1)} %bitcast.52), calls=%async_computation.3 | async-start | bytes 3145728 | tf_op jit(solution)/shard_map/all_to_all | solution.py:26
  149.9 31.1 %copy-start.18 = (bf16[1536,128]{1,0:T(8,128)(2,1)S(1)}, bf16[1536,128]{1,0:T(8,128)(2,1)}, u32[]{:S(2)}) copy-start(bf16[1536,128]{1,0:T(8,128)(2,1)} %get-tuple-element.47) | copy-start | bytes 1179652
  149.9 43.8 %collective-permute-start.15 = (bf16[1536,128]{1,0:T(8,128)(2,1)}, bf16[1536,128]{1,0:T(8,128)(2,1)}, u32[]{:S(2)}, u32[]{:S(2)}) collective-permute-start(bf16[1536,128]{1,0:T(8,128)(2,1)} %get-tuple-element.61), channel_id=1, source_target_pairs={{0,3},{1,0},{2,1},{3,2},{4,7},{5,4},{6,5},{7,6},{8,11},{9,8},{10,9... | collective-permute-start | bytes 1179656 | tf_op jit(solution)/shard_map/ppermute | solution.py:22
  160.8 9.2 %collective-permute-start.9 = (bf16[1536,128]{1,0:T(8,128)(2,1)S(1)}, bf16[1536,128]{1,0:T(8,128)(2,1)S(1)}, u32[]{:S(2)}, u32[]{:S(2)}) collective-permute-start(bf16[1536,128]{1,0:T(8,128)(2,1)S(1)} %add_convert_fusion.3), channel_id=1, source_target_pairs={{0,3},{1,0},{2,1},{3,2},{4,7},{5,4},{6,5},{7,6},{8,11},{9,8},{10,9... | collective-permute-start | bytes 1179656 | tf_op jit(solution)/shard_map/ppermute | solution.py:22
  162.0 30.3 %collective-permute-start.13 = (bf16[1536,128]{1,0:T(8,128)(2,1)}, bf16[1536,128]{1,0:T(8,128)(2,1)}, u32[]{:S(2)}, u32[]{:S(2)}) collective-permute-start(bf16[1536,128]{1,0:T(8,128)(2,1)} %get-tuple-element.60), channel_id=1, source_target_pairs={{0,1},{1,2},{2,3},{3,0},{4,5},{5,6},{6,7},{7,4},{8,9},{9,10},{10,1... | collective-permute-start | bytes 1179656 | tf_op jit(solution)/shard_map/ppermute | solution.py:22
  169.9 11.1 %collective-permute-start.5 = (bf16[1536,128]{1,0:T(8,128)(2,1)S(1)}, bf16[1536,128]{1,0:T(8,128)(2,1)S(1)}, u32[]{:S(2)}, u32[]{:S(2)}) collective-permute-start(bf16[1536,128]{1,0:T(8,128)(2,1)S(1)} %add_convert_fusion.5), channel_id=1, source_target_pairs={{0,1},{1,2},{2,3},{3,0},{4,5},{5,6},{6,7},{7,4},{8,9},{9,10},{10,1... | collective-permute-start | bytes 1179656 | tf_op jit(solution)/shard_map/ppermute | solution.py:22
  183.2 24.0 %all-to-all-start.2 = ((bf16[32,48,256]{2,1,0:T(8,128)(2,1)}), bf16[32,48,256]{2,1,0:T(8,128)(2,1)}, u32[]{:S(2)}, u32[]{:S(2)}) async-start(bf16[32,48,256]{2,1,0:T(8,128)(2,1)} %bitcast.11), calls=%async_computation.2 | async-start | bytes 1572864 | tf_op jit(solution)/shard_map/all_to_all | solution.py:26
  193.4 11.8 %collective-permute-start.14 = (bf16[1536,128]{1,0:T(8,128)(2,1)S(1)}, bf16[1536,128]{1,0:T(8,128)(2,1)S(1)}, u32[]{:S(2)}, u32[]{:S(2)}) collective-permute-start(bf16[1536,128]{1,0:T(8,128)(2,1)S(1)} %add_convert_fusion.1), channel_id=1, source_target_pairs={{0,1},{1,2},{2,3},{3,0},{4,5},{5,6},{6,7},{7,4},{8,9},{9,10},{10,1... | collective-permute-start | bytes 1179656 | tf_op jit(solution)/shard_map/ppermute | solution.py:22
  207.2 18.6 %all-to-all-start.4 = ((bf16[32,48,128]{2,1,0:T(8,128)(2,1)}), bf16[32,48,128]{2,1,0:T(8,128)(2,1)S(1)}, u32[]{:S(2)}, u32[]{:S(2)}) async-start(bf16[32,48,128]{2,1,0:T(8,128)(2,1)} %bitcast.15), calls=%async_computation.4 | async-start | bytes 786432 | tf_op jit(solution)/shard_map/all_to_all | solution.py:26
  218.2 23.1 %collective-permute-start.19 = (bf16[384,512]{1,0:T(8,128)(2,1)}, bf16[384,512]{1,0:T(8,128)(2,1)S(1)}, u32[]{:S(2)}, u32[]{:S(2)}) collective-permute-start(bf16[384,512]{1,0:T(8,128)(2,1)} %convolution_convert_fusion.1.refs_8_), channel_id=1, source_target_pairs={{0,1},{1,2},{2,3},{3,0},{4,5},{5,6},{6,7},{7,4},{8,9},{9,10},{10,1... | collective-permute-start | bytes 1179656 | tf_op jit(solution)/shard_map/ppermute | solution.py:22
  218.2 30.8 %collective-permute-start.20 = (bf16[384,512]{1,0:T(8,128)(2,1)}, bf16[384,512]{1,0:T(8,128)(2,1)S(1)}, u32[]{:S(2)}, u32[]{:S(2)}) collective-permute-start(bf16[384,512]{1,0:T(8,128)(2,1)} %convolution_convert_fusion.1.refs_8_), channel_id=1, source_target_pairs={{0,3},{1,0},{2,1},{3,2},{4,7},{5,4},{6,5},{7,6},{8,11},{9,8},{10,9... | collective-permute-start | bytes 1179656 | tf_op jit(solution)/shard_map/ppermute | solution.py:22
  223.1 15.4 %collective-permute-start.10 = (bf16[384,256]{1,0:T(8,128)(2,1)}, bf16[384,256]{1,0:T(8,128)(2,1)}, u32[]{:S(2)}, u32[]{:S(2)}) collective-permute-start(bf16[384,256]{1,0:T(8,128)(2,1)} %convolution_convert_fusion.2.refs_0_), channel_id=1, source_target_pairs={{0,1},{1,2},{2,3},{3,0},{4,5},{5,6},{6,7},{7,4},{8,9},{9,10},{10,1... | collective-permute-start | bytes 589832 | tf_op jit(solution)/shard_map/ppermute | solution.py:22
  223.1 15.4 %collective-permute-start.11 = (bf16[384,256]{1,0:T(8,128)(2,1)}, bf16[384,256]{1,0:T(8,128)(2,1)}, u32[]{:S(2)}, u32[]{:S(2)}) collective-permute-start(bf16[384,256]{1,0:T(8,128)(2,1)} %convolution_convert_fusion.2.refs_0_), channel_id=1, source_target_pairs={{0,3},{1,0},{2,1},{3,2},{4,7},{5,4},{6,5},{7,6},{8,11},{9,8},{10,9... | collective-permute-start | bytes 589832 | tf_op jit(solution)/shard_map/ppermute | solution.py:22
  225.8 12.8 %collective-permute-start.12 = (bf16[384,256]{1,0:T(8,128)(2,1)}, bf16[384,256]{1,0:T(8,128)(2,1)}, u32[]{:S(2)}, u32[]{:S(2)}) collective-permute-start(bf16[384,256]{1,0:T(8,128)(2,1)} %convolution_convert_fusion.2.refs_0_), channel_id=1, source_target_pairs={{0,2},{1,3},{2,0},{3,1},{4,6},{5,7},{6,4},{7,5},{8,10},{9,11},{10,... | collective-permute-start | bytes 589832 | tf_op jit(solution)/shard_map/ppermute | solution.py:22
  238.6 11.4 %collective-permute-start.21 = (bf16[384,512]{1,0:T(8,128)(2,1)}, bf16[384,512]{1,0:T(8,128)(2,1)S(1)}, u32[]{:S(2)}, u32[]{:S(2)}) collective-permute-start(bf16[384,512]{1,0:T(8,128)(2,1)} %convolution_convert_fusion.1.refs_8_), channel_id=1, source_target_pairs={{0,2},{1,3},{2,0},{3,1},{4,6},{5,7},{6,4},{7,5},{8,10},{9,11},{10,... | collective-permute-start | bytes 1179656 | tf_op jit(solution)/shard_map/ppermute | solution.py:22
  238.6 13.3 %collective-permute-start.16 = (bf16[384,128]{1,0:T(8,128)(2,1)S(1)}, bf16[384,128]{1,0:T(8,128)(2,1)S(1)}, u32[]{:S(2)}, u32[]{:S(2)}) collective-permute-start(bf16[384,128]{1,0:T(8,128)(2,1)S(1)} %convolution_convert_fusion.3.refs_4_), channel_id=1, source_target_pairs={{0,1},{1,2},{2,3},{3,0},{4,5},{5,6},{6,7},{7,4},{8,9},{9,10},{10,1... | collective-permute-start | bytes 294920 | tf_op jit(solution)/shard_map/ppermute | solution.py:22
  238.6 13.3 %collective-permute-start.17 = (bf16[384,128]{1,0:T(8,128)(2,1)S(1)}, bf16[384,128]{1,0:T(8,128)(2,1)S(1)}, u32[]{:S(2)}, u32[]{:S(2)}) collective-permute-start(bf16[384,128]{1,0:T(8,128)(2,1)S(1)} %convolution_convert_fusion.3.refs_4_), channel_id=1, source_target_pairs={{0,3},{1,0},{2,1},{3,2},{4,7},{5,4},{6,5},{7,6},{8,11},{9,8},{10,9... | collective-permute-start | bytes 294920 | tf_op jit(solution)/shard_map/ppermute | solution.py:22
  241.3 12.7 %collective-permute-start.18 = (bf16[384,128]{1,0:T(8,128)(2,1)S(1)}, bf16[384,128]{1,0:T(8,128)(2,1)}, u32[]{:S(2)}, u32[]{:S(2)}) collective-permute-start(bf16[384,128]{1,0:T(8,128)(2,1)S(1)} %convolution_convert_fusion.3.refs_4_), channel_id=1, source_target_pairs={{0,2},{1,3},{2,0},{3,1},{4,6},{5,7},{6,4},{7,5},{8,10},{9,11},{10,... | collective-permute-start | bytes 294920 | tf_op jit(solution)/shard_map/ppermute | solution.py:22
  269.0 30.7 %all-to-all-start.5 = ((bf16[32,64,256]{2,1,0:T(8,128)(2,1)}), bf16[32,64,256]{2,1,0:T(8,128)(2,1)}, u32[]{:S(2)}, u32[]{:S(2)}) async-start(bf16[32,64,256]{2,1,0:T(8,128)(2,1)} %bitcast.58), calls=%async_computation.5 | async-start | bytes 2097152 | tf_op jit(solution)/shard_map/all_to_all | solution.py:26
  283.8 12.7 %collective-permute-start.23 = (f32[2,256]{1,0:T(2,128)S(1)}, f32[2,256]{1,0:T(2,128)S(1)}, u32[]{:S(2)}, u32[]{:S(2)}) collective-permute-start(f32[2,256]{1,0:T(2,128)S(1)} %slice.52), channel_id=1, source_target_pairs={{4,0},{8,4},{12,8},{16,12},{20,16},{24,20},{28,24},{32,28},{36,32}... | collective-permute-start | bytes 6152 | tf_op jit(solution)/shard_map/ppermute | solution.py:17
  (25 other events, 272.1 us)

commit v2 on v1

--- a/solution.py
+++ b/solution.py
@@ -35,18 +35,46 @@
     return prev, nxt, far_top, far_low
 
 
-def placed_columns(lane, pieces, width):
-    piece, (prev, nxt, far_top, far_low) = pieces
-    half = piece.shape[0] // 2
-    size = piece.shape[1]
-    lanes = width // size
-    whole = jnp.zeros((piece.shape[0], width), piece.dtype)
-    whole = lax.dynamic_update_slice(whole, piece, (0, lane * size))
-    whole = lax.dynamic_update_slice(whole, prev, (0, ((lane + lanes - 1) % lanes) * size))
-    whole = lax.dynamic_update_slice(whole, nxt, (0, ((lane + 1) % lanes) * size))
-    far = ((lane + 2) % lanes) * size
-    whole = lax.dynamic_update_slice(whole, far_top, (0, far))
-    return lax.dynamic_update_slice(whole, far_low, (half, far))
+def place_kernel(lane_ref, own_ref, prev_ref, next_ref, top_ref, low_ref, out_ref):
+    size = own_ref.shape[1]
+    first_half = pl.program_id(0) < pl.num_programs(0) // 2
+
+    def columns(further):
+        return pl.ds(pl.multiple_of(((lane_ref[0] + further) % 4) * size, 128), size)
+
+    out_ref[:, columns(0)] = own_ref[...]
+    out_ref[:, columns(3)] = prev_ref[...]
+    out_ref[:, columns(1)] = next_ref[...]
+
+    @pl.when(first_half)
+    def _():
+        out_ref[:, columns(2)] = top_ref[...]
+
+    @pl.when(jnp.logical_not(first_half))
+    def _():
+        out_ref[:, columns(2)] = low_ref[...]
+
+
+def placed_columns(lane, piece, others):
+    slots, size = piece.shape
+    block = 192
+    steps = slots // block
+    half = steps // 2
+
+    def rows(where):
+        return pl.BlockSpec((block, size), lambda i, _: (where(i), 0))
+
+    return pl.pallas_call(
+        place_kernel,
+        grid_spec=pltpu.PrefetchScalarGridSpec(
+            num_scalar_prefetch=1,
+            grid=(steps,),
+            in_specs=[rows(lambda i: i)] * 3
+            + [rows(lambda i: jnp.minimum(i, half - 1)), rows(lambda i: jnp.maximum(i - half, 0))],
+            out_specs=pl.BlockSpec((block, 4 * size), lambda i, _: (i, 0)),
+        ),
+        out_shape=jax.ShapeDtypeStruct((slots, 4 * size), piece.dtype),
+    )(lane.reshape(1), piece, *others)
 
 
 def lane_gather(piece):
@@ -65,30 +93,37 @@
     width = grad_ref.shape[1]
     quarter = width // 4
     wide = wide_refs[0].shape[1]
-    for step, wide_ref, narrow_ref in zip(lane_steps, wide_refs, narrow_refs):
-        start = ((lane_ref[0] + (4 + step)) % 4) * quarter
-        grad_ref[:, pl.ds(pl.multiple_of(start, 128), wide)] = wide_ref[...].astype(f32)
-        grad_ref[:, pl.ds(pl.multiple_of(start + wide, 128), direct_width)] = narrow_ref[
-            ...
-        ].astype(f32)
-    direct = sum(ref[...].astype(f32) for ref in direct_refs)
-    for place in range(4):
-        end = (place + 1) * quarter
-        grad_ref[:, end - direct_width : end] = direct[
-            :, place * direct_width : (place + 1) * direct_width
-        ]
-    resid = resid_ref[...].astype(f32)
-    inv_rms = lax.rsqrt(jnp.mean(resid * resid, axis=1, keepdims=True) + norm_eps)
-    scaled = grad_ref[...] * gain_ref[...]
-    inner = jnp.mean(scaled * resid, axis=1, keepdims=True)
-    out_ref[...] = (
-        cot_ref[...].astype(f32) + inv_rms * scaled - resid * (inv_rms**3 * inner)
-    ).astype(bf16)
+    some = grad_ref.shape[0]
+
+    def some_rows(i, carry):
+        rows = pl.ds(pl.multiple_of(i * some, some), some)
+        for step, wide_ref, narrow_ref in zip(lane_steps, wide_refs, narrow_refs):
+            start = ((lane_ref[0] + (4 + step)) % 4) * quarter
+            grad_ref[:, pl.ds(pl.multiple_of(start, 128), wide)] = wide_ref[rows, :].astype(f32)
+            grad_ref[:, pl.ds(pl.multiple_of(start + wide, 128), direct_width)] = narrow_ref[
+                rows, :
+            ].astype(f32)
+        direct = sum(ref[rows, :].astype(f32) for ref in direct_refs)
+        for place in range(4):
+            end = (place + 1) * quarter
+            grad_ref[:, end - direct_width : end] = direct[
+                :, place * direct_width : (place + 1) * direct_width
+            ]
+        resid = resid_ref[rows, :].astype(f32)
+        inv_rms = lax.rsqrt(jnp.mean(resid * resid, axis=1, keepdims=True) + norm_eps)
+        scaled = grad_ref[...] * gain_ref[...]
+        inner = jnp.mean(scaled * resid, axis=1, keepdims=True)
+        out_ref[rows, :] = (
+            cot_ref[rows, :].astype(f32) + inv_rms * scaled - resid * (inv_rms**3 * inner)
+        ).astype(bf16)
+        return carry
+
+    lax.fori_loop(0, out_ref.shape[0] // some, some_rows, 0)
 
 
 def finish(lane, pieces, cotangent, resid_in, norm_gain):
     tokens, width = cotangent.shape
-    block = 128
+    block = 192
 
     def rows(array):
         return pl.BlockSpec((block, array.shape[1]), lambda i, _: (i, 0))
@@ -102,7 +137,7 @@
             in_specs=[rows(x) for x in (*pieces, cotangent, resid_in)]
             + [pl.BlockSpec((1, width), lambda i, _: (0, 0))],
             out_specs=pl.BlockSpec((block, width), lambda i, _: (i, 0)),
-            scratch_shapes=[pltpu.VMEM((block, width), f32)],
+            scratch_shapes=[pltpu.VMEM((32, width), f32)],
         ),
         out_shape=jax.ShapeDtypeStruct((tokens, width), bf16),
     )(lane.reshape(1), *pieces, cotangent, resid_in, gain)
@@ -167,7 +202,7 @@
     sent_ref[...] = jnp.dot(chooser, normed_ref[...], preferred_element_type=f32).astype(bf16)
 
 
-slot_block = 256
+slot_block = 512
 
 
 def chosen_rows(lane, routes, route_weights, resid_in, norm_gain, experts):
@@ -216,11 +251,14 @@
     share = jnp.sum(share * chooser.astype(f32), axis=1, keepdims=True)
     width = out_ref.shape[1]
     part = 512
-    for i in range(width // part):
-        rows = jnp.dot(
-            chooser, cot_ref[:, i * part : (i + 1) * part], preferred_element_type=f32
-        )
-        out_ref[:, i * part : (i + 1) * part] = (rows * share).astype(bf16)
+
+    def columns(i, carry):
+        at = pl.ds(pl.multiple_of(i * part, part), part)
+        rows = jnp.dot(chooser, cot_ref[:, at], preferred_element_type=f32)
+        out_ref[:, at] = (rows * share).astype(bf16)
+        return carry
+
+    lax.fori_loop(0, width // part, columns, 0)
     ranks = lax.dot_general(rank_ref[...], pattern, along_last, preferred_element_type=f32)
     slot = lax.broadcasted_iota(jnp.int32, (1, block), 1) + at
     token_ref[...] = (ranks == lax.rem(slot, capacity).astype(f32)).astype(f32).astype(bf16)
@@ -247,61 +285,6 @@
             jax.ShapeDtypeStruct((tokens, slots), bf16),
         ],
     )(chooser, cotangent, rank, high, low)
-
-
-def expert_kernel(lane_ref, gate_ref, up_ref, cot_ref, down_ref, gmat_ref, umat_ref, *outs):
-    hidden_ref, dgate_ref, dup_ref, direct_ref = outs[:4]
-    further_refs = (outs[4:7], outs[7:10], outs[10:13], outs[13:16])
-    quarter = gmat_ref.shape[0] // 4
-    dhidden = lax.dot_general(
-        cot_ref[...], down_ref[...], along_last, preferred_element_type=f32
-    )
-    gate_pre = gate_ref[...]
-    up_pre = up_ref[...]
-    logistic = jax.nn.sigmoid(gate_pre)
-    activated = gate_pre * logistic
-    hidden_ref[...] = (activated * up_pre).astype(bf16)
-    dgate = (dhidden * up_pre * logistic * (1.0 + gate_pre * (1.0 - logistic))).astype(bf16)
-    dup = (dhidden * activated).astype(bf16)
-    dgate_ref[...] = dgate
-    dup_ref[...] = dup
-    for further in range(4):
-        place = (lane_ref[0] + further) % 4
-        at = pl.ds(pl.multiple_of(place * quarter, 128), quarter)
-        part = lax.dot_general(
-            dgate, gmat_ref[at, :], along_last, preferred_element_type=f32
-        ) + lax.dot_general(dup, umat_ref[at, :], along_last, preferred_element_type=f32)
-        part = part.astype(bf16)
-        direct_ref[:, pl.ds(pl.multiple_of(place * direct_width, 128), direct_width)] = part[
-            :, quarter - direct_width :
-        ]
-        for i, ref in enumerate(further_refs[further]):
-            ref[...] = part[:, i * direct_width : (i + 1) * direct_width]
-
-
-def expert_grads(lane, gate_pre, up_pre, entry_cots, down_mat, gate_mat, up_mat):
-    slots, width = entry_cots.shape
-    inner = gate_pre.shape[1]
-    block = 256
-
-    def rows(size):
-        return pl.BlockSpec((block, size), lambda i, _: (i, 0))
-
-    def whole(array):
-        return pl.BlockSpec(array.shape, lambda i, _: (0, 0))
-
-    sizes = [inner] * 3 + [4 * direct_width] + [direct_width] * 12
-    return pl.pallas_call(
-        expert_kernel,
-        grid_spec=pltpu.PrefetchScalarGridSpec(
-            num_scalar_prefetch=1,
-            grid=(slots // block,),
-            in_specs=[rows(inner), rows(inner), rows(width)]
-            + [whole(x) for x in (down_mat, gate_mat, up_mat)],
-            out_specs=[rows(size) for size in sizes],
-        ),
-        out_shape=[jax.ShapeDtypeStruct((slots, size), bf16) for size in sizes],
-    )(lane.reshape(1), gate_pre, up_pre, entry_cots, down_mat, gate_mat, up_mat)
 
 
 def on_device(
@@ -336,18 +319,27 @@
     sent_cots, token_chooser = weighted_rows(chooser, cotangent, rank, high, low)
     entry_cots = exchanged(sent_cots.reshape(groups, capacity, model_width))
     entry_cots = entry_cots.reshape(slots, model_width)
-    entry_rows = placed_columns(lane, (got_part, ring_gather(got_part)), model_width)
+    entry_rows = placed_columns(lane, got_part, ring_gather(got_part))
 
     mixed = gate_c.astype(f32) * values_u.astype(f32)
     earlier = passed_along(mixed[-2:], "sp", 1)
 
+    both_mat = jnp.concatenate([gate_mat, up_mat], axis=1)
+    direct_mat = both_mat.reshape(lanes, quarter, -1)[:, -direct_width:].reshape(
+        lanes * direct_width, -1
+    )
+    both_mat, direct_mat = lax.optimization_barrier((both_mat, direct_mat))
     gate_pre = jnp.dot(entry_rows, gate_mat, preferred_element_type=f32)
     up_pre = jnp.dot(entry_rows, up_mat, preferred_element_type=f32)
-    hidden, dgate, dup, direct, *others = expert_grads(
-        lane, gate_pre, up_pre, entry_cots, down_mat, gate_mat, up_mat
-    )
-    a_own, b_own, c_own, a_ahead, b_ahead, c_ahead = others[:6]
-    a_far, b_far, c_far, a_behind, b_behind, c_behind = others[6:]
+    logistic = jax.nn.sigmoid(gate_pre)
+    activated = gate_pre * logistic
+    hidden = (activated * up_pre).astype(bf16)
+    slope = up_pre * logistic * (1.0 + gate_pre * (1.0 - logistic))
+    activated, slope, hidden = lax.optimization_barrier((activated, slope, hidden))
+    dhidden = jnp.einsum("rd,fd->rf", entry_cots, down_mat, preferred_element_type=f32)
+    dgate = (dhidden * slope).astype(bf16)
+    dup = (dhidden * activated).astype(bf16)
+    dboth = jnp.concatenate([dgate, dup], axis=1)
 
     def back(array):
         return exchanged(array.reshape(groups, capacity, -1)).reshape(slots, -1)
@@ -358,18 +350,33 @@
     def plus(*arrays):
         return sum(array.astype(f32) for array in arrays).astype(bf16)
 
-    a_far = turned(a_far, 1)
-    b_far = turned(b_far, -1)
-    direct = back(direct)
-    c_ahead, direct = lax.optimization_barrier((c_ahead, direct))
-    a_next = turned(a_behind, -1)
-    b_prev = turned(b_ahead, 1)
-    a_prev = turned(plus(a_ahead, a_far), 1)
-    b_next = turned(plus(b_behind, b_far), -1)
+    def part(further, first, count, rows=slice(None)):
+        at = ((lane + further) % lanes) * quarter + first * direct_width
+        mat = lax.dynamic_slice_in_dim(both_mat, at, count * direct_width, axis=0)
+        return jnp.einsum("rf,df->rd", dboth[rows], mat, preferred_element_type=f32)
+
+    top, low = slice(None, slots // 2), slice(slots // 2, None)
+    a_far = turned(part(2, 0, 2, top).astype(bf16), 1)
+    b_far = turned(part(2, 0, 2, low).astype(bf16), -1)
+    direct = jnp.einsum("rf,df->rd", dboth, direct_mat, preferred_element_type=f32)
+    direct = back(direct.astype(bf16))
+    a_next = turned(part(3, 0, 2, top).astype(bf16), -1)
+    b_prev = turned(part(1, 0, 2, low).astype(bf16), 1)
+    a_prev = turned((part(1, 0, 2, top) + a_far.astype(f32)).astype(bf16), 1)
+    b_next = turned((part(3, 0, 2, low) + b_far.astype(f32)).astype(bf16), -1)
+    c_far, c_behind, own, c_own, c_ahead = (
+        part(*which).astype(bf16)
+        for which in ((2, 2, 1), (3, 2, 1), (0, 0, 2), (0, 2, 1), (1, 2, 1))
+    )
     c_far = turned(c_far, 1)
     c_next = turned(c_behind, -1)
+    c_ahead, direct = lax.optimization_barrier((c_ahead, direct))
     grad_down = jnp.einsum("rf,rd->fd", hidden, entry_cots, preferred_element_type=f32)
-    wide = jnp.concatenate([plus(a_own, a_prev, a_next), plus(b_own, b_prev, b_next)], axis=1)
+    wide = plus(
+        own,
+        jnp.concatenate([a_prev, b_prev], axis=0),
+        jnp.concatenate([a_next, b_next], axis=0),
+    )
     c_own, wide = lax.optimization_barrier((c_own, wide))
     wide = back(wide)
     direct_parts = lane_gather(per_token(direct))
@@ -390,10 +397,10 @@
     out_parts = jnp.einsum("td,tc->dc", grad_resid, merged, preferred_element_type=f32).astype(bf16)
     out_tiles = exchanged(out_parts.reshape(groups, model_width // groups, -1))
     grad_out_weight = jnp.sum(out_tiles.astype(f32), axis=0)
-    dgate, out_parts = lax.optimization_barrier((dgate, out_parts))
-    grad_gate = jnp.einsum("rd,rf->df", entry_rows, dgate, preferred_element_type=f32)
-    late_resid, grad_gate, dup = lax.optimization_barrier((grad_resid, grad_gate, dup))
-    grad_up = jnp.einsum("rd,rf->df", entry_rows, dup, preferred_element_type=f32)
+    late_both, out_parts = lax.optimization_barrier((dboth, out_parts))
+    grad_both = jnp.einsum("rd,rf->df", entry_rows, late_both, preferred_element_type=f32)
+    late_resid, grad_both = lax.optimization_barrier((grad_resid, grad_both))
+    grad_gate, grad_up = jnp.split(grad_both, 2, axis=1)
     dmerged = jnp.dot(late_resid, out_weight, preferred_element_type=f32)
     grad_gate_b = (dmerged * conv).astype(bf16)
     dconv = dmerged * gate_b.astype(f32)

time: 303 us -> 297 us (0.980)
  matrix products: 35.5 us -> 52.9 us
  waiting for transfers between devices: 123 us -> 106 us
  Pallas kernels: 34.5 us -> 28.7 us
    ppermute x22, waiting for transfers between devices: 93.7 us -> 73.9 us  [turned(): lax.ppermute(array, 'tp', [(i, (i + by) % size) for i in range(size)])]
    dot_general x2 -> x14, matrix products: 12 us -> 25.9 us  [the longest x11 9.95 us: part(): return jnp.einsum('rf,df->rd', dboth[rows], mat, preferred_element_type=f32)]
    all_to_all x6, waiting for transfers between devices: 24.6 us -> 32.1 us  [exchanged(): return lax.all_to_all(array, 'sp', split_axis=0, concat_axis=0, tiled=True)]
    pallas_call x1, Pallas kernels: 13.6 us -> 7.84 us  [placed_columns(): pl.pallas_call(place_kernel, grid_spec=pltpu.PrefetchScalarGridSpec(num_s...]
    all_to_all x6, starting transfers between devices: 53.1 us -> 48.3 us  [exchanged(): return lax.all_to_all(array, 'sp', split_axis=0, concat_axis=0, tiled=True)]
    ppermute x2, waiting for transfers between devices: 4.34 us -> 0.01 us  [passed_along(): return lax.ppermute(array, axis, pairs)]
    convert_element_type x6 -> x2, other arithmetic: 7.91 us -> 4.05 us  [plus(): return sum((array.astype(f32) for array in arrays)).astype(bf16)]
    broadcast_in_dim x1, local copies, waits for them, and re-layouts: 0.78 us -> 4.61 us  [on_device(): grad_up[None]]
  transfers between devices with their start and end apart: 30 -> 30, of which waited for: 14 -> 14; matrix products, arithmetic and copies ran while one was open for 15% -> 20% of each run, Pallas kernels for 3% -> 6%
where the time goes in v2:
time: 297 us; the launch traced here: 295 us
  waiting for transfers between devices  106 us (36%)
  starting transfers between devices  86.6 us (29%)
  matrix products  52.9 us (18%)
  Pallas kernels  28.7 us (10%)
  other arithmetic  11.9 us (4%)
  local copies, waits for them, and re-layouts  8.3 us (3%)
    ppermute x22, waiting for transfers between devices, turned(): lax.ppermute(array, 'tp', [(i, (i + by) % size) for i in range(size)])  73.9 us
    all_to_all x6, starting transfers between devices, exchanged(): return lax.all_to_all(array, 'sp', split_axis=0, concat_axis=0, tiled=True)  48.3 us
    all_to_all x6, waiting for transfers between devices, exchanged(): return lax.all_to_all(array, 'sp', split_axis=0, concat_axis=0, tiled=True)  32.1 us
    ppermute x22, starting transfers between devices, turned(): lax.ppermute(array, 'tp', [(i, (i + by) % size) for i in range(size)])  28.6 us
    pallas_call x1, Pallas kernels, weighted_rows(): pl.pallas_call(weighted_kernel, grid=(slots // slot_block,), in_specs=[pl...  10.3 us
    dot_general x11, matrix products, part(): return jnp.einsum('rf,df->rd', dboth[rows], mat, preferred_element_type=f32)  9.95 us
    ppermute x2, starting transfers between devices, passed_along(): return lax.ppermute(array, axis, pairs)  9.64 us
    dot_general x1, matrix products, on_device(): jnp.einsum('rd,rf->df', entry_rows, late_both, preferred_element_type=f32)  8.22 us
  transfers between devices with their start and end apart: 30, of which 14 were waited for; matrix products, arithmetic and copies ran while one was open for 20% of the time, Pallas kernels for 6%

profile of v2, /device:TPU:1, one launch (start us, length us, event | category | flops | bytes accessed | tf_op | source)
XLA Modules:
  0.0 295.4 jit_solution(4985830580476450324)
XLA Ops:
  0.7 5.5 %shard_map.188 = (bf16[1536,512]{1,0:T(8,128)(2,1)}, bf16[1536,384]{1,0:T(8,128)(2,1)}, bf16[384,32]{1,0:T(8,128)(2,1)}, bf16[32,384]{1,0:T(8,128)(2,1)}, bf16[32,384]{1,0:T(8,128)(2,1)}) custom-call(s32[1]{0:T(128)} %bitcast.lane_ref, s32[2,384]{1,0:T(2,128)} %bitcast.78, f32[2,384]{1,0:T(2,128)} %bitcast.79, bf16[384,2048]{1,0:T(8,128)(2,1)} %refs_13_.1, ...), custom_call_target="tpu_custom_call" | custom-call | tf_op jit(solution)/shard_map/pallas_call | solution.py:216
  6.2 9.6 %all-to-all-start.1 = ((bf16[32,48,512]{2,1,0:T(8,128)(2,1)}), bf16[32,48,512]{2,1,0:T(8,128)(2,1)S(1)}, u32[]{:S(2)}, u32[]{:S(2)}) async-start(bf16[32,48,512]{2,1,0:T(8,128)(2,1)} %bitcast.66), calls=%async_computation.1 | async-start | bytes 3145728 | tf_op jit(solution)/shard_map/all_to_all | solution.py:26
  15.8 10.3 %shard_map.189 = (bf16[1536,2048]{1,0:T(8,128)(2,1)}, bf16[384,1536]{1,0:T(8,128)(2,1)}) custom-call(bf16[1536,384]{1,0:T(8,128)(2,1)} %get-tuple-element.27.chooser_ref, bf16[384,2048]{1,0:T(8,128)(2,1)} %refs_12_.1, bf16[384,32]{1,0:T(8,128)(2,1)} %get-tuple-element.28.rank_ref, bf16[32,384]{1,0:T(8,128)(2,1)} %get-tuple-element.29.high_ref, ...), custom_call_target="tpu_custom_call" | custom-call | tf_op jit(solution)/shard_map/pallas_call | solution.py:274
  26.0 11.9 %all-to-all-done.1 = bf16[32,48,512]{2,1,0:T(8,128)(2,1)S(1)} async-done(((bf16[32,48,512]{2,1,0:T(8,128)(2,1)}), bf16[32,48,512]{2,1,0:T(8,128)(2,1)S(1)}, u32[]{:S(2)}, u32[]{:S(2)}) %all-to-all-start.1) | async-done | bytes 1572896 | tf_op jit(solution)/shard_map/all_to_all | solution.py:26
  38.0 6.4 %all-to-all-start = ((bf16[32,48,2048]{2,1,0:T(8,128)(2,1)}), bf16[32,48,2048]{2,1,0:T(8,128)(2,1)}, u32[]{:S(2)}, u32[]{:S(2)}) async-start(bf16[32,48,2048]{2,1,0:T(8,128)(2,1)} %bitcast.57), calls=%async_computation | async-start | bytes 12582912 | tf_op jit(solution)/shard_map/all_to_all | solution.py:26
  47.2 34.2 %collective-permute-done.prev_ref = bf16[1536,512]{1,0:T(8,128)(2,1)S(1)} collective-permute-done((bf16[1536,512]{1,0:T(8,128)(2,1)S(1)}, bf16[1536,512]{1,0:T(8,128)(2,1)S(1)}, u32[]{:S(2)}, u32[]{:S(2)}) %collective-permute-start) | collective-permute-done | bytes 1572896 | tf_op jit(solution)/shard_map/ppermute | solution.py:22
  86.7 5.0 %collective-permute-start.22 = (f32[2,256]{1,0:T(2,128)}, f32[2,256]{1,0:T(2,128)}, u32[]{:S(2)}, u32[]{:S(2)}) collective-permute-start(f32[2,256]{1,0:T(2,128)} %slice.69), channel_id=1, source_target_pairs={{0,4},{4,8},{8,12},{12,16},{16,20},{20,24},{24,28},{28,32},{32,36}... | collective-permute-start | bytes 6152 | tf_op jit(solution)/shard_map/ppermute | solution.py:17
  95.2 6.7 %collective-permute-done.2.top_ref = bf16[768,512]{1,0:T(8,128)(2,1)} collective-permute-done((bf16[768,512]{1,0:T(8,128)(2,1)}, bf16[768,512]{1,0:T(8,128)(2,1)}, u32[]{:S(2)}, u32[]{:S(2)}) %collective-permute-start.2) | collective-permute-done | bytes 786464 | tf_op jit(solution)/shard_map/ppermute | solution.py:22
  101.9 7.8 %shard_map.190 = bf16[1536,2048]{1,0:T(8,128)(2,1)} custom-call(s32[1]{0:T(128)} %bitcast.lane_ref, bf16[1536,512]{1,0:T(8,128)(2,1)} %bitcast.60, bf16[1536,512]{1,0:T(8,128)(2,1)} %copy-done.7, bf16[1536,512]{1,0:T(8,128)(2,1)} %copy-done.8, bf16[768,512]{1,0:T(8,128)(2,1)} %collective-permute-done.2.top_ref, bf16[768,512]{1,0:T(8,128)(2,1)} %collective-permute-done.3.low_ref), custom_call_target="tpu_custom_call" | custom-call | tf_op jit(solution)/shard_map/pallas_call | solution.py:67
  109.7 4.8 %fusion.52 = f32[1536,256]{0,1:T(8,128)S(1)} fusion(bf16[1536,2048]{1,0:T(8,128)(2,1)} %shard_map.190, bf16[1,2048,256]{2,1,0:T(8,128)(2,1)S(1)} %copy-done.5), kind=kOutput, calls=%fused_computation.92 | convolution fusion | flops 1610612736 | bytes 8912896 | tf_op jit(solution)/shard_map/dot_general | solution.py:332
  114.5 4.3 %multiply_convert_fusion.2 = (bf16[1536,256]{0,1:T(8,128)(2,1)}, f32[1536,256]{0,1:T(8,128)}, f32[1536,256]{0,1:T(8,128)}) fusion(f32[1536,256]{0,1:T(8,128)S(1)} %fusion.52, bf16[1536,2048]{1,0:T(8,128)(2,1)S(1)} %copy-done.3, bf16[1,2048,256]{2,1,0:T(8,128)(2,1)S(1)} %copy-done.6), kind=kOutput, calls=%fused_computation.21 | convolution fusion | flops 1614938112 | bytes 12845056 | tf_op jit(solution)/shard_map/dot_general | solution.py:333
  118.8 5.6 %multiply_convert_fusion.1 = (bf16[1536,256]{0,1:T(8,128)(2,1)S(1)}, bf16[1536,256]{0,1:T(8,128)(2,1)S(1)}) fusion(f32[1536,256]{0,1:T(8,128)} %get-tuple-element.34, f32[1536,256]{0,1:T(8,128)} %get-tuple-element.35, bf16[1536,2048]{1,0:T(8,128)(2,1)} %bitcast.5, bf16[1,256,2048]{2,1,0:T(8,128)(2,1)S(1)} %copy-done), kind=kOutput, calls=%fused_computation.20 | convolution fusion | flops 1612185600 | bytes 12058624 | tf_op jit(solution)/shard_map/rd,fd->rf/dot_general | solution.py:339
  126.6 9.4 %all-to-all-start.3 = ((bf16[32,48,512]{2,1,0:T(8,128)(2,1)}), bf16[32,48,512]{2,1,0:T(8,128)(2,1)}, u32[]{:S(2)}, u32[]{:S(2)}) async-start(bf16[32,48,512]{2,1,0:T(8,128)(2,1)} %bitcast.65), calls=%async_computation.3 | async-start | bytes 3145728 | tf_op jit(solution)/shard_map/all_to_all | solution.py:26
  137.6 3.5 %collective-permute-start.8 = (bf16[768,256]{1,0:T(8,128)(2,1)S(1)}, bf16[768,256]{1,0:T(8,128)(2,1)S(1)}, u32[]{:S(2)}, u32[]{:S(2)}) collective-permute-start(bf16[768,256]{1,0:T(8,128)(2,1)S(1)} %convolution_convert_fusion.7), channel_id=1, source_target_pairs={{0,3},{1,0},{2,1},{3,2},{4,7},{5,4},{6,5},{7,6},{8,11},{9,8},{10,9... | collective-permute-start | bytes 1179656 | tf_op jit(solution)/shard_map/ppermute | solution.py:22
  146.1 3.1 %collective-permute-done.8 = bf16[768,256]{1,0:T(8,128)(2,1)S(1)} collective-permute-done((bf16[768,256]{1,0:T(8,128)(2,1)S(1)}, bf16[768,256]{1,0:T(8,128)(2,1)S(1)}, u32[]{:S(2)}, u32[]{:S(2)}) %collective-permute-start.8) | collective-permute-done | bytes 393248 | tf_op jit(solution)/shard_map/ppermute | solution.py:22
  149.7 3.6 %collective-permute-start.9 = (bf16[768,256]{1,0:T(8,128)(2,1)S(1)}, bf16[768,256]{1,0:T(8,128)(2,1)S(1)}, u32[]{:S(2)}, u32[]{:S(2)}) collective-permute-start(bf16[768,256]{1,0:T(8,128)(2,1)S(1)} %add_convert_fusion.3), channel_id=1, source_target_pairs={{0,3},{1,0},{2,1},{3,2},{4,7},{5,4},{6,5},{7,6},{8,11},{9,8},{10,9... | collective-permute-start | bytes 1179656 | tf_op jit(solution)/shard_map/ppermute | solution.py:22
  162.2 3.9 %collective-permute-done.9 = bf16[768,256]{1,0:T(8,128)(2,1)S(1)} collective-permute-done((bf16[768,256]{1,0:T(8,128)(2,1)S(1)}, bf16[768,256]{1,0:T(8,128)(2,1)S(1)}, u32[]{:S(2)}, u32[]{:S(2)}) %collective-permute-start.9) | collective-permute-done | bytes 393248 | tf_op jit(solution)/shard_map/ppermute | solution.py:22
  166.1 4.5 %collective-permute-done.5 = bf16[768,256]{1,0:T(8,128)(2,1)S(1)} collective-permute-done((bf16[768,256]{1,0:T(8,128)(2,1)S(1)}, bf16[768,256]{1,0:T(8,128)(2,1)S(1)}, u32[]{:S(2)}, u32[]{:S(2)}) %collective-permute-start.5) | collective-permute-done | bytes 393248 | tf_op jit(solution)/shard_map/ppermute | solution.py:22
  172.1 9.6 %all-to-all-start.2 = ((bf16[32,48,256]{2,1,0:T(8,128)(2,1)}), bf16[32,48,256]{2,1,0:T(8,128)(2,1)S(1)}, u32[]{:S(2)}, u32[]{:S(2)}) async-start(bf16[32,48,256]{2,1,0:T(8,128)(2,1)} %bitcast.14), calls=%async_computation.2 | async-start | bytes 1572864 | tf_op jit(solution)/shard_map/all_to_all | solution.py:26
  183.7 3.3 %convolution_convert_fusion.11.refs_8_ = bf16[384,512]{1,0:T(8,128)(2,1)} fusion(bf16[384,1536]{1,0:T(8,128)(2,1)} %get-tuple-element.31, bf16[1536,512]{1,0:T(8,128)(2,1)} %bitcast.17), kind=kOutput, calls=%fused_computation.29 | convolution fusion | flops 604176384 | bytes 3145728 | tf_op jit(solution)/shard_map/dot_general | solution.py:348
  187.0 8.9 %all-to-all-done.2 = bf16[32,48,256]{2,1,0:T(8,128)(2,1)S(1)} async-done(((bf16[32,48,256]{2,1,0:T(8,128)(2,1)}), bf16[32,48,256]{2,1,0:T(8,128)(2,1)S(1)}, u32[]{:S(2)}, u32[]{:S(2)}) %all-to-all-start.2) | async-done | bytes 786464 | tf_op jit(solution)/shard_map/all_to_all | solution.py:26
  200.5 6.1 %all-to-all-start.4 = ((bf16[32,48,128]{2,1,0:T(8,128)(2,1)}), bf16[32,48,128]{2,1,0:T(8,128)(2,1)S(1)}, u32[]{:S(2)}, u32[]{:S(2)}) async-start(bf16[32,48,128]{2,1,0:T(8,128)(2,1)} %bitcast.18), calls=%async_computation.4 | async-start | bytes 786432 | tf_op jit(solution)/shard_map/all_to_all | solution.py:26
  206.6 5.9 %convolution_bitcast_fusion = f32[1,256,2048]{2,1,0:T(8,128)} fusion(bf16[1536,256]{0,1:T(8,128)(2,1)S(1)} %copy-done.26, bf16[1536,2048]{1,0:T(8,128)(2,1)} %bitcast.5), kind=kOutput, calls=%fused_computation.1 | convolution fusion | flops 1610612736 | bytes 9175040 | tf_op jit(solution)/shard_map/rf,rd->fd/dot_general | solution.py:374
  218.8 16.9 %collective-permute-done.11.refs_2_ = bf16[384,256]{1,0:T(8,128)(2,1)} collective-permute-done((bf16[384,256]{1,0:T(8,128)(2,1)}, bf16[384,256]{1,0:T(8,128)(2,1)}, u32[]{:S(2)}, u32[]{:S(2)}) %collective-permute-start.11) | collective-permute-done | bytes 196640 | tf_op jit(solution)/shard_map/ppermute | solution.py:22
  235.7 6.6 %collective-permute-start.17 = (bf16[384,128]{1,0:T(8,128)(2,1)S(1)}, bf16[384,128]{1,0:T(8,128)(2,1)S(1)}, u32[]{:S(2)}, u32[]{:S(2)}) collective-permute-start(bf16[384,128]{1,0:T(8,128)(2,1)S(1)} %convolution_convert_fusion.13.refs_4_), channel_id=1, source_target_pairs={{0,3},{1,0},{2,1},{3,2},{4,7},{5,4},{6,5},{7,6},{8,11},{9,8},{10,9... | collective-permute-start | bytes 294920 | tf_op jit(solution)/shard_map/ppermute | solution.py:22
  248.0 5.0 %shard_map.191 = bf16[384,2048]{1,0:T(8,128)(2,1)} custom-call(s32[1]{0:T(128)} %bitcast.lane_ref, bf16[384,256]{1,0:T(8,128)(2,1)} %convolution_convert_fusion.12.refs_0_, bf16[384,256]{1,0:T(8,128)(2,1)} %copy-done.21, bf16[384,256]{1,0:T(8,128)(2,1)} %collective-permute-done.11.refs_2_, bf16[384,256]{1,0:T(8,128)(2,1)} %collective-permute-done.12.refs_3_, ...), custom_call_target="tpu_custom_call" | custom-call | tf_op jit(solution)/shard_map/pallas_call | solution.py:132
  253.0 3.3 %convolution_convert_fusion.1 = bf16[2048,256]{1,0:T(8,128)(2,1)} fusion(bf16[384,2048]{1,0:T(8,128)(2,1)} %shard_map.191, f32[384,256]{1,0:T(8,128)S(1)} %fusion.13, bf16[384,256]{1,0:T(8,128)(2,1)S(1)} %copy-done.20), kind=kOutput, calls=%fused_computation.2 | convolution fusion | flops 403472384 | bytes 3211264 | tf_op jit(solution)/shard_map/td,tc->dc/dot_general | solution.py:397
  256.3 8.2 %fusion.62 = f32[2048,512]{1,0:T(8,128)} fusion(bf16[1536,2048]{1,0:T(8,128)(2,1)} %shard_map.190, bf16[1536,512]{0,1:T(8,128)(2,1)S(1)} %copy-done.10), kind=kOutput, calls=%fused_computation.95 | convolution fusion | flops 3221225472 | bytes 12058624 | tf_op jit(solution)/shard_map/rd,rf->df/dot_general | solution.py:401
  265.8 4.6 %collective-permute-start.23 = (f32[2,256]{1,0:T(2,128)S(1)}, f32[2,256]{1,0:T(2,128)S(1)}, u32[]{:S(2)}, u32[]{:S(2)}) collective-permute-start(f32[2,256]{1,0:T(2,128)S(1)} %slice.72), channel_id=1, source_target_pairs={{4,0},{8,4},{12,8},{16,12},{20,16},{24,20},{28,24},{32,28},{36,32}... | collective-permute-start | bytes 6152 | tf_op jit(solution)/shard_map/ppermute | solution.py:17
  270.4 7.1 %all-to-all-start.5 = ((bf16[32,64,256]{2,1,0:T(8,128)(2,1)}), bf16[32,64,256]{2,1,0:T(8,128)(2,1)S(1)}, u32[]{:S(2)}, u32[]{:S(2)}) async-start(bf16[32,64,256]{2,1,0:T(8,128)(2,1)} %bitcast.26), calls=%async_computation.5 | async-start | bytes 2097152 | tf_op jit(solution)/shard_map/all_to_all | solution.py:26
  277.6 4.6 %slice_bitcast_fusion = (f32[1,2048,256]{2,1,0:T(8,128)}, f32[1,2048,256]{2,1,0:T(8,128)}) fusion(f32[2048,512]{1,0:T(8,128)} %fusion.62), kind=kLoop, calls=%fused_computation.11 | loop fusion | bytes 8388608 | tf_op jit(solution)/shard_map/broadcast_in_dim | solution.py:418
  283.8 10.8 %all-to-all-done.5 = bf16[32,64,256]{2,1,0:T(8,128)(2,1)S(1)} async-done(((bf16[32,64,256]{2,1,0:T(8,128)(2,1)}), bf16[32,64,256]{2,1,0:T(8,128)(2,1)S(1)}, u32[]{:S(2)}, u32[]{:S(2)}) %all-to-all-start.5) | async-done | bytes 1048608 | tf_op jit(solution)/shard_map/all_to_all | solution.py:26
  (124 shorter events, 53.0 us)
Async XLA Ops:
  0.6 118.2 %copy-start = (bf16[1,256,2048]{2,1,0:T(8,128)(2,1)S(1)}, bf16[1,256,2048]{2,1,0:T(8,128)(2,1)}, u32[]{:S(2)}) copy-start(bf16[1,256,2048]{2,1,0:T(8,128)(2,1)} %param.20) | copy-start | bytes 3145732
  6.2 31.8 %all-to-all-start.1 = ((bf16[32,48,512]{2,1,0:T(8,128)(2,1)}), bf16[32,48,512]{2,1,0:T(8,128)(2,1)S(1)}, u32[]{:S(2)}, u32[]{:S(2)}) async-start(bf16[32,48,512]{2,1,0:T(8,128)(2,1)} %bitcast.66), calls=%async_computation.1 | async-start | bytes 3145728 | tf_op jit(solution)/shard_map/all_to_all | solution.py:26
  38.0 80.9 %all-to-all-start = ((bf16[32,48,2048]{2,1,0:T(8,128)(2,1)}), bf16[32,48,2048]{2,1,0:T(8,128)(2,1)}, u32[]{:S(2)}, u32[]{:S(2)}) async-start(bf16[32,48,2048]{2,1,0:T(8,128)(2,1)} %bitcast.57), calls=%async_computation | async-start | bytes 12582912 | tf_op jit(solution)/shard_map/all_to_all | solution.py:26
  44.4 41.7 %copy-start.12 = (bf16[384,256]{1,0:T(8,128)(2,1)S(1)}, bf16[384,256]{1,0:T(8,128)(2,1)}, u32[]{:S(2)}) copy-start(bf16[384,256]{1,0:T(8,128)(2,1)} %param.24) | copy-start | bytes 589828
  44.4 36.9 %collective-permute-start = (bf16[1536,512]{1,0:T(8,128)(2,1)S(1)}, bf16[1536,512]{1,0:T(8,128)(2,1)S(1)}, u32[]{:S(2)}, u32[]{:S(2)}) collective-permute-start(bf16[1536,512]{1,0:T(8,128)(2,1)S(1)} %bitcast.58), channel_id=1, source_target_pairs={{0,1},{1,2},{2,3},{3,0},{4,5},{5,6},{6,7},{7,4},{8,9},{9,10},{10,1... | collective-permute-start | bytes 4718600 | tf_op jit(solution)/shard_map/ppermute | solution.py:22
  45.7 36.7 %collective-permute-start.1 = (bf16[1536,512]{1,0:T(8,128)(2,1)S(1)}, bf16[1536,512]{1,0:T(8,128)(2,1)S(1)}, u32[]{:S(2)}, u32[]{:S(2)}) collective-permute-start(bf16[1536,512]{1,0:T(8,128)(2,1)S(1)} %bitcast.59), channel_id=1, source_target_pairs={{0,3},{1,0},{2,1},{3,2},{4,7},{5,4},{6,5},{7,6},{8,11},{9,8},{10,9... | collective-permute-start | bytes 4718600 | tf_op jit(solution)/shard_map/ppermute | solution.py:22
  82.4 19.5 %collective-permute-start.2 = (bf16[768,512]{1,0:T(8,128)(2,1)}, bf16[768,512]{1,0:T(8,128)(2,1)}, u32[]{:S(2)}, u32[]{:S(2)}) collective-permute-start(bf16[768,512]{1,0:T(8,128)(2,1)} %slice.63), channel_id=1, source_target_pairs={{0,1},{1,2},{2,3},{3,0},{4,5},{5,6},{6,7},{7,4},{8,9},{9,10},{10,1... | collective-permute-start | bytes 2359304 | tf_op jit(solution)/shard_map/ppermute | solution.py:22
  83.4 18.4 %collective-permute-start.3 = (bf16[768,512]{1,0:T(8,128)(2,1)}, bf16[768,512]{1,0:T(8,128)(2,1)}, u32[]{:S(2)}, u32[]{:S(2)}) collective-permute-start(bf16[768,512]{1,0:T(8,128)(2,1)} %slice.64), channel_id=1, source_target_pairs={{0,3},{1,0},{2,1},{3,2},{4,7},{5,4},{6,5},{7,6},{8,11},{9,8},{10,9... | collective-permute-start | bytes 2359304 | tf_op jit(solution)/shard_map/ppermute | solution.py:22
  86.7 54.3 %collective-permute-start.22 = (f32[2,256]{1,0:T(2,128)}, f32[2,256]{1,0:T(2,128)}, u32[]{:S(2)}, u32[]{:S(2)}) collective-permute-start(f32[2,256]{1,0:T(2,128)} %slice.69), channel_id=1, source_target_pairs={{0,4},{4,8},{8,12},{12,16},{16,20},{20,24},{24,28},{28,32},{32,36}... | collective-permute-start | bytes 6152 | tf_op jit(solution)/shard_map/ppermute | solution.py:17
  126.6 45.5 %all-to-all-start.3 = ((bf16[32,48,512]{2,1,0:T(8,128)(2,1)}), bf16[32,48,512]{2,1,0:T(8,128)(2,1)}, u32[]{:S(2)}, u32[]{:S(2)}) async-start(bf16[32,48,512]{2,1,0:T(8,128)(2,1)} %bitcast.65), calls=%async_computation.3 | async-start | bytes 3145728 | tf_op jit(solution)/shard_map/all_to_all | solution.py:26
  137.6 11.7 %collective-permute-start.8 = (bf16[768,256]{1,0:T(8,128)(2,1)S(1)}, bf16[768,256]{1,0:T(8,128)(2,1)S(1)}, u32[]{:S(2)}, u32[]{:S(2)}) collective-permute-start(bf16[768,256]{1,0:T(8,128)(2,1)S(1)} %convolution_convert_fusion.7), channel_id=1, source_target_pairs={{0,3},{1,0},{2,1},{3,2},{4,7},{5,4},{6,5},{7,6},{8,11},{9,8},{10,9... | collective-permute-start | bytes 1179656 | tf_op jit(solution)/shard_map/ppermute | solution.py:22
  142.4 11.5 %collective-permute-start.4 = (bf16[768,256]{1,0:T(8,128)(2,1)S(1)}, bf16[768,256]{1,0:T(8,128)(2,1)S(1)}, u32[]{:S(2)}, u32[]{:S(2)}) collective-permute-start(bf16[768,256]{1,0:T(8,128)(2,1)S(1)} %convolution_convert_fusion.10), channel_id=1, source_target_pairs={{0,1},{1,2},{2,3},{3,0},{4,5},{5,6},{6,7},{7,4},{8,9},{9,10},{10,1... | collective-permute-start | bytes 1179656 | tf_op jit(solution)/shard_map/ppermute | solution.py:22
  142.9 16.3 %collective-permute-start.7 = (bf16[768,256]{1,0:T(8,128)(2,1)S(1)}, bf16[768,256]{1,0:T(8,128)(2,1)S(1)}, u32[]{:S(2)}, u32[]{:S(2)}) collective-permute-start(bf16[768,256]{1,0:T(8,128)(2,1)S(1)} %convolution_convert_fusion.8), channel_id=1, source_target_pairs={{0,3},{1,0},{2,1},{3,2},{4,7},{5,4},{6,5},{7,6},{8,11},{9,8},{10,9... | collective-permute-start | bytes 1179656 | tf_op jit(solution)/shard_map/ppermute | solution.py:22
  146.0 16.1 %collective-permute-start.6 = (bf16[768,256]{1,0:T(8,128)(2,1)S(1)}, bf16[768,256]{1,0:T(8,128)(2,1)S(1)}, u32[]{:S(2)}, u32[]{:S(2)}) collective-permute-start(bf16[768,256]{1,0:T(8,128)(2,1)S(1)} %convolution_convert_fusion.9), channel_id=1, source_target_pairs={{0,1},{1,2},{2,3},{3,0},{4,5},{5,6},{6,7},{7,4},{8,9},{9,10},{10,1... | collective-permute-start | bytes 1179656 | tf_op jit(solution)/shard_map/ppermute | solution.py:22
  149.7 16.4 %collective-permute-start.9 = (bf16[768,256]{1,0:T(8,128)(2,1)S(1)}, bf16[768,256]{1,0:T(8,128)(2,1)S(1)}, u32[]{:S(2)}, u32[]{:S(2)}) collective-permute-start(bf16[768,256]{1,0:T(8,128)(2,1)S(1)} %add_convert_fusion.3), channel_id=1, source_target_pairs={{0,3},{1,0},{2,1},{3,2},{4,7},{5,4},{6,5},{7,6},{8,11},{9,8},{10,9... | collective-permute-start | bytes 1179656 | tf_op jit(solution)/shard_map/ppermute | solution.py:22
  154.3 16.3 %collective-permute-start.5 = (bf16[768,256]{1,0:T(8,128)(2,1)S(1)}, bf16[768,256]{1,0:T(8,128)(2,1)S(1)}, u32[]{:S(2)}, u32[]{:S(2)}) collective-permute-start(bf16[768,256]{1,0:T(8,128)(2,1)S(1)} %add_convert_fusion.4), channel_id=1, source_target_pairs={{0,1},{1,2},{2,3},{3,0},{4,5},{5,6},{6,7},{7,4},{8,9},{9,10},{10,1... | collective-permute-start | bytes 1179656 | tf_op jit(solution)/shard_map/ppermute | solution.py:22
  155.8 25.9 %collective-permute-start.13 = (bf16[1536,128]{1,0:T(8,128)(2,1)}, bf16[1536,128]{1,0:T(8,128)(2,1)}, u32[]{:S(2)}, u32[]{:S(2)}) collective-permute-start(bf16[1536,128]{1,0:T(8,128)(2,1)} %convolution_convert_fusion.4), channel_id=1, source_target_pairs={{0,1},{1,2},{2,3},{3,0},{4,5},{5,6},{6,7},{7,4},{8,9},{9,10},{10,1... | collective-permute-start | bytes 1179656 | tf_op jit(solution)/shard_map/ppermute | solution.py:22
  159.2 39.2 %collective-permute-start.15 = (bf16[1536,128]{1,0:T(8,128)(2,1)}, bf16[1536,128]{1,0:T(8,128)(2,1)}, u32[]{:S(2)}, u32[]{:S(2)}) collective-permute-start(bf16[1536,128]{1,0:T(8,128)(2,1)} %convolution_convert_fusion.3), channel_id=1, source_target_pairs={{0,3},{1,0},{2,1},{3,2},{4,7},{5,4},{6,5},{7,6},{8,11},{9,8},{10,9... | collective-permute-start | bytes 1179656 | tf_op jit(solution)/shard_map/ppermute | solution.py:22
  172.1 23.8 %all-to-all-start.2 = ((bf16[32,48,256]{2,1,0:T(8,128)(2,1)}), bf16[32,48,256]{2,1,0:T(8,128)(2,1)S(1)}, u32[]{:S(2)}, u32[]{:S(2)}) async-start(bf16[32,48,256]{2,1,0:T(8,128)(2,1)} %bitcast.14), calls=%async_computation.2 | async-start | bytes 1572864 | tf_op jit(solution)/shard_map/all_to_all | solution.py:26
  183.7 14.7 %collective-permute-start.14 = (bf16[1536,128]{1,0:T(8,128)(2,1)}, bf16[1536,128]{1,0:T(8,128)(2,1)}, u32[]{:S(2)}, u32[]{:S(2)}) collective-permute-start(bf16[1536,128]{1,0:T(8,128)(2,1)} %add_convert_fusion.2), channel_id=1, source_target_pairs={{0,1},{1,2},{2,3},{3,0},{4,5},{5,6},{6,7},{7,4},{8,9},{9,10},{10,1... | collective-permute-start | bytes 1179656 | tf_op jit(solution)/shard_map/ppermute | solution.py:22
  187.0 55.4 %collective-permute-start.19 = (bf16[384,512]{1,0:T(8,128)(2,1)}, bf16[384,512]{1,0:T(8,128)(2,1)}, u32[]{:S(2)}, u32[]{:S(2)}) collective-permute-start(bf16[384,512]{1,0:T(8,128)(2,1)} %convolution_convert_fusion.11.refs_8_), channel_id=1, source_target_pairs={{0,1},{1,2},{2,3},{3,0},{4,5},{5,6},{6,7},{7,4},{8,9},{9,10},{10,1... | collective-permute-start | bytes 1179656 | tf_op jit(solution)/shard_map/ppermute | solution.py:22
  198.4 18.0 %collective-permute-start.10 = (bf16[384,256]{1,0:T(8,128)(2,1)}, bf16[384,256]{1,0:T(8,128)(2,1)S(1)}, u32[]{:S(2)}, u32[]{:S(2)}) collective-permute-start(bf16[384,256]{1,0:T(8,128)(2,1)} %convolution_convert_fusion.12.refs_0_), channel_id=1, source_target_pairs={{0,1},{1,2},{2,3},{3,0},{4,5},{5,6},{6,7},{7,4},{8,9},{9,10},{10,1... | collective-permute-start | bytes 589832 | tf_op jit(solution)/shard_map/ppermute | solution.py:22
  200.5 16.3 %all-to-all-start.4 = ((bf16[32,48,128]{2,1,0:T(8,128)(2,1)}), bf16[32,48,128]{2,1,0:T(8,128)(2,1)S(1)}, u32[]{:S(2)}, u32[]{:S(2)}) async-start(bf16[32,48,128]{2,1,0:T(8,128)(2,1)} %bitcast.18), calls=%async_computation.4 | async-start | bytes 786432 | tf_op jit(solution)/shard_map/all_to_all | solution.py:26
  212.5 31.1 %collective-permute-start.20 = (bf16[384,512]{1,0:T(8,128)(2,1)}, bf16[384,512]{1,0:T(8,128)(2,1)S(1)}, u32[]{:S(2)}, u32[]{:S(2)}) collective-permute-start(bf16[384,512]{1,0:T(8,128)(2,1)} %convolution_convert_fusion.11.refs_8_), channel_id=1, source_target_pairs={{0,3},{1,0},{2,1},{3,2},{4,7},{5,4},{6,5},{7,6},{8,11},{9,8},{10,9... | collective-permute-start | bytes 1179656 | tf_op jit(solution)/shard_map/ppermute | solution.py:22
  213.3 30.3 %collective-permute-start.21 = (bf16[384,512]{1,0:T(8,128)(2,1)}, bf16[384,512]{1,0:T(8,128)(2,1)S(1)}, u32[]{:S(2)}, u32[]{:S(2)}) collective-permute-start(bf16[384,512]{1,0:T(8,128)(2,1)} %convolution_convert_fusion.11.refs_8_), channel_id=1, source_target_pairs={{0,2},{1,3},{2,0},{3,1},{4,6},{5,7},{6,4},{7,5},{8,10},{9,11},{10,... | collective-permute-start | bytes 1179656 | tf_op jit(solution)/shard_map/ppermute | solution.py:22
  213.3 22.4 %collective-permute-start.11 = (bf16[384,256]{1,0:T(8,128)(2,1)}, bf16[384,256]{1,0:T(8,128)(2,1)}, u32[]{:S(2)}, u32[]{:S(2)}) collective-permute-start(bf16[384,256]{1,0:T(8,128)(2,1)} %convolution_convert_fusion.12.refs_0_), channel_id=1, source_target_pairs={{0,3},{1,0},{2,1},{3,2},{4,7},{5,4},{6,5},{7,6},{8,11},{9,8},{10,9... | collective-permute-start | bytes 589832 | tf_op jit(solution)/shard_map/ppermute | solution.py:22
  216.4 19.4 %collective-permute-start.12 = (bf16[384,256]{1,0:T(8,128)(2,1)}, bf16[384,256]{1,0:T(8,128)(2,1)}, u32[]{:S(2)}, u32[]{:S(2)}) collective-permute-start(bf16[384,256]{1,0:T(8,128)(2,1)} %convolution_convert_fusion.12.refs_0_), channel_id=1, source_target_pairs={{0,2},{1,3},{2,0},{3,1},{4,6},{5,7},{6,4},{7,5},{8,10},{9,11},{10,... | collective-permute-start | bytes 589832 | tf_op jit(solution)/shard_map/ppermute | solution.py:22
  235.7 7.9 %collective-permute-start.16 = (bf16[384,128]{1,0:T(8,128)(2,1)S(1)}, bf16[384,128]{1,0:T(8,128)(2,1)S(1)}, u32[]{:S(2)}, u32[]{:S(2)}) collective-permute-start(bf16[384,128]{1,0:T(8,128)(2,1)S(1)} %convolution_convert_fusion.13.refs_4_), channel_id=1, source_target_pairs={{0,1},{1,2},{2,3},{3,0},{4,5},{5,6},{6,7},{7,4},{8,9},{9,10},{10,1... | collective-permute-start | bytes 294920 | tf_op jit(solution)/shard_map/ppermute | solution.py:22
  235.7 10.5 %collective-permute-start.17 = (bf16[384,128]{1,0:T(8,128)(2,1)S(1)}, bf16[384,128]{1,0:T(8,128)(2,1)S(1)}, u32[]{:S(2)}, u32[]{:S(2)}) collective-permute-start(bf16[384,128]{1,0:T(8,128)(2,1)S(1)} %convolution_convert_fusion.13.refs_4_), channel_id=1, source_target_pairs={{0,3},{1,0},{2,1},{3,2},{4,7},{5,4},{6,5},{7,6},{8,11},{9,8},{10,9... | collective-permute-start | bytes 294920 | tf_op jit(solution)/shard_map/ppermute | solution.py:22
  242.3 5.0 %collective-permute-start.18 = (bf16[384,128]{1,0:T(8,128)(2,1)S(1)}, bf16[384,128]{1,0:T(8,128)(2,1)S(1)}, u32[]{:S(2)}, u32[]{:S(2)}) collective-permute-start(bf16[384,128]{1,0:T(8,128)(2,1)S(1)} %convolution_convert_fusion.13.refs_4_), channel_id=1, source_target_pairs={{0,2},{1,3},{2,0},{3,1},{4,6},{5,7},{6,4},{7,5},{8,10},{9,11},{10,... | collective-permute-start | bytes 294920 | tf_op jit(solution)/shard_map/ppermute | solution.py:22
  265.8 16.4 %collective-permute-start.23 = (f32[2,256]{1,0:T(2,128)S(1)}, f32[2,256]{1,0:T(2,128)S(1)}, u32[]{:S(2)}, u32[]{:S(2)}) collective-permute-start(f32[2,256]{1,0:T(2,128)S(1)} %slice.72), channel_id=1, source_target_pairs={{4,0},{8,4},{12,8},{16,12},{20,16},{24,20},{28,24},{32,28},{36,32}... | collective-permute-start | bytes 6152 | tf_op jit(solution)/shard_map/ppermute | solution.py:17
  270.4 24.2 %all-to-all-start.5 = ((bf16[32,64,256]{2,1,0:T(8,128)(2,1)}), bf16[32,64,256]{2,1,0:T(8,128)(2,1)S(1)}, u32[]{:S(2)}, u32[]{:S(2)}) async-start(bf16[32,64,256]{2,1,0:T(8,128)(2,1)} %bitcast.26), calls=%async_computation.5 | async-start | bytes 2097152 | tf_op jit(solution)/shard_map/all_to_all | solution.py:26
  (25 other events, 191.6 us)

commit v3 on v1

--- a/solution.py
+++ b/solution.py
@@ -88,7 +88,7 @@
 
 def finish(lane, pieces, cotangent, resid_in, norm_gain):
     tokens, width = cotangent.shape
-    block = 128
+    block = 192
 
     def rows(array):
         return pl.BlockSpec((block, array.shape[1]), lambda i, _: (i, 0))
@@ -167,7 +167,7 @@
     sent_ref[...] = jnp.dot(chooser, normed_ref[...], preferred_element_type=f32).astype(bf16)
 
 
-slot_block = 256
+slot_block = 512
 
 
 def chosen_rows(lane, routes, route_weights, resid_in, norm_gain, experts):
@@ -249,59 +249,47 @@
     )(chooser, cotangent, rank, high, low)
 
 
-def expert_kernel(lane_ref, gate_ref, up_ref, cot_ref, down_ref, gmat_ref, umat_ref, *outs):
-    hidden_ref, dgate_ref, dup_ref, direct_ref = outs[:4]
-    further_refs = (outs[4:7], outs[7:10], outs[10:13], outs[13:16])
-    quarter = gmat_ref.shape[0] // 4
+def write_parts(both, mat_ref, refs):
+    part = lax.dot_general(both, mat_ref[...], along_last, preferred_element_type=f32)
+    part = part.astype(bf16)
+    at = 0
+    for ref in refs:
+        ref[...] = part[:, at : at + ref.shape[1]]
+        at += ref.shape[1]
+
+
+def first_kernel(cot_ref, act_ref, slope_ref, down_ref, mat_ref, both_ref, *refs):
     dhidden = lax.dot_general(
         cot_ref[...], down_ref[...], along_last, preferred_element_type=f32
     )
-    gate_pre = gate_ref[...]
-    up_pre = up_ref[...]
-    logistic = jax.nn.sigmoid(gate_pre)
-    activated = gate_pre * logistic
-    hidden_ref[...] = (activated * up_pre).astype(bf16)
-    dgate = (dhidden * up_pre * logistic * (1.0 + gate_pre * (1.0 - logistic))).astype(bf16)
-    dup = (dhidden * activated).astype(bf16)
-    dgate_ref[...] = dgate
-    dup_ref[...] = dup
-    for further in range(4):
-        place = (lane_ref[0] + further) % 4
-        at = pl.ds(pl.multiple_of(place * quarter, 128), quarter)
-        part = lax.dot_general(
-            dgate, gmat_ref[at, :], along_last, preferred_element_type=f32
-        ) + lax.dot_general(dup, umat_ref[at, :], along_last, preferred_element_type=f32)
-        part = part.astype(bf16)
-        direct_ref[:, pl.ds(pl.multiple_of(place * direct_width, 128), direct_width)] = part[
-            :, quarter - direct_width :
-        ]
-        for i, ref in enumerate(further_refs[further]):
-            ref[...] = part[:, i * direct_width : (i + 1) * direct_width]
-
-
-def expert_grads(lane, gate_pre, up_pre, entry_cots, down_mat, gate_mat, up_mat):
-    slots, width = entry_cots.shape
-    inner = gate_pre.shape[1]
-    block = 256
+    dgate = (dhidden * slope_ref[...].astype(f32)).astype(bf16)
+    dup = (dhidden * act_ref[...].astype(f32)).astype(bf16)
+    both = jnp.concatenate([dgate, dup], axis=1)
+    both_ref[...] = both
+    write_parts(both, mat_ref, refs)
+
+
+def other_kernel(both_ref, mat_ref, *refs):
+    write_parts(both_ref[...], mat_ref, refs)
+
+
+part_block = 512
+
+
+def by_rows(kernel, rowwise, matrices, sizes):
+    slots = rowwise[0].shape[0]
 
     def rows(size):
-        return pl.BlockSpec((block, size), lambda i, _: (i, 0))
-
-    def whole(array):
-        return pl.BlockSpec(array.shape, lambda i, _: (0, 0))
-
-    sizes = [inner] * 3 + [4 * direct_width] + [direct_width] * 12
+        return pl.BlockSpec((part_block, size), lambda i: (i, 0))
+
     return pl.pallas_call(
-        expert_kernel,
-        grid_spec=pltpu.PrefetchScalarGridSpec(
-            num_scalar_prefetch=1,
-            grid=(slots // block,),
-            in_specs=[rows(inner), rows(inner), rows(width)]
-            + [whole(x) for x in (down_mat, gate_mat, up_mat)],
-            out_specs=[rows(size) for size in sizes],
-        ),
+        kernel,
+        grid=(slots // part_block,),
+        in_specs=[rows(x.shape[1]) for x in rowwise]
+        + [pl.BlockSpec(x.shape, lambda i: (0, 0)) for x in matrices],
+        out_specs=[rows(size) for size in sizes],
         out_shape=[jax.ShapeDtypeStruct((slots, size), bf16) for size in sizes],
-    )(lane.reshape(1), gate_pre, up_pre, entry_cots, down_mat, gate_mat, up_mat)
+    )(*rowwise, *matrices)
 
 
 def on_device(
@@ -343,11 +331,39 @@
 
     gate_pre = jnp.dot(entry_rows, gate_mat, preferred_element_type=f32)
     up_pre = jnp.dot(entry_rows, up_mat, preferred_element_type=f32)
-    hidden, dgate, dup, direct, *others = expert_grads(
-        lane, gate_pre, up_pre, entry_cots, down_mat, gate_mat, up_mat
-    )
-    a_own, b_own, c_own, a_ahead, b_ahead, c_ahead = others[:6]
-    a_far, b_far, c_far, a_behind, b_behind, c_behind = others[6:]
+    logistic = jax.nn.sigmoid(gate_pre)
+    activated = gate_pre * logistic
+    hidden = (activated * up_pre).astype(bf16)
+    slope = up_pre * logistic * (1.0 + gate_pre * (1.0 - logistic))
+    both_mat = jnp.concatenate([gate_mat, up_mat], axis=1)
+
+    def weight_rows(further, first, count):
+        at = ((lane + further) % lanes) * quarter + first * direct_width
+        return lax.dynamic_slice_in_dim(both_mat, at, count * direct_width, axis=0)
+
+    direct_mat = both_mat.reshape(lanes, quarter, -1)[:, -direct_width:]
+    first_mat = jnp.concatenate(
+        [weight_rows(2, 0, 2), weight_rows(3, 0, 1), weight_rows(1, 1, 1)]
+        + [direct_mat.reshape(lanes * direct_width, -1)],
+        axis=0,
+    )
+    other_mat = jnp.concatenate(
+        [weight_rows(0, 0, 3), weight_rows(1, 0, 1), weight_rows(1, 2, 1)]
+        + [weight_rows(3, 1, 2), weight_rows(2, 2, 1)],
+        axis=0,
+    )
+    activated, slope, hidden, first_mat, other_mat = lax.optimization_barrier(
+        (activated.astype(bf16), slope.astype(bf16), hidden, first_mat, other_mat)
+    )
+    dboth, a_far, b_far, a_behind, b_ahead, direct = by_rows(
+        first_kernel,
+        (entry_cots, activated, slope),
+        (down_mat, first_mat),
+        [both_mat.shape[1]] + [direct_width] * 4 + [lanes * direct_width],
+    )
+    a_own, b_own, c_own, a_ahead, c_ahead, b_behind, c_behind, c_far = by_rows(
+        other_kernel, (dboth,), (other_mat,), [direct_width] * 8
+    )
 
     def back(array):
         return exchanged(array.reshape(groups, capacity, -1)).reshape(slots, -1)
@@ -390,10 +406,10 @@
     out_parts = jnp.einsum("td,tc->dc", grad_resid, merged, preferred_element_type=f32).astype(bf16)
     out_tiles = exchanged(out_parts.reshape(groups, model_width // groups, -1))
     grad_out_weight = jnp.sum(out_tiles.astype(f32), axis=0)
-    dgate, out_parts = lax.optimization_barrier((dgate, out_parts))
-    grad_gate = jnp.einsum("rd,rf->df", entry_rows, dgate, preferred_element_type=f32)
-    late_resid, grad_gate, dup = lax.optimization_barrier((grad_resid, grad_gate, dup))
-    grad_up = jnp.einsum("rd,rf->df", entry_rows, dup, preferred_element_type=f32)
+    late_both, out_parts = lax.optimization_barrier((dboth, out_parts))
+    grad_both = jnp.einsum("rd,rf->df", entry_rows, late_both, preferred_element_type=f32)
+    late_resid, grad_both = lax.optimization_barrier((grad_resid, grad_both))
+    grad_gate, grad_up = jnp.split(grad_both, 2, axis=1)
     dmerged = jnp.dot(late_resid, out_weight, preferred_element_type=f32)
     grad_gate_b = (dmerged * conv).astype(bf16)
     dconv = dmerged * gate_b.astype(f32)

time: 303 us -> 305 us (level)
  matrix products: 35.5 us -> 30.6 us
  local copies, waits for them, and re-layouts: 8.37 us -> 12.9 us
    dot_general x2 -> x1, matrix products: 12 us -> 8.03 us  [on_device(): jnp.einsum('rd,rf->df', entry_rows, late_both, preferred_element_type=f32)]
    ppermute x2, waiting for transfers between devices: 4.34 us -> 8.01 us  [passed_along(): return lax.ppermute(array, axis, pairs)]
    pallas_call x1 -> x2, Pallas kernels: 13.6 us -> 15.3 us  [by_rows(): pl.pallas_call(kernel, grid=(slots // part_block,), in_specs=[rows(x.shap...]
  transfers between devices with their start and end apart: 30 -> 30, of which waited for: 14 -> 13; matrix products, arithmetic and copies ran while one was open for 15% -> 13% of each run, Pallas kernels for 3% -> 4%
where the time goes in v3:
time: 305 us; the launch traced here: 303 us
  waiting for transfers between devices  126 us (41%)
  starting transfers between devices  85 us (28%)
  Pallas kernels  33.6 us (11%)
  matrix products  30.6 us (10%)
  other arithmetic  13.7 us (4%)
  local copies, waits for them, and re-layouts  12.9 us (4%)
    ppermute x22, waiting for transfers between devices, turned(): lax.ppermute(array, 'tp', [(i, (i + by) % size) for i in range(size)])  93.1 us
    all_to_all x6, starting transfers between devices, exchanged(): return lax.all_to_all(array, 'sp', split_axis=0, concat_axis=0, tiled=True)  51.9 us
    all_to_all x6, waiting for transfers between devices, exchanged(): return lax.all_to_all(array, 'sp', split_axis=0, concat_axis=0, tiled=True)  25.3 us
    ppermute x22, starting transfers between devices, turned(): lax.ppermute(array, 'tp', [(i, (i + by) % size) for i in range(size)])  25 us
    pallas_call x2, Pallas kernels, by_rows(): pl.pallas_call(kernel, grid=(slots // part_block,), in_specs=[rows(x.shap...  15.3 us
    ppermute x2, starting transfers between devices, passed_along(): return lax.ppermute(array, axis, pairs)  8.13 us
    dot_general x1, matrix products, on_device(): jnp.einsum('rd,rf->df', entry_rows, late_both, preferred_element_type=f32)  8.03 us
    ppermute x2, waiting for transfers between devices, passed_along(): return lax.ppermute(array, axis, pairs)  8.01 us
  transfers between devices with their start and end apart: 30, of which 13 were waited for; matrix products, arithmetic and copies ran while one was open for 13% of the time, Pallas kernels for 4%

profile of v3, /device:TPU:1, one launch (start us, length us, event | category | flops | bytes accessed | tf_op | source)
XLA Modules:
  0.0 303.3 jit_solution(3721586641157963527)
XLA Ops:
  0.7 5.5 %shard_map.188 = (bf16[1536,512]{1,0:T(8,128)(2,1)}, bf16[1536,384]{1,0:T(8,128)(2,1)}, bf16[384,32]{1,0:T(8,128)(2,1)}, bf16[32,384]{1,0:T(8,128)(2,1)}, bf16[32,384]{1,0:T(8,128)(2,1)}) custom-call(s32[1]{0:T(128)} %bitcast.lane_ref, s32[2,384]{1,0:T(2,128)} %bitcast.81, f32[2,384]{1,0:T(2,128)} %bitcast.82, bf16[384,2048]{1,0:T(8,128)(2,1)} %refs_13_.1, ...), custom_call_target="tpu_custom_call" | custom-call | tf_op jit(solution)/shard_map/pallas_call | solution.py:181
  6.2 9.6 %all-to-all-start.1 = ((bf16[32,48,512]{2,1,0:T(8,128)(2,1)}), bf16[32,48,512]{2,1,0:T(8,128)(2,1)S(1)}, u32[]{:S(2)}, u32[]{:S(2)}) async-start(bf16[32,48,512]{2,1,0:T(8,128)(2,1)} %bitcast.69), calls=%async_computation.1 | async-start | bytes 3145728 | tf_op jit(solution)/shard_map/all_to_all | solution.py:26
  15.8 7.8 %shard_map.189 = (bf16[1536,2048]{1,0:T(8,128)(2,1)}, bf16[384,1536]{1,0:T(8,128)(2,1)}) custom-call(bf16[1536,384]{1,0:T(8,128)(2,1)} %get-tuple-element.41.chooser_ref, bf16[384,2048]{1,0:T(8,128)(2,1)} %refs_12_.1, bf16[384,32]{1,0:T(8,128)(2,1)} %get-tuple-element.42.rank_ref, bf16[32,384]{1,0:T(8,128)(2,1)} %get-tuple-element.43.high_ref, ...), custom_call_target="tpu_custom_call" | custom-call | tf_op jit(solution)/shard_map/pallas_call | solution.py:236
  23.5 14.4 %all-to-all-done.1 = bf16[32,48,512]{2,1,0:T(8,128)(2,1)S(1)} async-done(((bf16[32,48,512]{2,1,0:T(8,128)(2,1)}), bf16[32,48,512]{2,1,0:T(8,128)(2,1)S(1)}, u32[]{:S(2)}, u32[]{:S(2)}) %all-to-all-start.1) | async-done | bytes 1572896 | tf_op jit(solution)/shard_map/all_to_all | solution.py:26
  39.1 6.6 %all-to-all-start = ((bf16[32,48,2048]{2,1,0:T(8,128)(2,1)}), bf16[32,48,2048]{2,1,0:T(8,128)(2,1)}, u32[]{:S(2)}, u32[]{:S(2)}) async-start(bf16[32,48,2048]{2,1,0:T(8,128)(2,1)} %bitcast.63), calls=%async_computation | async-start | bytes 12582912 | tf_op jit(solution)/shard_map/all_to_all | solution.py:26
  50.7 32.1 %collective-permute-done = bf16[1536,512]{1,0:T(8,128)(2,1)} collective-permute-done((bf16[1536,512]{1,0:T(8,128)(2,1)}, bf16[1536,512]{1,0:T(8,128)(2,1)}, u32[]{:S(2)}, u32[]{:S(2)}) %collective-permute-start) | collective-permute-done | bytes 1572896 | tf_op jit(solution)/shard_map/ppermute | solution.py:22
  85.3 2.7 collective-permute-start.3
  92.5 10.8 %collective-permute-done.2 = bf16[768,512]{1,0:T(8,128)(2,1)S(1)} collective-permute-done((bf16[768,512]{1,0:T(8,128)(2,1)S(1)}, bf16[768,512]{1,0:T(8,128)(2,1)S(1)}, u32[]{:S(2)}, u32[]{:S(2)}) %collective-permute-start.2) | collective-permute-done | bytes 786464 | tf_op jit(solution)/shard_map/ppermute | solution.py:22
  106.1 3.5 %multiply_convert_fusion = (bf16[1536,256]{1,0:T(8,128)(2,1)S(1)}, bf16[1536,256]{1,0:T(8,128)(2,1)}, bf16[1536,256]{1,0:T(8,128)(2,1)}) fusion(f32[1536,256]{1,0:T(8,128)S(1)} %fusion.31, bf16[1536,2048]{1,0:T(8,128)(2,1)S(1)} %constant_dynamic-update-slice_fusion.4, bf16[1,2048,256]{2,1,0:T(8,128)(2,1)S(1)} %copy-done.2), kind=kOutput, calls=%fused_computation.21 | convolution fusion | flops 1615724544 | bytes 11272192 | tf_op jit(solution)/shard_map/dot_general | solution.py:333
  109.7 9.3 %all-to-all-done = bf16[32,48,2048]{2,1,0:T(8,128)(2,1)} async-done(((bf16[32,48,2048]{2,1,0:T(8,128)(2,1)}), bf16[32,48,2048]{2,1,0:T(8,128)(2,1)}, u32[]{:S(2)}, u32[]{:S(2)}) %all-to-all-start) | async-done | bytes 6291488 | tf_op jit(solution)/shard_map/all_to_all | solution.py:26
  119.0 10.4 %shard_map.190 = (bf16[1536,512]{1,0:T(8,128)(2,1)}, bf16[1536,128]{1,0:T(8,128)(2,1)}, bf16[1536,128]{1,0:T(8,128)(2,1)}, bf16[1536,128]{1,0:T(8,128)(2,1)}, bf...) custom-call(bf16[1536,2048]{1,0:T(8,128)(2,1)} %bitcast.5.cot_ref, bf16[1536,256]{1,0:T(8,128)(2,1)} %get-tuple-element.48.act_ref, ...), custom_call_target="tpu_custom_call" | custom-call | tf_op jit(solution)/shard_map/pallas_call | solution.py:285
  131.9 5.8 %collective-permute-start.22 = (f32[2,256]{1,0:T(2,128)S(1)}, f32[2,256]{1,0:T(2,128)S(1)}, u32[]{:S(2)}, u32[]{:S(2)}) collective-permute-start(f32[2,256]{1,0:T(2,128)S(1)} %slice.53), channel_id=1, source_target_pairs={{0,4},{4,8},{8,12},{12,16},{16,20},{20,24},{24,28},{28,32},{32,36}... | collective-permute-start | bytes 6152 | tf_op jit(solution)/shard_map/ppermute | solution.py:17
  137.8 2.7 collective-permute-start.6
  140.5 6.2 %all-to-all-start.3 = ((bf16[32,48,512]{2,1,0:T(8,128)(2,1)}), bf16[32,48,512]{2,1,0:T(8,128)(2,1)}, u32[]{:S(2)}, u32[]{:S(2)}) async-start(bf16[32,48,512]{2,1,0:T(8,128)(2,1)} %bitcast.68), calls=%async_computation.3 | async-start | bytes 3145728 | tf_op jit(solution)/shard_map/all_to_all | solution.py:26
  146.7 4.9 %shard_map.191 = (bf16[1536,128]{1,0:T(8,128)(2,1)}, bf16[1536,128]{1,0:T(8,128)(2,1)}, bf16[1536,128]{1,0:T(8,128)(2,1)}, bf16[1536,128]{1,0:T(8,128)(2,1)}, bf...) custom-call(bf16[1536,512]{1,0:T(8,128)(2,1)} %get-tuple-element.70., ...), custom_call_target="tpu_custom_call" | custom-call | tf_op jit(solution)/shard_map/pallas_call | solution.py:285
  151.7 2.7 collective-permute-start.15
  160.5 10.8 %collective-permute-done.9 = bf16[1536,128]{1,0:T(8,128)(2,1)S(1)} collective-permute-done((bf16[1536,128]{1,0:T(8,128)(2,1)S(1)}, bf16[1536,128]{1,0:T(8,128)(2,1)S(1)}, u32[]{:S(2)}, u32[]{:S(2)}) %collective-permute-start.9) | collective-permute-done | bytes 393248 | tf_op jit(solution)/shard_map/ppermute | solution.py:22
  172.4 10.6 %collective-permute-done.5 = bf16[1536,128]{1,0:T(8,128)(2,1)S(1)} collective-permute-done((bf16[1536,128]{1,0:T(8,128)(2,1)S(1)}, bf16[1536,128]{1,0:T(8,128)(2,1)S(1)}, u32[]{:S(2)}, u32[]{:S(2)}) %collective-permute-start.5) | collective-permute-done | bytes 393248 | tf_op jit(solution)/shard_map/ppermute | solution.py:22
  185.2 8.8 %all-to-all-start.2 = ((bf16[32,48,256]{2,1,0:T(8,128)(2,1)}), bf16[32,48,256]{2,1,0:T(8,128)(2,1)}, u32[]{:S(2)}, u32[]{:S(2)}) async-start(bf16[32,48,256]{2,1,0:T(8,128)(2,1)} %bitcast.14), calls=%async_computation.2 | async-start | bytes 1572864 | tf_op jit(solution)/shard_map/all_to_all | solution.py:26
  195.4 11.5 %collective-permute-done.14 = bf16[1536,128]{1,0:T(8,128)(2,1)S(1)} collective-permute-done((bf16[1536,128]{1,0:T(8,128)(2,1)S(1)}, bf16[1536,128]{1,0:T(8,128)(2,1)S(1)}, u32[]{:S(2)}, u32[]{:S(2)}) %collective-permute-start.14) | collective-permute-done | bytes 393248 | tf_op jit(solution)/shard_map/ppermute | solution.py:22
  208.8 8.0 %all-to-all-start.4 = ((bf16[32,48,128]{2,1,0:T(8,128)(2,1)}), bf16[32,48,128]{2,1,0:T(8,128)(2,1)S(1)}, u32[]{:S(2)}, u32[]{:S(2)}) async-start(bf16[32,48,128]{2,1,0:T(8,128)(2,1)} %bitcast.18), calls=%async_computation.4 | async-start | bytes 786432 | tf_op jit(solution)/shard_map/all_to_all | solution.py:26
  219.6 2.7 collective-permute-start.20
  224.5 2.7 collective-permute-start.11
  229.0 10.8 %collective-permute-done.10.refs_1_ = bf16[384,256]{1,0:T(8,128)(2,1)} collective-permute-done((bf16[384,256]{1,0:T(8,128)(2,1)}, bf16[384,256]{1,0:T(8,128)(2,1)}, u32[]{:S(2)}, u32[]{:S(2)}) %collective-permute-start.10) | collective-permute-done | bytes 196640 | tf_op jit(solution)/shard_map/ppermute | solution.py:22
  239.8 2.7 collective-permute-start.17
  244.2 5.9 %convolution_bitcast_fusion = f32[1,256,2048]{2,1,0:T(8,128)} fusion(bf16[1536,256]{1,0:T(8,128)(2,1)S(1)} %get-tuple-element.72, bf16[1536,2048]{1,0:T(8,128)(2,1)} %bitcast.5.cot_ref), kind=kOutput, calls=%fused_computation.16 | convolution fusion | flops 1610612736 | bytes 9175040 | tf_op jit(solution)/shard_map/rf,rd->fd/dot_general | solution.py:387
  250.9 3.7 %collective-permute-done.16.refs_5_ = bf16[384,128]{1,0:T(8,128)(2,1)S(1)} collective-permute-done((bf16[384,128]{1,0:T(8,128)(2,1)S(1)}, bf16[384,128]{1,0:T(8,128)(2,1)S(1)}, u32[]{:S(2)}, u32[]{:S(2)}) %collective-permute-start.16) | collective-permute-done | bytes 98336 | tf_op jit(solution)/shard_map/ppermute | solution.py:22
  255.3 5.0 %shard_map.192 = bf16[384,2048]{1,0:T(8,128)(2,1)} custom-call(s32[1]{0:T(128)} %bitcast.lane_ref, bf16[384,256]{1,0:T(8,128)(2,1)} %convolution_convert_fusion.2.refs_0_, bf16[384,256]{1,0:T(8,128)(2,1)} %collective-permute-done.10.refs_1_, bf16[384,256]{1,0:T(8,128)(2,1)} %collective-permute-done.11.refs_2_, ...), custom_call_target="tpu_custom_call" | custom-call | tf_op jit(solution)/shard_map/pallas_call | solution.py:97
  260.3 3.3 %convolution_convert_fusion = bf16[2048,256]{1,0:T(8,128)(2,1)} fusion(bf16[384,2048]{1,0:T(8,128)(2,1)} %shard_map.192, f32[384,256]{1,0:T(8,128)S(1)} %fusion.8, bf16[384,256]{1,0:T(8,128)(2,1)S(1)} %copy-done.23), kind=kOutput, calls=%fused_computation.17 | convolution fusion | flops 403472384 | bytes 3211264 | tf_op jit(solution)/shard_map/td,tc->dc/dot_general | solution.py:406
  263.6 8.0 %fusion.35 = f32[2048,512]{1,0:T(8,128)} fusion(bf16[1536,2048]{1,0:T(8,128)(2,1)} %copy-done.4, bf16[1536,512]{1,0:T(8,128)(2,1)S(1)} %copy-done.9), kind=kOutput, calls=%fused_computation.86 | convolution fusion | flops 3221225472 | bytes 12058624 | tf_op jit(solution)/shard_map/rd,rf->df/dot_general | solution.py:410
  271.6 12.7 %all-to-all-start.5 = ((bf16[32,64,256]{2,1,0:T(8,128)(2,1)}), bf16[32,64,256]{2,1,0:T(8,128)(2,1)}, u32[]{:S(2)}, u32[]{:S(2)}) async-start(bf16[32,64,256]{2,1,0:T(8,128)(2,1)} %bitcast.72), calls=%async_computation.5 | async-start | bytes 2097152 | tf_op jit(solution)/shard_map/all_to_all | solution.py:26
  290.2 8.0 %collective-permute-done.23 = f32[2,256]{1,0:T(2,128)S(1)} collective-permute-done((f32[2,256]{1,0:T(2,128)S(1)}, f32[2,256]{1,0:T(2,128)S(1)}, u32[]{:S(2)}, u32[]{:S(2)}) %collective-permute-start.23) | collective-permute-done | bytes 2080 | tf_op jit(solution)/shard_map/ppermute | solution.py:17
  (127 shorter events, 52.1 us)
Async XLA Ops:
  0.6 283.6 %copy-start = (bf16[2048,256]{1,0:T(8,128)(2,1)S(1)}, bf16[2048,256]{1,0:T(8,128)(2,1)}, u32[]{:S(2)}) copy-start(bf16[2048,256]{1,0:T(8,128)(2,1)} %param.21) | copy-start | bytes 3145732
  6.2 31.8 %all-to-all-start.1 = ((bf16[32,48,512]{2,1,0:T(8,128)(2,1)}), bf16[32,48,512]{2,1,0:T(8,128)(2,1)S(1)}, u32[]{:S(2)}, u32[]{:S(2)}) async-start(bf16[32,48,512]{2,1,0:T(8,128)(2,1)} %bitcast.69), calls=%async_computation.1 | async-start | bytes 3145728 | tf_op jit(solution)/shard_map/all_to_all | solution.py:26
  39.1 79.9 %all-to-all-start = ((bf16[32,48,2048]{2,1,0:T(8,128)(2,1)}), bf16[32,48,2048]{2,1,0:T(8,128)(2,1)}, u32[]{:S(2)}, u32[]{:S(2)}) async-start(bf16[32,48,2048]{2,1,0:T(8,128)(2,1)} %bitcast.63), calls=%async_computation | async-start | bytes 12582912 | tf_op jit(solution)/shard_map/all_to_all | solution.py:26
  45.7 37.1 %collective-permute-start = (bf16[1536,512]{1,0:T(8,128)(2,1)}, bf16[1536,512]{1,0:T(8,128)(2,1)}, u32[]{:S(2)}, u32[]{:S(2)}) collective-permute-start(bf16[1536,512]{1,0:T(8,128)(2,1)} %bitcast.64), channel_id=1, source_target_pairs={{0,1},{1,2},{2,3},{3,0},{4,5},{5,6},{6,7},{7,4},{8,9},{9,10},{10,1... | collective-permute-start | bytes 4718600 | tf_op jit(solution)/shard_map/ppermute | solution.py:22
  47.0 37.1 %collective-permute-start.1 = (bf16[1536,512]{1,0:T(8,128)(2,1)}, bf16[1536,512]{1,0:T(8,128)(2,1)}, u32[]{:S(2)}, u32[]{:S(2)}) collective-permute-start(bf16[1536,512]{1,0:T(8,128)(2,1)} %bitcast.65), channel_id=1, source_target_pairs={{0,3},{1,0},{2,1},{3,2},{4,7},{5,4},{6,5},{7,6},{8,11},{9,8},{10,9... | collective-permute-start | bytes 4718600 | tf_op jit(solution)/shard_map/ppermute | solution.py:22
  84.0 19.2 %collective-permute-start.2 = (bf16[768,512]{1,0:T(8,128)(2,1)S(1)}, bf16[768,512]{1,0:T(8,128)(2,1)S(1)}, u32[]{:S(2)}, u32[]{:S(2)}) collective-permute-start(bf16[768,512]{1,0:T(8,128)(2,1)S(1)} %slice.51), channel_id=1, source_target_pairs={{0,1},{1,2},{2,3},{3,0},{4,5},{5,6},{6,7},{7,4},{8,9},{9,10},{10,1... | collective-permute-start | bytes 2359304 | tf_op jit(solution)/shard_map/ppermute | solution.py:22
  85.3 18.1 %collective-permute-start.3 = (bf16[768,512]{1,0:T(8,128)(2,1)S(1)}, bf16[768,512]{1,0:T(8,128)(2,1)S(1)}, u32[]{:S(2)}, u32[]{:S(2)}) collective-permute-start(bf16[768,512]{1,0:T(8,128)(2,1)S(1)} %slice.52), channel_id=1, source_target_pairs={{0,3},{1,0},{2,1},{3,2},{4,7},{5,4},{6,5},{7,6},{8,11},{9,8},{10,9... | collective-permute-start | bytes 2359304 | tf_op jit(solution)/shard_map/ppermute | solution.py:22
  129.4 22.3 %collective-permute-start.8 = (bf16[1536,128]{1,0:T(8,128)(2,1)}, bf16[1536,128]{1,0:T(8,128)(2,1)}, u32[]{:S(2)}, u32[]{:S(2)}) collective-permute-start(bf16[1536,128]{1,0:T(8,128)(2,1)} %get-tuple-element.61), channel_id=1, source_target_pairs={{0,3},{1,0},{2,1},{3,2},{4,7},{5,4},{6,5},{7,6},{8,11},{9,8},{10,9... | collective-permute-start | bytes 1179656 | tf_op jit(solution)/shard_map/ppermute | solution.py:22
  131.9 63.3 %collective-permute-start.22 = (f32[2,256]{1,0:T(2,128)S(1)}, f32[2,256]{1,0:T(2,128)S(1)}, u32[]{:S(2)}, u32[]{:S(2)}) collective-permute-start(f32[2,256]{1,0:T(2,128)S(1)} %slice.53), channel_id=1, source_target_pairs={{0,4},{4,8},{8,12},{12,16},{16,20},{20,24},{24,28},{28,32},{32,36}... | collective-permute-start | bytes 6152 | tf_op jit(solution)/shard_map/ppermute | solution.py:17
  137.7 21.2 %collective-permute-start.7 = (bf16[1536,128]{1,0:T(8,128)(2,1)}, bf16[1536,128]{1,0:T(8,128)(2,1)S(1)}, u32[]{:S(2)}, u32[]{:S(2)}) collective-permute-start(bf16[1536,128]{1,0:T(8,128)(2,1)} %get-tuple-element.59), channel_id=1, source_target_pairs={{0,1},{1,2},{2,3},{3,0},{4,5},{5,6},{6,7},{7,4},{8,9},{9,10},{10,1... | collective-permute-start | bytes 1179656 | tf_op jit(solution)/shard_map/ppermute | solution.py:22
  137.8 34.6 %collective-permute-start.6 = (bf16[1536,128]{1,0:T(8,128)(2,1)}, bf16[1536,128]{1,0:T(8,128)(2,1)S(1)}, u32[]{:S(2)}, u32[]{:S(2)}) collective-permute-start(bf16[1536,128]{1,0:T(8,128)(2,1)} %get-tuple-element.57), channel_id=1, source_target_pairs={{0,3},{1,0},{2,1},{3,2},{4,7},{5,4},{6,5},{7,6},{8,11},{9,8},{10,9... | collective-permute-start | bytes 1179656 | tf_op jit(solution)/shard_map/ppermute | solution.py:22
  140.5 17.2 %collective-permute-start.4 = (bf16[1536,128]{1,0:T(8,128)(2,1)}, bf16[1536,128]{1,0:T(8,128)(2,1)}, u32[]{:S(2)}, u32[]{:S(2)}) collective-permute-start(bf16[1536,128]{1,0:T(8,128)(2,1)} %get-tuple-element.56), channel_id=1, source_target_pairs={{0,1},{1,2},{2,3},{3,0},{4,5},{5,6},{6,7},{7,4},{8,9},{9,10},{10,1... | collective-permute-start | bytes 1179656 | tf_op jit(solution)/shard_map/ppermute | solution.py:22
  140.5 44.7 %all-to-all-start.3 = ((bf16[32,48,512]{2,1,0:T(8,128)(2,1)}), bf16[32,48,512]{2,1,0:T(8,128)(2,1)}, u32[]{:S(2)}, u32[]{:S(2)}) async-start(bf16[32,48,512]{2,1,0:T(8,128)(2,1)} %bitcast.68), calls=%async_computation.3 | async-start | bytes 3145728 | tf_op jit(solution)/shard_map/all_to_all | solution.py:26
  151.6 31.3 %copy-start.21 = (bf16[1536,128]{1,0:T(8,128)(2,1)S(1)}, bf16[1536,128]{1,0:T(8,128)(2,1)}, u32[]{:S(2)}) copy-start(bf16[1536,128]{1,0:T(8,128)(2,1)} %get-tuple-element.54) | copy-start | bytes 1179652
  151.7 43.7 %collective-permute-start.15 = (bf16[1536,128]{1,0:T(8,128)(2,1)}, bf16[1536,128]{1,0:T(8,128)(2,1)}, u32[]{:S(2)}, u32[]{:S(2)}) collective-permute-start(bf16[1536,128]{1,0:T(8,128)(2,1)} %get-tuple-element.68), channel_id=1, source_target_pairs={{0,3},{1,0},{2,1},{3,2},{4,7},{5,4},{6,5},{7,6},{8,11},{9,8},{10,9... | collective-permute-start | bytes 1179656 | tf_op jit(solution)/shard_map/ppermute | solution.py:22
  157.7 13.5 %collective-permute-start.9 = (bf16[1536,128]{1,0:T(8,128)(2,1)S(1)}, bf16[1536,128]{1,0:T(8,128)(2,1)S(1)}, u32[]{:S(2)}, u32[]{:S(2)}) collective-permute-start(bf16[1536,128]{1,0:T(8,128)(2,1)S(1)} %add_convert_fusion.3), channel_id=1, source_target_pairs={{0,3},{1,0},{2,1},{3,2},{4,7},{5,4},{6,5},{7,6},{8,11},{9,8},{10,9... | collective-permute-start | bytes 1179656 | tf_op jit(solution)/shard_map/ppermute | solution.py:22
  158.9 35.1 %collective-permute-start.13 = (bf16[1536,128]{1,0:T(8,128)(2,1)}, bf16[1536,128]{1,0:T(8,128)(2,1)}, u32[]{:S(2)}, u32[]{:S(2)}) collective-permute-start(bf16[1536,128]{1,0:T(8,128)(2,1)} %get-tuple-element.67), channel_id=1, source_target_pairs={{0,1},{1,2},{2,3},{3,0},{4,5},{5,6},{6,7},{7,4},{8,9},{9,10},{10,1... | collective-permute-start | bytes 1179656 | tf_op jit(solution)/shard_map/ppermute | solution.py:22
  171.2 11.7 %collective-permute-start.5 = (bf16[1536,128]{1,0:T(8,128)(2,1)S(1)}, bf16[1536,128]{1,0:T(8,128)(2,1)S(1)}, u32[]{:S(2)}, u32[]{:S(2)}) collective-permute-start(bf16[1536,128]{1,0:T(8,128)(2,1)S(1)} %add_convert_fusion.5), channel_id=1, source_target_pairs={{0,1},{1,2},{2,3},{3,0},{4,5},{5,6},{6,7},{7,4},{8,9},{9,10},{10,1... | collective-permute-start | bytes 1179656 | tf_op jit(solution)/shard_map/ppermute | solution.py:22
  185.2 23.6 %all-to-all-start.2 = ((bf16[32,48,256]{2,1,0:T(8,128)(2,1)}), bf16[32,48,256]{2,1,0:T(8,128)(2,1)}, u32[]{:S(2)}, u32[]{:S(2)}) async-start(bf16[32,48,256]{2,1,0:T(8,128)(2,1)} %bitcast.14), calls=%async_computation.2 | async-start | bytes 1572864 | tf_op jit(solution)/shard_map/all_to_all | solution.py:26
  195.1 11.8 %collective-permute-start.14 = (bf16[1536,128]{1,0:T(8,128)(2,1)S(1)}, bf16[1536,128]{1,0:T(8,128)(2,1)S(1)}, u32[]{:S(2)}, u32[]{:S(2)}) collective-permute-start(bf16[1536,128]{1,0:T(8,128)(2,1)S(1)} %add_convert_fusion.1), channel_id=1, source_target_pairs={{0,1},{1,2},{2,3},{3,0},{4,5},{5,6},{6,7},{7,4},{8,9},{9,10},{10,1... | collective-permute-start | bytes 1179656 | tf_op jit(solution)/shard_map/ppermute | solution.py:22
  208.8 18.4 %all-to-all-start.4 = ((bf16[32,48,128]{2,1,0:T(8,128)(2,1)}), bf16[32,48,128]{2,1,0:T(8,128)(2,1)S(1)}, u32[]{:S(2)}, u32[]{:S(2)}) async-start(bf16[32,48,128]{2,1,0:T(8,128)(2,1)} %bitcast.18), calls=%async_computation.4 | async-start | bytes 786432 | tf_op jit(solution)/shard_map/all_to_all | solution.py:26
  219.5 22.9 %collective-permute-start.19 = (bf16[384,512]{1,0:T(8,128)(2,1)S(1)}, bf16[384,512]{1,0:T(8,128)(2,1)}, u32[]{:S(2)}, u32[]{:S(2)}) collective-permute-start(bf16[384,512]{1,0:T(8,128)(2,1)S(1)} %convolution_convert_fusion.1.refs_8_), channel_id=1, source_target_pairs={{0,1},{1,2},{2,3},{3,0},{4,5},{5,6},{6,7},{7,4},{8,9},{9,10},{10,1... | collective-permute-start | bytes 1179656 | tf_op jit(solution)/shard_map/ppermute | solution.py:22
  219.6 30.5 %collective-permute-start.20 = (bf16[384,512]{1,0:T(8,128)(2,1)S(1)}, bf16[384,512]{1,0:T(8,128)(2,1)}, u32[]{:S(2)}, u32[]{:S(2)}) collective-permute-start(bf16[384,512]{1,0:T(8,128)(2,1)S(1)} %convolution_convert_fusion.1.refs_8_), channel_id=1, source_target_pairs={{0,3},{1,0},{2,1},{3,2},{4,7},{5,4},{6,5},{7,6},{8,11},{9,8},{10,9... | collective-permute-start | bytes 1179656 | tf_op jit(solution)/shard_map/ppermute | solution.py:22
  224.5 15.2 %collective-permute-start.10 = (bf16[384,256]{1,0:T(8,128)(2,1)}, bf16[384,256]{1,0:T(8,128)(2,1)}, u32[]{:S(2)}, u32[]{:S(2)}) collective-permute-start(bf16[384,256]{1,0:T(8,128)(2,1)} %convolution_convert_fusion.2.refs_0_), channel_id=1, source_target_pairs={{0,1},{1,2},{2,3},{3,0},{4,5},{5,6},{6,7},{7,4},{8,9},{9,10},{10,1... | collective-permute-start | bytes 589832 | tf_op jit(solution)/shard_map/ppermute | solution.py:22
  224.5 15.2 %collective-permute-start.11 = (bf16[384,256]{1,0:T(8,128)(2,1)}, bf16[384,256]{1,0:T(8,128)(2,1)}, u32[]{:S(2)}, u32[]{:S(2)}) collective-permute-start(bf16[384,256]{1,0:T(8,128)(2,1)} %convolution_convert_fusion.2.refs_0_), channel_id=1, source_target_pairs={{0,3},{1,0},{2,1},{3,2},{4,7},{5,4},{6,5},{7,6},{8,11},{9,8},{10,9... | collective-permute-start | bytes 589832 | tf_op jit(solution)/shard_map/ppermute | solution.py:22
  227.2 12.6 %collective-permute-start.12 = (bf16[384,256]{1,0:T(8,128)(2,1)}, bf16[384,256]{1,0:T(8,128)(2,1)}, u32[]{:S(2)}, u32[]{:S(2)}) collective-permute-start(bf16[384,256]{1,0:T(8,128)(2,1)} %convolution_convert_fusion.2.refs_0_), channel_id=1, source_target_pairs={{0,2},{1,3},{2,0},{3,1},{4,6},{5,7},{6,4},{7,5},{8,10},{9,11},{10,... | collective-permute-start | bytes 589832 | tf_op jit(solution)/shard_map/ppermute | solution.py:22
  239.7 11.2 %collective-permute-start.21 = (bf16[384,512]{1,0:T(8,128)(2,1)S(1)}, bf16[384,512]{1,0:T(8,128)(2,1)S(1)}, u32[]{:S(2)}, u32[]{:S(2)}) collective-permute-start(bf16[384,512]{1,0:T(8,128)(2,1)S(1)} %convolution_convert_fusion.1.refs_8_), channel_id=1, source_target_pairs={{0,2},{1,3},{2,0},{3,1},{4,6},{5,7},{6,4},{7,5},{8,10},{9,11},{10,... | collective-permute-start | bytes 1179656 | tf_op jit(solution)/shard_map/ppermute | solution.py:22
  239.7 14.8 %collective-permute-start.16 = (bf16[384,128]{1,0:T(8,128)(2,1)S(1)}, bf16[384,128]{1,0:T(8,128)(2,1)S(1)}, u32[]{:S(2)}, u32[]{:S(2)}) collective-permute-start(bf16[384,128]{1,0:T(8,128)(2,1)S(1)} %convolution_convert_fusion.3.refs_4_), channel_id=1, source_target_pairs={{0,1},{1,2},{2,3},{3,0},{4,5},{5,6},{6,7},{7,4},{8,9},{9,10},{10,1... | collective-permute-start | bytes 294920 | tf_op jit(solution)/shard_map/ppermute | solution.py:22
  239.8 14.8 %collective-permute-start.17 = (bf16[384,128]{1,0:T(8,128)(2,1)S(1)}, bf16[384,128]{1,0:T(8,128)(2,1)S(1)}, u32[]{:S(2)}, u32[]{:S(2)}) collective-permute-start(bf16[384,128]{1,0:T(8,128)(2,1)S(1)} %convolution_convert_fusion.3.refs_4_), channel_id=1, source_target_pairs={{0,3},{1,0},{2,1},{3,2},{4,7},{5,4},{6,5},{7,6},{8,11},{9,8},{10,9... | collective-permute-start | bytes 294920 | tf_op jit(solution)/shard_map/ppermute | solution.py:22
  242.4 12.8 %collective-permute-start.18 = (bf16[384,128]{1,0:T(8,128)(2,1)S(1)}, bf16[384,128]{1,0:T(8,128)(2,1)}, u32[]{:S(2)}, u32[]{:S(2)}) collective-permute-start(bf16[384,128]{1,0:T(8,128)(2,1)S(1)} %convolution_convert_fusion.3.refs_4_), channel_id=1, source_target_pairs={{0,2},{1,3},{2,0},{3,1},{4,6},{5,7},{6,4},{7,5},{8,10},{9,11},{10,... | collective-permute-start | bytes 294920 | tf_op jit(solution)/shard_map/ppermute | solution.py:22
  271.6 29.8 %all-to-all-start.5 = ((bf16[32,64,256]{2,1,0:T(8,128)(2,1)}), bf16[32,64,256]{2,1,0:T(8,128)(2,1)}, u32[]{:S(2)}, u32[]{:S(2)}) async-start(bf16[32,64,256]{2,1,0:T(8,128)(2,1)} %bitcast.72), calls=%async_computation.5 | async-start | bytes 2097152 | tf_op jit(solution)/shard_map/all_to_all | solution.py:26
  285.5 12.7 %collective-permute-start.23 = (f32[2,256]{1,0:T(2,128)S(1)}, f32[2,256]{1,0:T(2,128)S(1)}, u32[]{:S(2)}, u32[]{:S(2)}) collective-permute-start(f32[2,256]{1,0:T(2,128)S(1)} %slice.56), channel_id=1, source_target_pairs={{4,0},{8,4},{12,8},{16,12},{20,16},{24,20},{28,24},{32,28},{36,32}... | collective-permute-start | bytes 6152 | tf_op jit(solution)/shard_map/ppermute | solution.py:17
  (25 other events, 244.2 us)

commit v4 on v3

--- a/solution.py
+++ b/solution.py
@@ -269,8 +269,13 @@
     write_parts(both, mat_ref, refs)
 
 
-def other_kernel(both_ref, mat_ref, *refs):
-    write_parts(both_ref[...], mat_ref, refs)
+def other_kernel(both_ref, a_far_ref, b_far_ref, mat_ref, *refs):
+    part = lax.dot_general(both_ref[...], mat_ref[...], along_last, preferred_element_type=f32)
+    for i, ref in enumerate(refs):
+        piece = part[:, i * direct_width : (i + 1) * direct_width]
+        if i < 2:
+            piece = piece + (a_far_ref, b_far_ref)[i][...].astype(f32)
+        ref[...] = piece.astype(bf16)
 
 
 part_block = 512
@@ -348,8 +353,8 @@
         axis=0,
     )
     other_mat = jnp.concatenate(
-        [weight_rows(0, 0, 3), weight_rows(1, 0, 1), weight_rows(1, 2, 1)]
-        + [weight_rows(3, 1, 2), weight_rows(2, 2, 1)],
+        [weight_rows(1, 0, 1), weight_rows(3, 1, 2), weight_rows(2, 2, 1)]
+        + [weight_rows(0, 0, 3), weight_rows(1, 2, 1)],
         axis=0,
     )
     activated, slope, hidden, first_mat, other_mat = lax.optimization_barrier(
@@ -361,9 +366,6 @@
         (down_mat, first_mat),
         [both_mat.shape[1]] + [direct_width] * 4 + [lanes * direct_width],
     )
-    a_own, b_own, c_own, a_ahead, c_ahead, b_behind, c_behind, c_far = by_rows(
-        other_kernel, (dboth,), (other_mat,), [direct_width] * 8
-    )
 
     def back(array):
         return exchanged(array.reshape(groups, capacity, -1)).reshape(slots, -1)
@@ -377,13 +379,16 @@
     a_far = turned(a_far, 1)
     b_far = turned(b_far, -1)
     direct = back(direct)
-    c_ahead, direct = lax.optimization_barrier((c_ahead, direct))
     a_next = turned(a_behind, -1)
     b_prev = turned(b_ahead, 1)
-    a_prev = turned(plus(a_ahead, a_far), 1)
-    b_next = turned(plus(b_behind, b_far), -1)
+    a_ahead, b_behind, c_behind, c_far, a_own, b_own, c_own, c_ahead = by_rows(
+        other_kernel, (dboth, a_far, b_far), (other_mat,), [direct_width] * 8
+    )
+    a_prev = turned(a_ahead, 1)
+    b_next = turned(b_behind, -1)
     c_far = turned(c_far, 1)
     c_next = turned(c_behind, -1)
+    c_ahead, direct = lax.optimization_barrier((c_ahead, direct))
     grad_down = jnp.einsum("rf,rd->fd", hidden, entry_cots, preferred_element_type=f32)
     wide = jnp.concatenate([plus(a_own, a_prev, a_next), plus(b_own, b_prev, b_next)], axis=1)
     c_own, wide = lax.optimization_barrier((c_own, wide))

time: 305 us -> 294 us (0.964)
  waiting for transfers between devices: 126 us -> 121 us
  other arithmetic: 13.7 us -> 10.5 us
    ppermute x22, waiting for transfers between devices: 93.1 us -> 83.4 us  [turned(): lax.ppermute(array, 'tp', [(i, (i + by) % size) for i in range(size)])]
    all_to_all x6, waiting for transfers between devices: 25.3 us -> 29.7 us  [exchanged(): return lax.all_to_all(array, 'sp', split_axis=0, concat_axis=0, tiled=True)]
    convert_element_type x6 -> x4, other arithmetic: 7.79 us -> 4.54 us  [plus(): return sum((array.astype(f32) for array in arrays)).astype(bf16)]
  transfers between devices with their start and end apart: 30 -> 30, of which waited for: 13 -> 14; matrix products, arithmetic and copies ran while one was open for 13% -> 13% of each run, Pallas kernels for 4% -> 4%
where the time goes in v4:
time: 294 us; the launch traced here: 293 us
  waiting for transfers between devices  121 us (41%)
  starting transfers between devices  82.1 us (28%)
  Pallas kernels  33.8 us (11%)
  matrix products  30.6 us (10%)
  local copies, waits for them, and re-layouts  13.8 us (5%)
  other arithmetic  10.5 us (4%)
    ppermute x22, waiting for transfers between devices, turned(): lax.ppermute(array, 'tp', [(i, (i + by) % size) for i in range(size)])  83.4 us
    all_to_all x6, starting transfers between devices, exchanged(): return lax.all_to_all(array, 'sp', split_axis=0, concat_axis=0, tiled=True)  52.2 us
    all_to_all x6, waiting for transfers between devices, exchanged(): return lax.all_to_all(array, 'sp', split_axis=0, concat_axis=0, tiled=True)  29.7 us
    ppermute x22, starting transfers between devices, turned(): lax.ppermute(array, 'tp', [(i, (i + by) % size) for i in range(size)])  23.9 us
    pallas_call x2, Pallas kernels, by_rows(): pl.pallas_call(kernel, grid=(slots // part_block,), in_specs=[rows(x.shap...  15.5 us
    dot_general x1, matrix products, on_device(): jnp.einsum('rd,rf->df', entry_rows, late_both, preferred_element_type=f32)  8.03 us
    ppermute x2, waiting for transfers between devices, passed_along(): return lax.ppermute(array, axis, pairs)  8.01 us
    pallas_call x1, Pallas kernels, weighted_rows(): pl.pallas_call(weighted_kernel, grid=(slots // slot_block,), in_specs=[pl...  7.77 us
  transfers between devices with their start and end apart: 30, of which 14 were waited for; matrix products, arithmetic and copies ran while one was open for 13% of the time, Pallas kernels for 4%

profile of v4, /device:TPU:1, one launch (start us, length us, event | category | flops | bytes accessed | tf_op | source)
XLA Modules:
  0.0 293.0 jit_solution(12505957913500932408)
XLA Ops:
  0.7 5.5 %shard_map.188 = (bf16[1536,512]{1,0:T(8,128)(2,1)}, bf16[1536,384]{1,0:T(8,128)(2,1)}, bf16[384,32]{1,0:T(8,128)(2,1)}, bf16[32,384]{1,0:T(8,128)(2,1)}, bf16[32,384]{1,0:T(8,128)(2,1)}) custom-call(s32[1]{0:T(128)} %bitcast.lane_ref, s32[2,384]{1,0:T(2,128)} %bitcast.81, f32[2,384]{1,0:T(2,128)} %bitcast.82, bf16[384,2048]{1,0:T(8,128)(2,1)} %refs_13_.1, ...), custom_call_target="tpu_custom_call" | custom-call | tf_op jit(solution)/shard_map/pallas_call | solution.py:181
  6.2 9.6 %all-to-all-start.1 = ((bf16[32,48,512]{2,1,0:T(8,128)(2,1)}), bf16[32,48,512]{2,1,0:T(8,128)(2,1)S(1)}, u32[]{:S(2)}, u32[]{:S(2)}) async-start(bf16[32,48,512]{2,1,0:T(8,128)(2,1)} %bitcast.69), calls=%async_computation.1 | async-start | bytes 3145728 | tf_op jit(solution)/shard_map/all_to_all | solution.py:26
  15.8 7.8 %shard_map.189 = (bf16[1536,2048]{1,0:T(8,128)(2,1)}, bf16[384,1536]{1,0:T(8,128)(2,1)}) custom-call(bf16[1536,384]{1,0:T(8,128)(2,1)} %get-tuple-element.41.chooser_ref, bf16[384,2048]{1,0:T(8,128)(2,1)} %refs_12_.1, bf16[384,32]{1,0:T(8,128)(2,1)} %get-tuple-element.42.rank_ref, bf16[32,384]{1,0:T(8,128)(2,1)} %get-tuple-element.43.high_ref, ...), custom_call_target="tpu_custom_call" | custom-call | tf_op jit(solution)/shard_map/pallas_call | solution.py:236
  23.5 14.4 %all-to-all-done.1 = bf16[32,48,512]{2,1,0:T(8,128)(2,1)S(1)} async-done(((bf16[32,48,512]{2,1,0:T(8,128)(2,1)}), bf16[32,48,512]{2,1,0:T(8,128)(2,1)S(1)}, u32[]{:S(2)}, u32[]{:S(2)}) %all-to-all-start.1) | async-done | bytes 1572896 | tf_op jit(solution)/shard_map/all_to_all | solution.py:26
  39.1 6.6 %all-to-all-start = ((bf16[32,48,2048]{2,1,0:T(8,128)(2,1)}), bf16[32,48,2048]{2,1,0:T(8,128)(2,1)}, u32[]{:S(2)}, u32[]{:S(2)}) async-start(bf16[32,48,2048]{2,1,0:T(8,128)(2,1)} %bitcast.63), calls=%async_computation | async-start | bytes 12582912 | tf_op jit(solution)/shard_map/all_to_all | solution.py:26
  50.7 32.1 %collective-permute-done = bf16[1536,512]{1,0:T(8,128)(2,1)} collective-permute-done((bf16[1536,512]{1,0:T(8,128)(2,1)}, bf16[1536,512]{1,0:T(8,128)(2,1)}, u32[]{:S(2)}, u32[]{:S(2)}) %collective-permute-start) | collective-permute-done | bytes 1572896 | tf_op jit(solution)/shard_map/ppermute | solution.py:22
  85.3 2.7 collective-permute-start.3
  92.5 10.8 %collective-permute-done.2 = bf16[768,512]{1,0:T(8,128)(2,1)S(1)} collective-permute-done((bf16[768,512]{1,0:T(8,128)(2,1)S(1)}, bf16[768,512]{1,0:T(8,128)(2,1)S(1)}, u32[]{:S(2)}, u32[]{:S(2)}) %collective-permute-start.2) | collective-permute-done | bytes 786464 | tf_op jit(solution)/shard_map/ppermute | solution.py:22
  106.1 3.5 %multiply_convert_fusion = (bf16[1536,256]{1,0:T(8,128)(2,1)S(1)}, bf16[1536,256]{1,0:T(8,128)(2,1)}, bf16[1536,256]{1,0:T(8,128)(2,1)}) fusion(f32[1536,256]{1,0:T(8,128)S(1)} %fusion.31, bf16[1536,2048]{1,0:T(8,128)(2,1)S(1)} %constant_dynamic-update-slice_fusion.4, bf16[1,2048,256]{2,1,0:T(8,128)(2,1)S(1)} %copy-done.2), kind=kOutput, calls=%fused_computation.21 | convolution fusion | flops 1615724544 | bytes 11272192 | tf_op jit(solution)/shard_map/dot_general | solution.py:338
  109.7 9.3 %all-to-all-done = bf16[32,48,2048]{2,1,0:T(8,128)(2,1)} async-done(((bf16[32,48,2048]{2,1,0:T(8,128)(2,1)}), bf16[32,48,2048]{2,1,0:T(8,128)(2,1)}, u32[]{:S(2)}, u32[]{:S(2)}) %all-to-all-start) | async-done | bytes 6291488 | tf_op jit(solution)/shard_map/all_to_all | solution.py:26
  119.0 10.3 %shard_map.190 = (bf16[1536,512]{1,0:T(8,128)(2,1)}, bf16[1536,128]{1,0:T(8,128)(2,1)}, bf16[1536,128]{1,0:T(8,128)(2,1)}, bf16[1536,128]{1,0:T(8,128)(2,1)}, bf...) custom-call(bf16[1536,2048]{1,0:T(8,128)(2,1)} %bitcast.5.cot_ref, bf16[1536,256]{1,0:T(8,128)(2,1)} %get-tuple-element.48.act_ref, ...), custom_call_target="tpu_custom_call" | custom-call | tf_op jit(solution)/shard_map/pallas_call | solution.py:290
  132.1 5.3 %collective-permute-done.4.a_far_ref = bf16[1536,128]{1,0:T(8,128)(2,1)S(1)} collective-permute-done((bf16[1536,128]{1,0:T(8,128)(2,1)}, bf16[1536,128]{1,0:T(8,128)(2,1)S(1)}, u32[]{:S(2)}, u32[]{:S(2)}) %collective-permute-start.4) | collective-permute-done | bytes 393248 | tf_op jit(solution)/shard_map/ppermute | solution.py:22
  138.3 5.2 %shard_map.191 = (bf16[1536,128]{1,0:T(8,128)(2,1)}, bf16[1536,128]{1,0:T(8,128)(2,1)}, bf16[1536,128]{1,0:T(8,128)(2,1)}, bf16[1536,128]{1,0:T(8,128)(2,1)}, bf...) custom-call(bf16[1536,512]{1,0:T(8,128)(2,1)} %get-tuple-element.70., ...), custom_call_target="tpu_custom_call" | custom-call | tf_op jit(solution)/shard_map/pallas_call | solution.py:290
  143.5 2.7 collective-permute-start.9
  146.2 12.7 %all-to-all-start.3 = ((bf16[32,48,512]{2,1,0:T(8,128)(2,1)}), bf16[32,48,512]{2,1,0:T(8,128)(2,1)}, u32[]{:S(2)}, u32[]{:S(2)}) async-start(bf16[32,48,512]{2,1,0:T(8,128)(2,1)} %bitcast.68), calls=%async_computation.3 | async-start | bytes 3145728 | tf_op jit(solution)/shard_map/all_to_all | solution.py:26
  159.0 3.7 %collective-permute-start.22 = (f32[2,256]{1,0:T(2,128)S(1)}, f32[2,256]{1,0:T(2,128)S(1)}, u32[]{:S(2)}, u32[]{:S(2)}) collective-permute-start(f32[2,256]{1,0:T(2,128)S(1)} %slice.53), channel_id=1, source_target_pairs={{0,4},{4,8},{8,12},{12,16},{16,20},{20,24},{24,28},{28,32},{32,36}... | collective-permute-start | bytes 6152 | tf_op jit(solution)/shard_map/ppermute | solution.py:17
  167.0 7.1 %collective-permute-done.7 = bf16[1536,128]{1,0:T(8,128)(2,1)S(1)} collective-permute-done((bf16[1536,128]{1,0:T(8,128)(2,1)}, bf16[1536,128]{1,0:T(8,128)(2,1)S(1)}, u32[]{:S(2)}, u32[]{:S(2)}) %collective-permute-start.7) | collective-permute-done | bytes 393248 | tf_op jit(solution)/shard_map/ppermute | solution.py:22
  176.7 4.4 %all-to-all-done.3 = bf16[32,48,512]{2,1,0:T(8,128)(2,1)} async-done(((bf16[32,48,512]{2,1,0:T(8,128)(2,1)}), bf16[32,48,512]{2,1,0:T(8,128)(2,1)}, u32[]{:S(2)}, u32[]{:S(2)}) %all-to-all-start.3) | async-done | bytes 1572896 | tf_op jit(solution)/shard_map/all_to_all | solution.py:26
  181.1 6.2 %all-to-all-start.2 = ((bf16[32,48,256]{2,1,0:T(8,128)(2,1)}), bf16[32,48,256]{2,1,0:T(8,128)(2,1)}, u32[]{:S(2)}, u32[]{:S(2)}) async-start(bf16[32,48,256]{2,1,0:T(8,128)(2,1)} %bitcast.14), calls=%async_computation.2 | async-start | bytes 1572864 | tf_op jit(solution)/shard_map/all_to_all | solution.py:26
  188.7 11.3 %collective-permute-done.14 = bf16[1536,128]{1,0:T(8,128)(2,1)S(1)} collective-permute-done((bf16[1536,128]{1,0:T(8,128)(2,1)S(1)}, bf16[1536,128]{1,0:T(8,128)(2,1)S(1)}, u32[]{:S(2)}, u32[]{:S(2)}) %collective-permute-start.14) | collective-permute-done | bytes 393248 | tf_op jit(solution)/shard_map/ppermute | solution.py:22
  201.9 8.3 %all-to-all-start.4 = ((bf16[32,48,128]{2,1,0:T(8,128)(2,1)}), bf16[32,48,128]{2,1,0:T(8,128)(2,1)S(1)}, u32[]{:S(2)}, u32[]{:S(2)}) async-start(bf16[32,48,128]{2,1,0:T(8,128)(2,1)} %bitcast.18), calls=%async_computation.4 | async-start | bytes 786432 | tf_op jit(solution)/shard_map/all_to_all | solution.py:26
  213.0 2.7 collective-permute-start.20
  217.9 2.7 collective-permute-start.11
  222.4 10.8 %collective-permute-done.10.refs_1_ = bf16[384,256]{1,0:T(8,128)(2,1)} collective-permute-done((bf16[384,256]{1,0:T(8,128)(2,1)}, bf16[384,256]{1,0:T(8,128)(2,1)}, u32[]{:S(2)}, u32[]{:S(2)}) %collective-permute-start.10) | collective-permute-done | bytes 196640 | tf_op jit(solution)/shard_map/ppermute | solution.py:22
  233.2 2.7 collective-permute-start.17
  237.6 5.9 %convolution_bitcast_fusion = f32[1,256,2048]{2,1,0:T(8,128)} fusion(bf16[1536,256]{1,0:T(8,128)(2,1)S(1)} %get-tuple-element.72, bf16[1536,2048]{1,0:T(8,128)(2,1)} %bitcast.5.cot_ref), kind=kOutput, calls=%fused_computation.16 | convolution fusion | flops 1610612736 | bytes 9175040 | tf_op jit(solution)/shard_map/rf,rd->fd/dot_general | solution.py:392
  244.3 3.7 %collective-permute-done.16.refs_5_ = bf16[384,128]{1,0:T(8,128)(2,1)S(1)} collective-permute-done((bf16[384,128]{1,0:T(8,128)(2,1)S(1)}, bf16[384,128]{1,0:T(8,128)(2,1)S(1)}, u32[]{:S(2)}, u32[]{:S(2)}) %collective-permute-start.16) | collective-permute-done | bytes 98336 | tf_op jit(solution)/shard_map/ppermute | solution.py:22
  248.7 5.0 %shard_map.192 = bf16[384,2048]{1,0:T(8,128)(2,1)} custom-call(s32[1]{0:T(128)} %bitcast.lane_ref, bf16[384,256]{1,0:T(8,128)(2,1)} %convolution_convert_fusion.2.refs_0_, bf16[384,256]{1,0:T(8,128)(2,1)} %collective-permute-done.10.refs_1_, bf16[384,256]{1,0:T(8,128)(2,1)} %collective-permute-done.11.refs_2_, ...), custom_call_target="tpu_custom_call" | custom-call | tf_op jit(solution)/shard_map/pallas_call | solution.py:97
  253.7 3.3 %convolution_convert_fusion = bf16[2048,256]{1,0:T(8,128)(2,1)} fusion(bf16[384,2048]{1,0:T(8,128)(2,1)} %shard_map.192, f32[384,256]{1,0:T(8,128)S(1)} %fusion.8, bf16[384,256]{1,0:T(8,128)(2,1)S(1)} %copy-done.23), kind=kOutput, calls=%fused_computation.17 | convolution fusion | flops 403472384 | bytes 3211264 | tf_op jit(solution)/shard_map/td,tc->dc/dot_general | solution.py:411
  257.0 8.0 %fusion.35 = f32[2048,512]{1,0:T(8,128)} fusion(bf16[1536,2048]{1,0:T(8,128)(2,1)} %copy-done.4, bf16[1536,512]{1,0:T(8,128)(2,1)S(1)} %copy-done.8), kind=kOutput, calls=%fused_computation.84 | convolution fusion | flops 3221225472 | bytes 12058624 | tf_op jit(solution)/shard_map/rd,rf->df/dot_general | solution.py:415
  265.0 8.9 %all-to-all-start.5 = ((bf16[32,64,256]{2,1,0:T(8,128)(2,1)}), bf16[32,64,256]{2,1,0:T(8,128)(2,1)}, u32[]{:S(2)}, u32[]{:S(2)}) async-start(bf16[32,64,256]{2,1,0:T(8,128)(2,1)} %bitcast.72), calls=%async_computation.5 | async-start | bytes 2097152 | tf_op jit(solution)/shard_map/all_to_all | solution.py:26
  279.9 8.0 %collective-permute-done.23 = f32[2,256]{1,0:T(2,128)S(1)} collective-permute-done((f32[2,256]{1,0:T(2,128)S(1)}, f32[2,256]{1,0:T(2,128)S(1)}, u32[]{:S(2)}, u32[]{:S(2)}) %collective-permute-start.23) | collective-permute-done | bytes 2080 | tf_op jit(solution)/shard_map/ppermute | solution.py:17
  (125 shorter events, 50.7 us)
Async XLA Ops:
  0.6 273.3 %copy-start = (bf16[2048,256]{1,0:T(8,128)(2,1)S(1)}, bf16[2048,256]{1,0:T(8,128)(2,1)}, u32[]{:S(2)}) copy-start(bf16[2048,256]{1,0:T(8,128)(2,1)} %param.21) | copy-start | bytes 3145732
  6.2 31.8 %all-to-all-start.1 = ((bf16[32,48,512]{2,1,0:T(8,128)(2,1)}), bf16[32,48,512]{2,1,0:T(8,128)(2,1)S(1)}, u32[]{:S(2)}, u32[]{:S(2)}) async-start(bf16[32,48,512]{2,1,0:T(8,128)(2,1)} %bitcast.69), calls=%async_computation.1 | async-start | bytes 3145728 | tf_op jit(solution)/shard_map/all_to_all | solution.py:26
  39.1 79.9 %all-to-all-start = ((bf16[32,48,2048]{2,1,0:T(8,128)(2,1)}), bf16[32,48,2048]{2,1,0:T(8,128)(2,1)}, u32[]{:S(2)}, u32[]{:S(2)}) async-start(bf16[32,48,2048]{2,1,0:T(8,128)(2,1)} %bitcast.63), calls=%async_computation | async-start | bytes 12582912 | tf_op jit(solution)/shard_map/all_to_all | solution.py:26
  45.7 37.1 %collective-permute-start = (bf16[1536,512]{1,0:T(8,128)(2,1)}, bf16[1536,512]{1,0:T(8,128)(2,1)}, u32[]{:S(2)}, u32[]{:S(2)}) collective-permute-start(bf16[1536,512]{1,0:T(8,128)(2,1)} %bitcast.64), channel_id=1, source_target_pairs={{0,1},{1,2},{2,3},{3,0},{4,5},{5,6},{6,7},{7,4},{8,9},{9,10},{10,1... | collective-permute-start | bytes 4718600 | tf_op jit(solution)/shard_map/ppermute | solution.py:22
  47.0 37.1 %collective-permute-start.1 = (bf16[1536,512]{1,0:T(8,128)(2,1)}, bf16[1536,512]{1,0:T(8,128)(2,1)}, u32[]{:S(2)}, u32[]{:S(2)}) collective-permute-start(bf16[1536,512]{1,0:T(8,128)(2,1)} %bitcast.65), channel_id=1, source_target_pairs={{0,3},{1,0},{2,1},{3,2},{4,7},{5,4},{6,5},{7,6},{8,11},{9,8},{10,9... | collective-permute-start | bytes 4718600 | tf_op jit(solution)/shard_map/ppermute | solution.py:22
  84.0 19.2 %collective-permute-start.2 = (bf16[768,512]{1,0:T(8,128)(2,1)S(1)}, bf16[768,512]{1,0:T(8,128)(2,1)S(1)}, u32[]{:S(2)}, u32[]{:S(2)}) collective-permute-start(bf16[768,512]{1,0:T(8,128)(2,1)S(1)} %slice.51), channel_id=1, source_target_pairs={{0,1},{1,2},{2,3},{3,0},{4,5},{5,6},{6,7},{7,4},{8,9},{9,10},{10,1... | collective-permute-start | bytes 2359304 | tf_op jit(solution)/shard_map/ppermute | solution.py:22
  85.3 18.1 %collective-permute-start.3 = (bf16[768,512]{1,0:T(8,128)(2,1)S(1)}, bf16[768,512]{1,0:T(8,128)(2,1)S(1)}, u32[]{:S(2)}, u32[]{:S(2)}) collective-permute-start(bf16[768,512]{1,0:T(8,128)(2,1)S(1)} %slice.52), channel_id=1, source_target_pairs={{0,3},{1,0},{2,1},{3,2},{4,7},{5,4},{6,5},{7,6},{8,11},{9,8},{10,9... | collective-permute-start | bytes 2359304 | tf_op jit(solution)/shard_map/ppermute | solution.py:22
  129.3 8.0 %collective-permute-start.4 = (bf16[1536,128]{1,0:T(8,128)(2,1)}, bf16[1536,128]{1,0:T(8,128)(2,1)S(1)}, u32[]{:S(2)}, u32[]{:S(2)}) collective-permute-start(bf16[1536,128]{1,0:T(8,128)(2,1)} %get-tuple-element.52), channel_id=1, source_target_pairs={{0,1},{1,2},{2,3},{3,0},{4,5},{5,6},{6,7},{7,4},{8,9},{9,10},{10,1... | collective-permute-start | bytes 1179656 | tf_op jit(solution)/shard_map/ppermute | solution.py:22
  130.6 6.8 %collective-permute-start.5 = (bf16[1536,128]{1,0:T(8,128)(2,1)}, bf16[1536,128]{1,0:T(8,128)(2,1)S(1)}, u32[]{:S(2)}, u32[]{:S(2)}) collective-permute-start(bf16[1536,128]{1,0:T(8,128)(2,1)} %get-tuple-element.53), channel_id=1, source_target_pairs={{0,3},{1,0},{2,1},{3,2},{4,7},{5,4},{6,5},{7,6},{8,11},{9,8},{10,9... | collective-permute-start | bytes 1179656 | tf_op jit(solution)/shard_map/ppermute | solution.py:22
  132.1 32.1 %collective-permute-start.8 = (bf16[1536,128]{1,0:T(8,128)(2,1)}, bf16[1536,128]{1,0:T(8,128)(2,1)S(1)}, u32[]{:S(2)}, u32[]{:S(2)}) collective-permute-start(bf16[1536,128]{1,0:T(8,128)(2,1)} %get-tuple-element.60), channel_id=1, source_target_pairs={{0,1},{1,2},{2,3},{3,0},{4,5},{5,6},{6,7},{7,4},{8,9},{9,10},{10,1... | collective-permute-start | bytes 1179656 | tf_op jit(solution)/shard_map/ppermute | solution.py:22
  143.5 22.1 %collective-permute-start.9 = (bf16[1536,128]{1,0:T(8,128)(2,1)}, bf16[1536,128]{1,0:T(8,128)(2,1)}, u32[]{:S(2)}, u32[]{:S(2)}) collective-permute-start(bf16[1536,128]{1,0:T(8,128)(2,1)} %get-tuple-element.61), channel_id=1, source_target_pairs={{0,3},{1,0},{2,1},{3,2},{4,7},{5,4},{6,5},{7,6},{8,11},{9,8},{10,9... | collective-permute-start | bytes 1179656 | tf_op jit(solution)/shard_map/ppermute | solution.py:22
  146.2 35.0 %all-to-all-start.3 = ((bf16[32,48,512]{2,1,0:T(8,128)(2,1)}), bf16[32,48,512]{2,1,0:T(8,128)(2,1)}, u32[]{:S(2)}, u32[]{:S(2)}) async-start(bf16[32,48,512]{2,1,0:T(8,128)(2,1)} %bitcast.68), calls=%async_computation.3 | async-start | bytes 3145728 | tf_op jit(solution)/shard_map/all_to_all | solution.py:26
  159.0 29.6 %collective-permute-start.22 = (f32[2,256]{1,0:T(2,128)S(1)}, f32[2,256]{1,0:T(2,128)S(1)}, u32[]{:S(2)}, u32[]{:S(2)}) collective-permute-start(f32[2,256]{1,0:T(2,128)S(1)} %slice.53), channel_id=1, source_target_pairs={{0,4},{4,8},{8,12},{12,16},{16,20},{20,24},{24,28},{28,32},{32,36}... | collective-permute-start | bytes 6152 | tf_op jit(solution)/shard_map/ppermute | solution.py:17
  162.6 11.5 %collective-permute-start.7 = (bf16[1536,128]{1,0:T(8,128)(2,1)}, bf16[1536,128]{1,0:T(8,128)(2,1)S(1)}, u32[]{:S(2)}, u32[]{:S(2)}) collective-permute-start(bf16[1536,128]{1,0:T(8,128)(2,1)} %get-tuple-element.58), channel_id=1, source_target_pairs={{0,3},{1,0},{2,1},{3,2},{4,7},{5,4},{6,5},{7,6},{8,11},{9,8},{10,9... | collective-permute-start | bytes 1179656 | tf_op jit(solution)/shard_map/ppermute | solution.py:22
  162.9 12.7 %collective-permute-start.6 = (bf16[1536,128]{1,0:T(8,128)(2,1)}, bf16[1536,128]{1,0:T(8,128)(2,1)S(1)}, u32[]{:S(2)}, u32[]{:S(2)}) collective-permute-start(bf16[1536,128]{1,0:T(8,128)(2,1)} %get-tuple-element.57), channel_id=1, source_target_pairs={{0,1},{1,2},{2,3},{3,0},{4,5},{5,6},{6,7},{7,4},{8,9},{9,10},{10,1... | collective-permute-start | bytes 1179656 | tf_op jit(solution)/shard_map/ppermute | solution.py:22
  164.2 24.5 %collective-permute-start.15 = (bf16[1536,128]{1,0:T(8,128)(2,1)}, bf16[1536,128]{1,0:T(8,128)(2,1)}, u32[]{:S(2)}, u32[]{:S(2)}) collective-permute-start(bf16[1536,128]{1,0:T(8,128)(2,1)} %get-tuple-element.68), channel_id=1, source_target_pairs={{0,3},{1,0},{2,1},{3,2},{4,7},{5,4},{6,5},{7,6},{8,11},{9,8},{10,9... | collective-permute-start | bytes 1179656 | tf_op jit(solution)/shard_map/ppermute | solution.py:22
  165.6 21.7 %collective-permute-start.13 = (bf16[1536,128]{1,0:T(8,128)(2,1)}, bf16[1536,128]{1,0:T(8,128)(2,1)}, u32[]{:S(2)}, u32[]{:S(2)}) collective-permute-start(bf16[1536,128]{1,0:T(8,128)(2,1)} %get-tuple-element.67), channel_id=1, source_target_pairs={{0,1},{1,2},{2,3},{3,0},{4,5},{5,6},{6,7},{7,4},{8,9},{9,10},{10,1... | collective-permute-start | bytes 1179656 | tf_op jit(solution)/shard_map/ppermute | solution.py:22
  181.1 20.8 %all-to-all-start.2 = ((bf16[32,48,256]{2,1,0:T(8,128)(2,1)}), bf16[32,48,256]{2,1,0:T(8,128)(2,1)}, u32[]{:S(2)}, u32[]{:S(2)}) async-start(bf16[32,48,256]{2,1,0:T(8,128)(2,1)} %bitcast.14), calls=%async_computation.2 | async-start | bytes 1572864 | tf_op jit(solution)/shard_map/all_to_all | solution.py:26
  188.4 11.6 %collective-permute-start.14 = (bf16[1536,128]{1,0:T(8,128)(2,1)S(1)}, bf16[1536,128]{1,0:T(8,128)(2,1)S(1)}, u32[]{:S(2)}, u32[]{:S(2)}) collective-permute-start(bf16[1536,128]{1,0:T(8,128)(2,1)S(1)} %add_convert_fusion.1), channel_id=1, source_target_pairs={{0,1},{1,2},{2,3},{3,0},{4,5},{5,6},{6,7},{7,4},{8,9},{9,10},{10,1... | collective-permute-start | bytes 1179656 | tf_op jit(solution)/shard_map/ppermute | solution.py:22
  201.9 18.7 %all-to-all-start.4 = ((bf16[32,48,128]{2,1,0:T(8,128)(2,1)}), bf16[32,48,128]{2,1,0:T(8,128)(2,1)S(1)}, u32[]{:S(2)}, u32[]{:S(2)}) async-start(bf16[32,48,128]{2,1,0:T(8,128)(2,1)} %bitcast.18), calls=%async_computation.4 | async-start | bytes 786432 | tf_op jit(solution)/shard_map/all_to_all | solution.py:26
  212.9 30.6 %copy-start.15 = (bf16[384,512]{1,0:T(8,128)(2,1)}, bf16[384,512]{1,0:T(8,128)(2,1)S(1)}, u32[]{:S(2)}) copy-start(bf16[384,512]{1,0:T(8,128)(2,1)S(1)} %convolution_convert_fusion.1.refs_8_) | copy-start | bytes 1179652
  212.9 22.9 %collective-permute-start.19 = (bf16[384,512]{1,0:T(8,128)(2,1)S(1)}, bf16[384,512]{1,0:T(8,128)(2,1)}, u32[]{:S(2)}, u32[]{:S(2)}) collective-permute-start(bf16[384,512]{1,0:T(8,128)(2,1)S(1)} %convolution_convert_fusion.1.refs_8_), channel_id=1, source_target_pairs={{0,1},{1,2},{2,3},{3,0},{4,5},{5,6},{6,7},{7,4},{8,9},{9,10},{10,1... | collective-permute-start | bytes 1179656 | tf_op jit(solution)/shard_map/ppermute | solution.py:22
  213.0 30.5 %collective-permute-start.20 = (bf16[384,512]{1,0:T(8,128)(2,1)S(1)}, bf16[384,512]{1,0:T(8,128)(2,1)}, u32[]{:S(2)}, u32[]{:S(2)}) collective-permute-start(bf16[384,512]{1,0:T(8,128)(2,1)S(1)} %convolution_convert_fusion.1.refs_8_), channel_id=1, source_target_pairs={{0,3},{1,0},{2,1},{3,2},{4,7},{5,4},{6,5},{7,6},{8,11},{9,8},{10,9... | collective-permute-start | bytes 1179656 | tf_op jit(solution)/shard_map/ppermute | solution.py:22
  217.9 15.2 %collective-permute-start.10 = (bf16[384,256]{1,0:T(8,128)(2,1)}, bf16[384,256]{1,0:T(8,128)(2,1)}, u32[]{:S(2)}, u32[]{:S(2)}) collective-permute-start(bf16[384,256]{1,0:T(8,128)(2,1)} %convolution_convert_fusion.2.refs_0_), channel_id=1, source_target_pairs={{0,1},{1,2},{2,3},{3,0},{4,5},{5,6},{6,7},{7,4},{8,9},{9,10},{10,1... | collective-permute-start | bytes 589832 | tf_op jit(solution)/shard_map/ppermute | solution.py:22
  217.9 15.2 %collective-permute-start.11 = (bf16[384,256]{1,0:T(8,128)(2,1)}, bf16[384,256]{1,0:T(8,128)(2,1)}, u32[]{:S(2)}, u32[]{:S(2)}) collective-permute-start(bf16[384,256]{1,0:T(8,128)(2,1)} %convolution_convert_fusion.2.refs_0_), channel_id=1, source_target_pairs={{0,3},{1,0},{2,1},{3,2},{4,7},{5,4},{6,5},{7,6},{8,11},{9,8},{10,9... | collective-permute-start | bytes 589832 | tf_op jit(solution)/shard_map/ppermute | solution.py:22
  220.6 12.6 %collective-permute-start.12 = (bf16[384,256]{1,0:T(8,128)(2,1)}, bf16[384,256]{1,0:T(8,128)(2,1)}, u32[]{:S(2)}, u32[]{:S(2)}) collective-permute-start(bf16[384,256]{1,0:T(8,128)(2,1)} %convolution_convert_fusion.2.refs_0_), channel_id=1, source_target_pairs={{0,2},{1,3},{2,0},{3,1},{4,6},{5,7},{6,4},{7,5},{8,10},{9,11},{10,... | collective-permute-start | bytes 589832 | tf_op jit(solution)/shard_map/ppermute | solution.py:22
  233.1 11.2 %collective-permute-start.21 = (bf16[384,512]{1,0:T(8,128)(2,1)S(1)}, bf16[384,512]{1,0:T(8,128)(2,1)S(1)}, u32[]{:S(2)}, u32[]{:S(2)}) collective-permute-start(bf16[384,512]{1,0:T(8,128)(2,1)S(1)} %convolution_convert_fusion.1.refs_8_), channel_id=1, source_target_pairs={{0,2},{1,3},{2,0},{3,1},{4,6},{5,7},{6,4},{7,5},{8,10},{9,11},{10,... | collective-permute-start | bytes 1179656 | tf_op jit(solution)/shard_map/ppermute | solution.py:22
  233.2 14.8 %collective-permute-start.16 = (bf16[384,128]{1,0:T(8,128)(2,1)S(1)}, bf16[384,128]{1,0:T(8,128)(2,1)S(1)}, u32[]{:S(2)}, u32[]{:S(2)}) collective-permute-start(bf16[384,128]{1,0:T(8,128)(2,1)S(1)} %convolution_convert_fusion.3.refs_4_), channel_id=1, source_target_pairs={{0,1},{1,2},{2,3},{3,0},{4,5},{5,6},{6,7},{7,4},{8,9},{9,10},{10,1... | collective-permute-start | bytes 294920 | tf_op jit(solution)/shard_map/ppermute | solution.py:22
  233.2 14.8 %collective-permute-start.17 = (bf16[384,128]{1,0:T(8,128)(2,1)S(1)}, bf16[384,128]{1,0:T(8,128)(2,1)S(1)}, u32[]{:S(2)}, u32[]{:S(2)}) collective-permute-start(bf16[384,128]{1,0:T(8,128)(2,1)S(1)} %convolution_convert_fusion.3.refs_4_), channel_id=1, source_target_pairs={{0,3},{1,0},{2,1},{3,2},{4,7},{5,4},{6,5},{7,6},{8,11},{9,8},{10,9... | collective-permute-start | bytes 294920 | tf_op jit(solution)/shard_map/ppermute | solution.py:22
  235.8 12.8 %collective-permute-start.18 = (bf16[384,128]{1,0:T(8,128)(2,1)S(1)}, bf16[384,128]{1,0:T(8,128)(2,1)}, u32[]{:S(2)}, u32[]{:S(2)}) collective-permute-start(bf16[384,128]{1,0:T(8,128)(2,1)S(1)} %convolution_convert_fusion.3.refs_4_), channel_id=1, source_target_pairs={{0,2},{1,3},{2,0},{3,1},{4,6},{5,7},{6,4},{7,5},{8,10},{9,11},{10,... | collective-permute-start | bytes 294920 | tf_op jit(solution)/shard_map/ppermute | solution.py:22
  265.0 26.0 %all-to-all-start.5 = ((bf16[32,64,256]{2,1,0:T(8,128)(2,1)}), bf16[32,64,256]{2,1,0:T(8,128)(2,1)}, u32[]{:S(2)}, u32[]{:S(2)}) async-start(bf16[32,64,256]{2,1,0:T(8,128)(2,1)} %bitcast.72), calls=%async_computation.5 | async-start | bytes 2097152 | tf_op jit(solution)/shard_map/all_to_all | solution.py:26
  275.2 12.7 %collective-permute-start.23 = (f32[2,256]{1,0:T(2,128)S(1)}, f32[2,256]{1,0:T(2,128)S(1)}, u32[]{:S(2)}, u32[]{:S(2)}) collective-permute-start(f32[2,256]{1,0:T(2,128)S(1)} %slice.56), channel_id=1, source_target_pairs={{4,0},{8,4},{12,8},{16,12},{20,16},{24,20},{28,24},{32,28},{36,32}... | collective-permute-start | bytes 6152 | tf_op jit(solution)/shard_map/ppermute | solution.py:17
  (25 other events, 196.3 us)

commit v5 on v4

--- a/solution.py
+++ b/solution.py
@@ -271,11 +271,20 @@
 
 def other_kernel(both_ref, a_far_ref, b_far_ref, mat_ref, *refs):
     part = lax.dot_general(both_ref[...], mat_ref[...], along_last, preferred_element_type=f32)
+    at = 0
     for i, ref in enumerate(refs):
-        piece = part[:, i * direct_width : (i + 1) * direct_width]
+        piece = part[:, at : at + ref.shape[1]]
+        at += ref.shape[1]
         if i < 2:
             piece = piece + (a_far_ref, b_far_ref)[i][...].astype(f32)
         ref[...] = piece.astype(bf16)
+
+
+def wide_kernel(own_ref, a_prev_ref, a_next_ref, b_prev_ref, b_next_ref, out_ref):
+    for at, refs in ((0, (a_prev_ref, a_next_ref)), (direct_width, (b_prev_ref, b_next_ref))):
+        columns = slice(at, at + direct_width)
+        total = own_ref[:, columns].astype(f32) + refs[0][...].astype(f32)
+        out_ref[:, columns] = (total + refs[1][...].astype(f32)).astype(bf16)
 
 
 part_block = 512
@@ -381,8 +390,9 @@
     direct = back(direct)
     a_next = turned(a_behind, -1)
     b_prev = turned(b_ahead, 1)
-    a_ahead, b_behind, c_behind, c_far, a_own, b_own, c_own, c_ahead = by_rows(
-        other_kernel, (dboth, a_far, b_far), (other_mat,), [direct_width] * 8
+    sizes = [direct_width] * 4 + [2 * direct_width] + [direct_width] * 2
+    a_ahead, b_behind, c_behind, c_far, wide_own, c_own, c_ahead = by_rows(
+        other_kernel, (dboth, a_far, b_far), (other_mat,), sizes
     )
     a_prev = turned(a_ahead, 1)
     b_next = turned(b_behind, -1)
@@ -390,7 +400,9 @@
     c_next = turned(c_behind, -1)
     c_ahead, direct = lax.optimization_barrier((c_ahead, direct))
     grad_down = jnp.einsum("rf,rd->fd", hidden, entry_cots, preferred_element_type=f32)
-    wide = jnp.concatenate([plus(a_own, a_prev, a_next), plus(b_own, b_prev, b_next)], axis=1)
+    (wide,) = by_rows(
+        wide_kernel, (wide_own, a_prev, a_next, b_prev, b_next), (), [2 * direct_width]
+    )
     c_own, wide = lax.optimization_barrier((c_own, wide))
     wide = back(wide)
     direct_parts = lane_gather(per_token(direct))

time: 294 us -> 294 us (level)
  waiting for transfers between devices: 121 us -> 105 us
  starting transfers between devices: 82.1 us -> 96.3 us
  Pallas kernels: 33.8 us -> 37.3 us
    ppermute x22, waiting for transfers between devices: 83.4 us -> 72.1 us  [turned(): lax.ppermute(array, 'tp', [(i, (i + by) % size) for i in range(size)])]
    ppermute x22, starting transfers between devices: 23.9 us -> 33.9 us  [turned(): lax.ppermute(array, 'tp', [(i, (i + by) % size) for i in range(size)])]
    all_to_all x6, waiting for transfers between devices: 29.7 us -> 25.3 us  [exchanged(): return lax.all_to_all(array, 'sp', split_axis=0, concat_axis=0, tiled=True)]
    pallas_call x2 -> x3, Pallas kernels: 15.5 us -> 19 us  [by_rows(): pl.pallas_call(kernel, grid=(slots // part_block,), in_specs=[rows(x.shap...]
  transfers between devices with their start and end apart: 30 -> 30, of which waited for: 14 -> 10; matrix products, arithmetic and copies ran while one was open for 13% -> 12% of each run, Pallas kernels for 4% -> 6%
where the time goes in v5:
time: 294 us; the launch traced here: 292 us
  waiting for transfers between devices  105 us (36%)
  starting transfers between devices  96.3 us (33%)
  Pallas kernels  37.3 us (13%)
  matrix products  30.6 us (10%)
  local copies, waits for them, and re-layouts  13.8 us (5%)
  other arithmetic  7.94 us (3%)
    ppermute x22, waiting for transfers between devices, turned(): lax.ppermute(array, 'tp', [(i, (i + by) % size) for i in range(size)])  72.1 us
    all_to_all x6, starting transfers between devices, exchanged(): return lax.all_to_all(array, 'sp', split_axis=0, concat_axis=0, tiled=True)  54.4 us
    ppermute x22, starting transfers between devices, turned(): lax.ppermute(array, 'tp', [(i, (i + by) % size) for i in range(size)])  33.9 us
    all_to_all x6, waiting for transfers between devices, exchanged(): return lax.all_to_all(array, 'sp', split_axis=0, concat_axis=0, tiled=True)  25.3 us
    pallas_call x3, Pallas kernels, by_rows(): pl.pallas_call(kernel, grid=(slots // part_block,), in_specs=[rows(x.shap...  19 us
    ppermute x2, starting transfers between devices, passed_along(): return lax.ppermute(array, axis, pairs)  8.07 us
    dot_general x1, matrix products, on_device(): jnp.einsum('rd,rf->df', entry_rows, late_both, preferred_element_type=f32)  8.03 us
    ppermute x2, waiting for transfers between devices, passed_along(): return lax.ppermute(array, axis, pairs)  8.01 us
  transfers between devices with their start and end apart: 30, of which 10 were waited for; matrix products, arithmetic and copies ran while one was open for 12% of the time, Pallas kernels for 6%

profile of v5, /device:TPU:1, one launch (start us, length us, event | category | flops | bytes accessed | tf_op | source)
XLA Modules:
  0.0 292.3 jit_solution(4248866180433342859)
XLA Ops:
  0.7 5.5 %shard_map.188 = (bf16[1536,512]{1,0:T(8,128)(2,1)}, bf16[1536,384]{1,0:T(8,128)(2,1)}, bf16[384,32]{1,0:T(8,128)(2,1)}, bf16[32,384]{1,0:T(8,128)(2,1)}, bf16[32,384]{1,0:T(8,128)(2,1)}) custom-call(s32[1]{0:T(128)} %bitcast.lane_ref, s32[2,384]{1,0:T(2,128)} %bitcast.82, f32[2,384]{1,0:T(2,128)} %bitcast.83, bf16[384,2048]{1,0:T(8,128)(2,1)} %refs_13_.1, ...), custom_call_target="tpu_custom_call" | custom-call | tf_op jit(solution)/shard_map/pallas_call | solution.py:181
  6.2 9.6 %all-to-all-start.1 = ((bf16[32,48,512]{2,1,0:T(8,128)(2,1)}), bf16[32,48,512]{2,1,0:T(8,128)(2,1)S(1)}, u32[]{:S(2)}, u32[]{:S(2)}) async-start(bf16[32,48,512]{2,1,0:T(8,128)(2,1)} %bitcast.70), calls=%async_computation.1 | async-start | bytes 3145728 | tf_op jit(solution)/shard_map/all_to_all | solution.py:26
  15.8 7.8 %shard_map.189 = (bf16[1536,2048]{1,0:T(8,128)(2,1)}, bf16[384,1536]{1,0:T(8,128)(2,1)}) custom-call(bf16[1536,384]{1,0:T(8,128)(2,1)} %get-tuple-element.40.chooser_ref, bf16[384,2048]{1,0:T(8,128)(2,1)} %refs_12_.1, bf16[384,32]{1,0:T(8,128)(2,1)} %get-tuple-element.41.rank_ref, bf16[32,384]{1,0:T(8,128)(2,1)} %get-tuple-element.42.high_ref, ...), custom_call_target="tpu_custom_call" | custom-call | tf_op jit(solution)/shard_map/pallas_call | solution.py:236
  23.5 14.4 %all-to-all-done.1 = bf16[32,48,512]{2,1,0:T(8,128)(2,1)S(1)} async-done(((bf16[32,48,512]{2,1,0:T(8,128)(2,1)}), bf16[32,48,512]{2,1,0:T(8,128)(2,1)S(1)}, u32[]{:S(2)}, u32[]{:S(2)}) %all-to-all-start.1) | async-done | bytes 1572896 | tf_op jit(solution)/shard_map/all_to_all | solution.py:26
  39.1 6.6 %all-to-all-start = ((bf16[32,48,2048]{2,1,0:T(8,128)(2,1)}), bf16[32,48,2048]{2,1,0:T(8,128)(2,1)}, u32[]{:S(2)}, u32[]{:S(2)}) async-start(bf16[32,48,2048]{2,1,0:T(8,128)(2,1)} %bitcast.63), calls=%async_computation | async-start | bytes 12582912 | tf_op jit(solution)/shard_map/all_to_all | solution.py:26
  50.7 32.1 %collective-permute-done = bf16[1536,512]{1,0:T(8,128)(2,1)} collective-permute-done((bf16[1536,512]{1,0:T(8,128)(2,1)}, bf16[1536,512]{1,0:T(8,128)(2,1)}, u32[]{:S(2)}, u32[]{:S(2)}) %collective-permute-start) | collective-permute-done | bytes 1572896 | tf_op jit(solution)/shard_map/ppermute | solution.py:22
  85.3 2.7 collective-permute-start.3
  92.5 10.8 %collective-permute-done.2 = bf16[768,512]{1,0:T(8,128)(2,1)S(1)} collective-permute-done((bf16[768,512]{1,0:T(8,128)(2,1)S(1)}, bf16[768,512]{1,0:T(8,128)(2,1)S(1)}, u32[]{:S(2)}, u32[]{:S(2)}) %collective-permute-start.2) | collective-permute-done | bytes 786464 | tf_op jit(solution)/shard_map/ppermute | solution.py:22
  106.1 3.6 %multiply_convert_fusion = (bf16[1536,256]{1,0:T(8,128)(2,1)S(1)}, bf16[1536,256]{1,0:T(8,128)(2,1)}, bf16[1536,256]{1,0:T(8,128)(2,1)}) fusion(f32[1536,256]{1,0:T(8,128)S(1)} %fusion.31, bf16[1536,2048]{1,0:T(8,128)(2,1)S(1)} %constant_dynamic-update-slice_fusion.4, bf16[1,2048,256]{2,1,0:T(8,128)(2,1)S(1)} %copy-done.2), kind=kOutput, calls=%fused_computation.21 | convolution fusion | flops 1615724544 | bytes 11272192 | tf_op jit(solution)/shard_map/dot_general | solution.py:347
  109.7 9.3 %all-to-all-done = bf16[32,48,2048]{2,1,0:T(8,128)(2,1)} async-done(((bf16[32,48,2048]{2,1,0:T(8,128)(2,1)}), bf16[32,48,2048]{2,1,0:T(8,128)(2,1)}, u32[]{:S(2)}, u32[]{:S(2)}) %all-to-all-start) | async-done | bytes 6291488 | tf_op jit(solution)/shard_map/all_to_all | solution.py:26
  119.0 10.3 %shard_map.190 = (bf16[1536,512]{1,0:T(8,128)(2,1)}, bf16[1536,128]{1,0:T(8,128)(2,1)}, bf16[1536,128]{1,0:T(8,128)(2,1)}, bf16[1536,128]{1,0:T(8,128)(2,1)}, bf...) custom-call(bf16[1536,2048]{1,0:T(8,128)(2,1)} %bitcast.5.cot_ref, bf16[1536,256]{1,0:T(8,128)(2,1)} %get-tuple-element.47.act_ref, ...), custom_call_target="tpu_custom_call" | custom-call | tf_op jit(solution)/shard_map/pallas_call | solution.py:299
  129.3 9.4 %all-to-all-start.3 = ((bf16[32,48,512]{2,1,0:T(8,128)(2,1)}), bf16[32,48,512]{2,1,0:T(8,128)(2,1)}, u32[]{:S(2)}, u32[]{:S(2)}) async-start(bf16[32,48,512]{2,1,0:T(8,128)(2,1)} %bitcast.69), calls=%async_computation.3 | async-start | bytes 3145728 | tf_op jit(solution)/shard_map/all_to_all | solution.py:26
  143.0 7.6 %collective-permute-done.4.a_far_ref = bf16[1536,128]{1,0:T(8,128)(2,1)S(1)} collective-permute-done((bf16[1536,128]{1,0:T(8,128)(2,1)}, bf16[1536,128]{1,0:T(8,128)(2,1)S(1)}, u32[]{:S(2)}, u32[]{:S(2)}) %collective-permute-start.4) | collective-permute-done | bytes 393248 | tf_op jit(solution)/shard_map/ppermute | solution.py:22
  151.4 5.2 %shard_map.191 = (bf16[1536,128]{1,0:T(8,128)(2,1)}, bf16[1536,128]{1,0:T(8,128)(2,1)}, bf16[1536,128]{1,0:T(8,128)(2,1)}, bf16[1536,128]{1,0:T(8,128)(2,1)}, bf...) custom-call(bf16[1536,512]{1,0:T(8,128)(2,1)} %get-tuple-element.68.both_ref, ...), custom_call_target="tpu_custom_call" | custom-call | tf_op jit(solution)/shard_map/pallas_call | solution.py:299
  159.5 5.7 %collective-permute-start.22 = (f32[2,256]{1,0:T(2,128)S(1)}, f32[2,256]{1,0:T(2,128)S(1)}, u32[]{:S(2)}, u32[]{:S(2)}) collective-permute-start(f32[2,256]{1,0:T(2,128)S(1)} %slice.53), channel_id=1, source_target_pairs={{0,4},{4,8},{8,12},{12,16},{16,20},{20,24},{24,28},{28,32},{32,36}... | collective-permute-start | bytes 6152 | tf_op jit(solution)/shard_map/ppermute | solution.py:17
  165.2 3.0 %collective-permute-start.15 = (bf16[1536,128]{1,0:T(8,128)(2,1)}, bf16[1536,128]{1,0:T(8,128)(2,1)}, u32[]{:S(2)}, u32[]{:S(2)}) collective-permute-start(bf16[1536,128]{1,0:T(8,128)(2,1)} %get-tuple-element.66), channel_id=1, source_target_pairs={{0,3},{1,0},{2,1},{3,2},{4,7},{5,4},{6,5},{7,6},{8,11},{9,8},{10,9... | collective-permute-start | bytes 1179656 | tf_op jit(solution)/shard_map/ppermute | solution.py:22
  168.2 3.5 %shard_map.192 = bf16[1536,256]{1,0:T(8,128)(2,1)} custom-call(bf16[1536,256]{1,0:T(8,128)(2,1)} %get-tuple-element.55.own_ref, bf16[1536,128]{1,0:T(8,128)(2,1)} %collective-permute-done.6.a_prev_ref, bf16[1536,128]{1,0:T(8,128)(2,1)} %copy-done.17, bf16[1536,128]{1,0:T(8,128)(2,1)} %collective-permute-done.8.b_prev_ref, ...), custom_call_target="tpu_custom_call" | custom-call | tf_op jit(solution)/shard_map/pallas_call | solution.py:299
  171.7 11.3 %all-to-all-start.2 = ((bf16[32,48,256]{2,1,0:T(8,128)(2,1)}), bf16[32,48,256]{2,1,0:T(8,128)(2,1)}, u32[]{:S(2)}, u32[]{:S(2)}) async-start(bf16[32,48,256]{2,1,0:T(8,128)(2,1)} %bitcast.67), calls=%async_computation.2 | async-start | bytes 1572864 | tf_op jit(solution)/shard_map/all_to_all | solution.py:26
  184.7 11.2 %collective-permute-done.14 = bf16[1536,128]{1,0:T(8,128)(2,1)S(1)} collective-permute-done((bf16[1536,128]{1,0:T(8,128)(2,1)S(1)}, bf16[1536,128]{1,0:T(8,128)(2,1)S(1)}, u32[]{:S(2)}, u32[]{:S(2)}) %collective-permute-start.14) | collective-permute-done | bytes 393248 | tf_op jit(solution)/shard_map/ppermute | solution.py:22
  197.8 8.0 %all-to-all-start.4 = ((bf16[32,48,128]{2,1,0:T(8,128)(2,1)}), bf16[32,48,128]{2,1,0:T(8,128)(2,1)S(1)}, u32[]{:S(2)}, u32[]{:S(2)}) async-start(bf16[32,48,128]{2,1,0:T(8,128)(2,1)} %bitcast.18), calls=%async_computation.4 | async-start | bytes 786432 | tf_op jit(solution)/shard_map/all_to_all | solution.py:26
  205.9 2.6 convolution_convert_fusion.1.refs_8_
  208.6 2.7 collective-permute-start.20
  213.5 2.7 collective-permute-start.11
  218.0 6.8 %collective-permute-done.10.refs_1_ = bf16[384,256]{1,0:T(8,128)(2,1)} collective-permute-done((bf16[384,256]{1,0:T(8,128)(2,1)}, bf16[384,256]{1,0:T(8,128)(2,1)}, u32[]{:S(2)}, u32[]{:S(2)}) %collective-permute-start.10) | collective-permute-done | bytes 196640 | tf_op jit(solution)/shard_map/ppermute | solution.py:22
  225.1 3.4 %collective-permute-done.12.refs_3_ = bf16[384,256]{1,0:T(8,128)(2,1)} collective-permute-done((bf16[384,256]{1,0:T(8,128)(2,1)}, bf16[384,256]{1,0:T(8,128)(2,1)}, u32[]{:S(2)}, u32[]{:S(2)}) %collective-permute-start.12) | collective-permute-done | bytes 196640 | tf_op jit(solution)/shard_map/ppermute | solution.py:22
  228.5 10.8 %collective-permute-start.17 = (bf16[384,128]{1,0:T(8,128)(2,1)S(1)}, bf16[384,128]{1,0:T(8,128)(2,1)S(1)}, u32[]{:S(2)}, u32[]{:S(2)}) collective-permute-start(bf16[384,128]{1,0:T(8,128)(2,1)S(1)} %convolution_convert_fusion.3.refs_4_), channel_id=1, source_target_pairs={{0,3},{1,0},{2,1},{3,2},{4,7},{5,4},{6,5},{7,6},{8,11},{9,8},{10,9... | collective-permute-start | bytes 294920 | tf_op jit(solution)/shard_map/ppermute | solution.py:22
  240.8 5.9 %convolution_bitcast_fusion = f32[1,256,2048]{2,1,0:T(8,128)} fusion(bf16[1536,256]{1,0:T(8,128)(2,1)S(1)} %get-tuple-element.70, bf16[1536,2048]{1,0:T(8,128)(2,1)} %bitcast.5.cot_ref), kind=kOutput, calls=%fused_computation.16 | convolution fusion | flops 1610612736 | bytes 9175040 | tf_op jit(solution)/shard_map/rf,rd->fd/dot_general | solution.py:402
  247.5 5.0 %shard_map.193 = bf16[384,2048]{1,0:T(8,128)(2,1)} custom-call(s32[1]{0:T(128)} %bitcast.lane_ref, bf16[384,256]{1,0:T(8,128)(2,1)} %convolution_convert_fusion.2.refs_0_, bf16[384,256]{1,0:T(8,128)(2,1)} %collective-permute-done.10.refs_1_, bf16[384,256]{1,0:T(8,128)(2,1)} %collective-permute-done.11.refs_2_, ...), custom_call_target="tpu_custom_call" | custom-call | tf_op jit(solution)/shard_map/pallas_call | solution.py:97
  252.5 3.3 %convolution_convert_fusion = bf16[2048,256]{1,0:T(8,128)(2,1)} fusion(bf16[384,2048]{1,0:T(8,128)(2,1)} %shard_map.193, f32[384,256]{1,0:T(8,128)S(1)} %fusion.8, bf16[384,256]{1,0:T(8,128)(2,1)S(1)} %copy-done.21), kind=kOutput, calls=%fused_computation.17 | convolution fusion | flops 403472384 | bytes 3211264 | tf_op jit(solution)/shard_map/td,tc->dc/dot_general | solution.py:423
  255.8 8.0 %fusion.35 = f32[2048,512]{1,0:T(8,128)} fusion(bf16[1536,2048]{1,0:T(8,128)(2,1)} %copy-done.4, bf16[1536,512]{1,0:T(8,128)(2,1)S(1)} %copy-done.8), kind=kOutput, calls=%fused_computation.81 | convolution fusion | flops 3221225472 | bytes 12058624 | tf_op jit(solution)/shard_map/rd,rf->df/dot_general | solution.py:427
  263.8 9.4 %all-to-all-start.5 = ((bf16[32,64,256]{2,1,0:T(8,128)(2,1)}), bf16[32,64,256]{2,1,0:T(8,128)(2,1)}, u32[]{:S(2)}, u32[]{:S(2)}) async-start(bf16[32,64,256]{2,1,0:T(8,128)(2,1)} %bitcast.73), calls=%async_computation.5 | async-start | bytes 2097152 | tf_op jit(solution)/shard_map/all_to_all | solution.py:26
  279.2 8.0 %collective-permute-done.23 = f32[2,256]{1,0:T(2,128)S(1)} collective-permute-done((f32[2,256]{1,0:T(2,128)S(1)}, f32[2,256]{1,0:T(2,128)S(1)}, u32[]{:S(2)}, u32[]{:S(2)}) %collective-permute-start.23) | collective-permute-done | bytes 2080 | tf_op jit(solution)/shard_map/ppermute | solution.py:17
  (119 shorter events, 44.9 us)
Async XLA Ops:
  0.6 272.6 %copy-start = (bf16[2048,256]{1,0:T(8,128)(2,1)S(1)}, bf16[2048,256]{1,0:T(8,128)(2,1)}, u32[]{:S(2)}) copy-start(bf16[2048,256]{1,0:T(8,128)(2,1)} %param.21) | copy-start | bytes 3145732
  6.2 31.8 %all-to-all-start.1 = ((bf16[32,48,512]{2,1,0:T(8,128)(2,1)}), bf16[32,48,512]{2,1,0:T(8,128)(2,1)S(1)}, u32[]{:S(2)}, u32[]{:S(2)}) async-start(bf16[32,48,512]{2,1,0:T(8,128)(2,1)} %bitcast.70), calls=%async_computation.1 | async-start | bytes 3145728 | tf_op jit(solution)/shard_map/all_to_all | solution.py:26
  39.1 79.9 %all-to-all-start = ((bf16[32,48,2048]{2,1,0:T(8,128)(2,1)}), bf16[32,48,2048]{2,1,0:T(8,128)(2,1)}, u32[]{:S(2)}, u32[]{:S(2)}) async-start(bf16[32,48,2048]{2,1,0:T(8,128)(2,1)} %bitcast.63), calls=%async_computation | async-start | bytes 12582912 | tf_op jit(solution)/shard_map/all_to_all | solution.py:26
  45.7 37.1 %collective-permute-start = (bf16[1536,512]{1,0:T(8,128)(2,1)}, bf16[1536,512]{1,0:T(8,128)(2,1)}, u32[]{:S(2)}, u32[]{:S(2)}) collective-permute-start(bf16[1536,512]{1,0:T(8,128)(2,1)} %bitcast.64), channel_id=1, source_target_pairs={{0,1},{1,2},{2,3},{3,0},{4,5},{5,6},{6,7},{7,4},{8,9},{9,10},{10,1... | collective-permute-start | bytes 4718600 | tf_op jit(solution)/shard_map/ppermute | solution.py:22
  47.0 37.1 %collective-permute-start.1 = (bf16[1536,512]{1,0:T(8,128)(2,1)}, bf16[1536,512]{1,0:T(8,128)(2,1)}, u32[]{:S(2)}, u32[]{:S(2)}) collective-permute-start(bf16[1536,512]{1,0:T(8,128)(2,1)} %bitcast.65), channel_id=1, source_target_pairs={{0,3},{1,0},{2,1},{3,2},{4,7},{5,4},{6,5},{7,6},{8,11},{9,8},{10,9... | collective-permute-start | bytes 4718600 | tf_op jit(solution)/shard_map/ppermute | solution.py:22
  84.0 19.2 %collective-permute-start.2 = (bf16[768,512]{1,0:T(8,128)(2,1)S(1)}, bf16[768,512]{1,0:T(8,128)(2,1)S(1)}, u32[]{:S(2)}, u32[]{:S(2)}) collective-permute-start(bf16[768,512]{1,0:T(8,128)(2,1)S(1)} %slice.51), channel_id=1, source_target_pairs={{0,1},{1,2},{2,3},{3,0},{4,5},{5,6},{6,7},{7,4},{8,9},{9,10},{10,1... | collective-permute-start | bytes 2359304 | tf_op jit(solution)/shard_map/ppermute | solution.py:22
  85.3 18.1 %collective-permute-start.3 = (bf16[768,512]{1,0:T(8,128)(2,1)S(1)}, bf16[768,512]{1,0:T(8,128)(2,1)S(1)}, u32[]{:S(2)}, u32[]{:S(2)}) collective-permute-start(bf16[768,512]{1,0:T(8,128)(2,1)S(1)} %slice.52), channel_id=1, source_target_pairs={{0,3},{1,0},{2,1},{3,2},{4,7},{5,4},{6,5},{7,6},{8,11},{9,8},{10,9... | collective-permute-start | bytes 2359304 | tf_op jit(solution)/shard_map/ppermute | solution.py:22
  129.3 42.4 %all-to-all-start.3 = ((bf16[32,48,512]{2,1,0:T(8,128)(2,1)}), bf16[32,48,512]{2,1,0:T(8,128)(2,1)}, u32[]{:S(2)}, u32[]{:S(2)}) async-start(bf16[32,48,512]{2,1,0:T(8,128)(2,1)} %bitcast.69), calls=%async_computation.3 | async-start | bytes 3145728 | tf_op jit(solution)/shard_map/all_to_all | solution.py:26
  138.8 11.9 %collective-permute-start.4 = (bf16[1536,128]{1,0:T(8,128)(2,1)}, bf16[1536,128]{1,0:T(8,128)(2,1)S(1)}, u32[]{:S(2)}, u32[]{:S(2)}) collective-permute-start(bf16[1536,128]{1,0:T(8,128)(2,1)} %get-tuple-element.51), channel_id=1, source_target_pairs={{0,1},{1,2},{2,3},{3,0},{4,5},{5,6},{6,7},{7,4},{8,9},{9,10},{10,1... | collective-permute-start | bytes 1179656 | tf_op jit(solution)/shard_map/ppermute | solution.py:22
  140.1 10.6 %collective-permute-start.5 = (bf16[1536,128]{1,0:T(8,128)(2,1)}, bf16[1536,128]{1,0:T(8,128)(2,1)}, u32[]{:S(2)}, u32[]{:S(2)}) collective-permute-start(bf16[1536,128]{1,0:T(8,128)(2,1)} %get-tuple-element.52), channel_id=1, source_target_pairs={{0,3},{1,0},{2,1},{3,2},{4,7},{5,4},{6,5},{7,6},{8,11},{9,8},{10,9... | collective-permute-start | bytes 1179656 | tf_op jit(solution)/shard_map/ppermute | solution.py:22
  141.6 17.9 %collective-permute-start.7 = (bf16[1536,128]{1,0:T(8,128)(2,1)}, bf16[1536,128]{1,0:T(8,128)(2,1)S(1)}, u32[]{:S(2)}, u32[]{:S(2)}) collective-permute-start(bf16[1536,128]{1,0:T(8,128)(2,1)} %get-tuple-element.57), channel_id=1, source_target_pairs={{0,3},{1,0},{2,1},{3,2},{4,7},{5,4},{6,5},{7,6},{8,11},{9,8},{10,9... | collective-permute-start | bytes 1179656 | tf_op jit(solution)/shard_map/ppermute | solution.py:22
  142.8 22.4 %collective-permute-start.8 = (bf16[1536,128]{1,0:T(8,128)(2,1)}, bf16[1536,128]{1,0:T(8,128)(2,1)}, u32[]{:S(2)}, u32[]{:S(2)}) collective-permute-start(bf16[1536,128]{1,0:T(8,128)(2,1)} %get-tuple-element.58), channel_id=1, source_target_pairs={{0,1},{1,2},{2,3},{3,0},{4,5},{5,6},{6,7},{7,4},{8,9},{9,10},{10,1... | collective-permute-start | bytes 1179656 | tf_op jit(solution)/shard_map/ppermute | solution.py:22
  156.6 11.6 %collective-permute-start.6 = (bf16[1536,128]{1,0:T(8,128)(2,1)}, bf16[1536,128]{1,0:T(8,128)(2,1)}, u32[]{:S(2)}, u32[]{:S(2)}) collective-permute-start(bf16[1536,128]{1,0:T(8,128)(2,1)} %get-tuple-element.56), channel_id=1, source_target_pairs={{0,1},{1,2},{2,3},{3,0},{4,5},{5,6},{6,7},{7,4},{8,9},{9,10},{10,1... | collective-permute-start | bytes 1179656 | tf_op jit(solution)/shard_map/ppermute | solution.py:22
  156.9 11.4 %collective-permute-start.9 = (bf16[1536,128]{1,0:T(8,128)(2,1)}, bf16[1536,128]{1,0:T(8,128)(2,1)}, u32[]{:S(2)}, u32[]{:S(2)}) collective-permute-start(bf16[1536,128]{1,0:T(8,128)(2,1)} %get-tuple-element.59), channel_id=1, source_target_pairs={{0,3},{1,0},{2,1},{3,2},{4,7},{5,4},{6,5},{7,6},{8,11},{9,8},{10,9... | collective-permute-start | bytes 1179656 | tf_op jit(solution)/shard_map/ppermute | solution.py:22
  159.4 23.6 %collective-permute-start.13 = (bf16[1536,128]{1,0:T(8,128)(2,1)}, bf16[1536,128]{1,0:T(8,128)(2,1)}, u32[]{:S(2)}, u32[]{:S(2)}) collective-permute-start(bf16[1536,128]{1,0:T(8,128)(2,1)} %get-tuple-element.65), channel_id=1, source_target_pairs={{0,1},{1,2},{2,3},{3,0},{4,5},{5,6},{6,7},{7,4},{8,9},{9,10},{10,1... | collective-permute-start | bytes 1179656 | tf_op jit(solution)/shard_map/ppermute | solution.py:22
  159.5 25.1 %collective-permute-start.22 = (f32[2,256]{1,0:T(2,128)S(1)}, f32[2,256]{1,0:T(2,128)S(1)}, u32[]{:S(2)}, u32[]{:S(2)}) collective-permute-start(f32[2,256]{1,0:T(2,128)S(1)} %slice.53), channel_id=1, source_target_pairs={{0,4},{4,8},{8,12},{12,16},{16,20},{20,24},{24,28},{28,32},{32,36}... | collective-permute-start | bytes 6152 | tf_op jit(solution)/shard_map/ppermute | solution.py:17
  165.2 19.4 %collective-permute-start.15 = (bf16[1536,128]{1,0:T(8,128)(2,1)}, bf16[1536,128]{1,0:T(8,128)(2,1)}, u32[]{:S(2)}, u32[]{:S(2)}) collective-permute-start(bf16[1536,128]{1,0:T(8,128)(2,1)} %get-tuple-element.66), channel_id=1, source_target_pairs={{0,3},{1,0},{2,1},{3,2},{4,7},{5,4},{6,5},{7,6},{8,11},{9,8},{10,9... | collective-permute-start | bytes 1179656 | tf_op jit(solution)/shard_map/ppermute | solution.py:22
  171.7 26.1 %all-to-all-start.2 = ((bf16[32,48,256]{2,1,0:T(8,128)(2,1)}), bf16[32,48,256]{2,1,0:T(8,128)(2,1)}, u32[]{:S(2)}, u32[]{:S(2)}) async-start(bf16[32,48,256]{2,1,0:T(8,128)(2,1)} %bitcast.67), calls=%async_computation.2 | async-start | bytes 1572864 | tf_op jit(solution)/shard_map/all_to_all | solution.py:26
  184.1 11.8 %collective-permute-start.14 = (bf16[1536,128]{1,0:T(8,128)(2,1)S(1)}, bf16[1536,128]{1,0:T(8,128)(2,1)S(1)}, u32[]{:S(2)}, u32[]{:S(2)}) collective-permute-start(bf16[1536,128]{1,0:T(8,128)(2,1)S(1)} %add_convert_fusion.1), channel_id=1, source_target_pairs={{0,1},{1,2},{2,3},{3,0},{4,5},{5,6},{6,7},{7,4},{8,9},{9,10},{10,1... | collective-permute-start | bytes 1179656 | tf_op jit(solution)/shard_map/ppermute | solution.py:22
  197.8 18.4 %all-to-all-start.4 = ((bf16[32,48,128]{2,1,0:T(8,128)(2,1)}), bf16[32,48,128]{2,1,0:T(8,128)(2,1)S(1)}, u32[]{:S(2)}, u32[]{:S(2)}) async-start(bf16[32,48,128]{2,1,0:T(8,128)(2,1)} %bitcast.18), calls=%async_computation.4 | async-start | bytes 786432 | tf_op jit(solution)/shard_map/all_to_all | solution.py:26
  208.5 38.2 %copy-start.15 = (bf16[384,512]{1,0:T(8,128)(2,1)}, bf16[384,512]{1,0:T(8,128)(2,1)S(1)}, u32[]{:S(2)}) copy-start(bf16[384,512]{1,0:T(8,128)(2,1)S(1)} %convolution_convert_fusion.1.refs_8_) | copy-start | bytes 1179652
  208.5 30.8 %collective-permute-start.19 = (bf16[384,512]{1,0:T(8,128)(2,1)S(1)}, bf16[384,512]{1,0:T(8,128)(2,1)}, u32[]{:S(2)}, u32[]{:S(2)}) collective-permute-start(bf16[384,512]{1,0:T(8,128)(2,1)S(1)} %convolution_convert_fusion.1.refs_8_), channel_id=1, source_target_pairs={{0,1},{1,2},{2,3},{3,0},{4,5},{5,6},{6,7},{7,4},{8,9},{9,10},{10,1... | collective-permute-start | bytes 1179656 | tf_op jit(solution)/shard_map/ppermute | solution.py:22
  208.6 38.1 %collective-permute-start.20 = (bf16[384,512]{1,0:T(8,128)(2,1)S(1)}, bf16[384,512]{1,0:T(8,128)(2,1)}, u32[]{:S(2)}, u32[]{:S(2)}) collective-permute-start(bf16[384,512]{1,0:T(8,128)(2,1)S(1)} %convolution_convert_fusion.1.refs_8_), channel_id=1, source_target_pairs={{0,3},{1,0},{2,1},{3,2},{4,7},{5,4},{6,5},{7,6},{8,11},{9,8},{10,9... | collective-permute-start | bytes 1179656 | tf_op jit(solution)/shard_map/ppermute | solution.py:22
  213.5 11.3 %collective-permute-start.10 = (bf16[384,256]{1,0:T(8,128)(2,1)}, bf16[384,256]{1,0:T(8,128)(2,1)}, u32[]{:S(2)}, u32[]{:S(2)}) collective-permute-start(bf16[384,256]{1,0:T(8,128)(2,1)} %convolution_convert_fusion.2.refs_0_), channel_id=1, source_target_pairs={{0,1},{1,2},{2,3},{3,0},{4,5},{5,6},{6,7},{7,4},{8,9},{9,10},{10,1... | collective-permute-start | bytes 589832 | tf_op jit(solution)/shard_map/ppermute | solution.py:22
  213.5 11.3 %collective-permute-start.11 = (bf16[384,256]{1,0:T(8,128)(2,1)}, bf16[384,256]{1,0:T(8,128)(2,1)}, u32[]{:S(2)}, u32[]{:S(2)}) collective-permute-start(bf16[384,256]{1,0:T(8,128)(2,1)} %convolution_convert_fusion.2.refs_0_), channel_id=1, source_target_pairs={{0,3},{1,0},{2,1},{3,2},{4,7},{5,4},{6,5},{7,6},{8,11},{9,8},{10,9... | collective-permute-start | bytes 589832 | tf_op jit(solution)/shard_map/ppermute | solution.py:22
  216.2 12.3 %collective-permute-start.12 = (bf16[384,256]{1,0:T(8,128)(2,1)}, bf16[384,256]{1,0:T(8,128)(2,1)}, u32[]{:S(2)}, u32[]{:S(2)}) collective-permute-start(bf16[384,256]{1,0:T(8,128)(2,1)} %convolution_convert_fusion.2.refs_0_), channel_id=1, source_target_pairs={{0,2},{1,3},{2,0},{3,1},{4,6},{5,7},{6,4},{7,5},{8,10},{9,11},{10,... | collective-permute-start | bytes 589832 | tf_op jit(solution)/shard_map/ppermute | solution.py:22
  224.8 21.9 %collective-permute-start.21 = (bf16[384,512]{1,0:T(8,128)(2,1)S(1)}, bf16[384,512]{1,0:T(8,128)(2,1)S(1)}, u32[]{:S(2)}, u32[]{:S(2)}) collective-permute-start(bf16[384,512]{1,0:T(8,128)(2,1)S(1)} %convolution_convert_fusion.1.refs_8_), channel_id=1, source_target_pairs={{0,2},{1,3},{2,0},{3,1},{4,6},{5,7},{6,4},{7,5},{8,10},{9,11},{10,... | collective-permute-start | bytes 1179656 | tf_op jit(solution)/shard_map/ppermute | solution.py:22
  224.8 21.9 %collective-permute-start.16 = (bf16[384,128]{1,0:T(8,128)(2,1)S(1)}, bf16[384,128]{1,0:T(8,128)(2,1)S(1)}, u32[]{:S(2)}, u32[]{:S(2)}) collective-permute-start(bf16[384,128]{1,0:T(8,128)(2,1)S(1)} %convolution_convert_fusion.3.refs_4_), channel_id=1, source_target_pairs={{0,1},{1,2},{2,3},{3,0},{4,5},{5,6},{6,7},{7,4},{8,9},{9,10},{10,1... | collective-permute-start | bytes 294920 | tf_op jit(solution)/shard_map/ppermute | solution.py:22
  228.5 18.2 %collective-permute-start.17 = (bf16[384,128]{1,0:T(8,128)(2,1)S(1)}, bf16[384,128]{1,0:T(8,128)(2,1)S(1)}, u32[]{:S(2)}, u32[]{:S(2)}) collective-permute-start(bf16[384,128]{1,0:T(8,128)(2,1)S(1)} %convolution_convert_fusion.3.refs_4_), channel_id=1, source_target_pairs={{0,3},{1,0},{2,1},{3,2},{4,7},{5,4},{6,5},{7,6},{8,11},{9,8},{10,9... | collective-permute-start | bytes 294920 | tf_op jit(solution)/shard_map/ppermute | solution.py:22
  239.3 8.1 %collective-permute-start.18 = (bf16[384,128]{1,0:T(8,128)(2,1)S(1)}, bf16[384,128]{1,0:T(8,128)(2,1)}, u32[]{:S(2)}, u32[]{:S(2)}) collective-permute-start(bf16[384,128]{1,0:T(8,128)(2,1)S(1)} %convolution_convert_fusion.3.refs_4_), channel_id=1, source_target_pairs={{0,2},{1,3},{2,0},{3,1},{4,6},{5,7},{6,4},{7,5},{8,10},{9,11},{10,... | collective-permute-start | bytes 294920 | tf_op jit(solution)/shard_map/ppermute | solution.py:22
  263.8 26.5 %all-to-all-start.5 = ((bf16[32,64,256]{2,1,0:T(8,128)(2,1)}), bf16[32,64,256]{2,1,0:T(8,128)(2,1)}, u32[]{:S(2)}, u32[]{:S(2)}) async-start(bf16[32,64,256]{2,1,0:T(8,128)(2,1)} %bitcast.73), calls=%async_computation.5 | async-start | bytes 2097152 | tf_op jit(solution)/shard_map/all_to_all | solution.py:26
  274.5 12.7 %collective-permute-start.23 = (f32[2,256]{1,0:T(2,128)S(1)}, f32[2,256]{1,0:T(2,128)S(1)}, u32[]{:S(2)}, u32[]{:S(2)}) collective-permute-start(f32[2,256]{1,0:T(2,128)S(1)} %slice.56), channel_id=1, source_target_pairs={{4,0},{8,4},{12,8},{16,12},{20,16},{24,20},{28,24},{32,28},{36,32}... | collective-permute-start | bytes 6152 | tf_op jit(solution)/shard_map/ppermute | solution.py:17
  (23 other events, 200.6 us)

commit v6 on v3

--- a/solution.py
+++ b/solution.py
@@ -269,8 +269,19 @@
     write_parts(both, mat_ref, refs)
 
 
-def other_kernel(both_ref, mat_ref, *refs):
-    write_parts(both_ref[...], mat_ref, refs)
+def other_kernel(both_ref, a_next_ref, b_prev_ref, mat_ref, own_ref, *refs):
+    part = lax.dot_general(both_ref[...], mat_ref[...], along_last, preferred_element_type=f32)
+    for i, ref in enumerate((a_next_ref, b_prev_ref)):
+        at = slice(i * direct_width, (i + 1) * direct_width)
+        own_ref[:, at] = (part[:, at] + ref[...].astype(f32)).astype(bf16)
+    for i, ref in enumerate(refs):
+        ref[...] = part[:, (i + 2) * direct_width : (i + 3) * direct_width].astype(bf16)
+
+
+def wide_kernel(own_ref, a_prev_ref, b_next_ref, out_ref):
+    for i, ref in enumerate((a_prev_ref, b_next_ref)):
+        at = slice(i * direct_width, (i + 1) * direct_width)
+        out_ref[:, at] = (own_ref[:, at].astype(f32) + ref[...].astype(f32)).astype(bf16)
 
 
 part_block = 512
@@ -343,26 +354,22 @@
 
     direct_mat = both_mat.reshape(lanes, quarter, -1)[:, -direct_width:]
     first_mat = jnp.concatenate(
-        [weight_rows(2, 0, 2), weight_rows(3, 0, 1), weight_rows(1, 1, 1)]
+        [weight_rows(2, 0, 2), weight_rows(3, 0, 2), weight_rows(1, 0, 2)]
         + [direct_mat.reshape(lanes * direct_width, -1)],
         axis=0,
     )
     other_mat = jnp.concatenate(
-        [weight_rows(0, 0, 3), weight_rows(1, 0, 1), weight_rows(1, 2, 1)]
-        + [weight_rows(3, 1, 2), weight_rows(2, 2, 1)],
+        [weight_rows(0, 0, 3), weight_rows(1, 2, 1), weight_rows(3, 2, 1), weight_rows(2, 2, 1)],
         axis=0,
     )
     activated, slope, hidden, first_mat, other_mat = lax.optimization_barrier(
         (activated.astype(bf16), slope.astype(bf16), hidden, first_mat, other_mat)
     )
-    dboth, a_far, b_far, a_behind, b_ahead, direct = by_rows(
+    dboth, a_far, b_far, a_behind, b_behind, a_ahead, b_ahead, direct = by_rows(
         first_kernel,
         (entry_cots, activated, slope),
         (down_mat, first_mat),
-        [both_mat.shape[1]] + [direct_width] * 4 + [lanes * direct_width],
-    )
-    a_own, b_own, c_own, a_ahead, c_ahead, b_behind, c_behind, c_far = by_rows(
-        other_kernel, (dboth,), (other_mat,), [direct_width] * 8
+        [both_mat.shape[1]] + [direct_width] * 6 + [lanes * direct_width],
     )
 
     def back(array):
@@ -377,15 +384,21 @@
     a_far = turned(a_far, 1)
     b_far = turned(b_far, -1)
     direct = back(direct)
-    c_ahead, direct = lax.optimization_barrier((c_ahead, direct))
     a_next = turned(a_behind, -1)
     b_prev = turned(b_ahead, 1)
     a_prev = turned(plus(a_ahead, a_far), 1)
     b_next = turned(plus(b_behind, b_far), -1)
+    wide_own, c_own, c_ahead, c_behind, c_far = by_rows(
+        other_kernel,
+        (dboth, a_next, b_prev),
+        (other_mat,),
+        [2 * direct_width] + [direct_width] * 4,
+    )
     c_far = turned(c_far, 1)
     c_next = turned(c_behind, -1)
+    c_ahead, direct = lax.optimization_barrier((c_ahead, direct))
     grad_down = jnp.einsum("rf,rd->fd", hidden, entry_cots, preferred_element_type=f32)
-    wide = jnp.concatenate([plus(a_own, a_prev, a_next), plus(b_own, b_prev, b_next)], axis=1)
+    (wide,) = by_rows(wide_kernel, (wide_own, a_prev, b_next), (), [2 * direct_width])
     c_own, wide = lax.optimization_barrier((c_own, wide))
     wide = back(wide)
     direct_parts = lane_gather(per_token(direct))

time: 305 us -> 294 us (0.964)
  waiting for transfers between devices: 126 us -> 116 us
    ppermute x22, waiting for transfers between devices: 93.1 us -> 83 us  [turned(): lax.ppermute(array, 'tp', [(i, (i + by) % size) for i in range(size)])]
    pallas_call x2 -> x3, Pallas kernels: 15.3 us -> 18.3 us  [by_rows(): pl.pallas_call(kernel, grid=(slots // part_block,), in_specs=[rows(x.shap...]
    convert_element_type x6 -> x4, other arithmetic: 7.79 us -> 5.72 us  [plus(): return sum((array.astype(f32) for array in arrays)).astype(bf16)]
  transfers between devices with their start and end apart: 30 -> 30, of which waited for: 13 -> 11; matrix products, arithmetic and copies ran while one was open for 13% -> 13% of each run, Pallas kernels for 4% -> 5%
where the time goes in v6:
time: 294 us; the launch traced here: 293 us
  waiting for transfers between devices  116 us (39%)
  starting transfers between devices  83.2 us (28%)
  Pallas kernels  36.5 us (12%)
  matrix products  30.6 us (10%)
  local copies, waits for them, and re-layouts  13.6 us (5%)
  other arithmetic  11.7 us (4%)
    ppermute x22, waiting for transfers between devices, turned(): lax.ppermute(array, 'tp', [(i, (i + by) % size) for i in range(size)])  83 us
    all_to_all x6, starting transfers between devices, exchanged(): return lax.all_to_all(array, 'sp', split_axis=0, concat_axis=0, tiled=True)  49.5 us
    ppermute x22, starting transfers between devices, turned(): lax.ppermute(array, 'tp', [(i, (i + by) % size) for i in range(size)])  26.7 us
    all_to_all x6, waiting for transfers between devices, exchanged(): return lax.all_to_all(array, 'sp', split_axis=0, concat_axis=0, tiled=True)  25.3 us
    pallas_call x3, Pallas kernels, by_rows(): pl.pallas_call(kernel, grid=(slots // part_block,), in_specs=[rows(x.shap...  18.3 us
    dot_general x1, matrix products, on_device(): jnp.einsum('rd,rf->df', entry_rows, late_both, preferred_element_type=f32)  8.03 us
    ppermute x2, waiting for transfers between devices, passed_along(): return lax.ppermute(array, axis, pairs)  8.01 us
    pallas_call x1, Pallas kernels, weighted_rows(): pl.pallas_call(weighted_kernel, grid=(slots // slot_block,), in_specs=[pl...  7.77 us
  transfers between devices with their start and end apart: 30, of which 11 were waited for; matrix products, arithmetic and copies ran while one was open for 13% of the time, Pallas kernels for 5%

profile of v6, /device:TPU:1, one launch (start us, length us, event | category | flops | bytes accessed | tf_op | source)
XLA Modules:
  0.0 293.0 jit_solution(2494002373481768403)
XLA Ops:
  0.7 5.5 %shard_map.188 = (bf16[1536,512]{1,0:T(8,128)(2,1)}, bf16[1536,384]{1,0:T(8,128)(2,1)}, bf16[384,32]{1,0:T(8,128)(2,1)}, bf16[32,384]{1,0:T(8,128)(2,1)}, bf16[32,384]{1,0:T(8,128)(2,1)}) custom-call(s32[1]{0:T(128)} %bitcast.lane_ref, s32[2,384]{1,0:T(2,128)} %bitcast.78, f32[2,384]{1,0:T(2,128)} %bitcast.79, bf16[384,2048]{1,0:T(8,128)(2,1)} %refs_13_.1, ...), custom_call_target="tpu_custom_call" | custom-call | tf_op jit(solution)/shard_map/pallas_call | solution.py:181
  6.2 9.6 %all-to-all-start.1 = ((bf16[32,48,512]{2,1,0:T(8,128)(2,1)}), bf16[32,48,512]{2,1,0:T(8,128)(2,1)S(1)}, u32[]{:S(2)}, u32[]{:S(2)}) async-start(bf16[32,48,512]{2,1,0:T(8,128)(2,1)} %bitcast.66), calls=%async_computation.1 | async-start | bytes 3145728 | tf_op jit(solution)/shard_map/all_to_all | solution.py:26
  15.8 7.8 %shard_map.189 = (bf16[1536,2048]{1,0:T(8,128)(2,1)}, bf16[384,1536]{1,0:T(8,128)(2,1)}) custom-call(bf16[1536,384]{1,0:T(8,128)(2,1)} %get-tuple-element.40.chooser_ref, bf16[384,2048]{1,0:T(8,128)(2,1)} %refs_12_.1, bf16[384,32]{1,0:T(8,128)(2,1)} %get-tuple-element.41.rank_ref, bf16[32,384]{1,0:T(8,128)(2,1)} %get-tuple-element.42.high_ref, ...), custom_call_target="tpu_custom_call" | custom-call | tf_op jit(solution)/shard_map/pallas_call | solution.py:236
  23.5 14.4 %all-to-all-done.1 = bf16[32,48,512]{2,1,0:T(8,128)(2,1)S(1)} async-done(((bf16[32,48,512]{2,1,0:T(8,128)(2,1)}), bf16[32,48,512]{2,1,0:T(8,128)(2,1)S(1)}, u32[]{:S(2)}, u32[]{:S(2)}) %all-to-all-start.1) | async-done | bytes 1572896 | tf_op jit(solution)/shard_map/all_to_all | solution.py:26
  39.1 6.6 %all-to-all-start = ((bf16[32,48,2048]{2,1,0:T(8,128)(2,1)}), bf16[32,48,2048]{2,1,0:T(8,128)(2,1)}, u32[]{:S(2)}, u32[]{:S(2)}) async-start(bf16[32,48,2048]{2,1,0:T(8,128)(2,1)} %bitcast.59), calls=%async_computation | async-start | bytes 12582912 | tf_op jit(solution)/shard_map/all_to_all | solution.py:26
  50.7 32.1 %collective-permute-done = bf16[1536,512]{1,0:T(8,128)(2,1)} collective-permute-done((bf16[1536,512]{1,0:T(8,128)(2,1)}, bf16[1536,512]{1,0:T(8,128)(2,1)}, u32[]{:S(2)}, u32[]{:S(2)}) %collective-permute-start) | collective-permute-done | bytes 1572896 | tf_op jit(solution)/shard_map/ppermute | solution.py:22
  85.3 2.7 collective-permute-start.3
  92.5 10.8 %collective-permute-done.2 = bf16[768,512]{1,0:T(8,128)(2,1)S(1)} collective-permute-done((bf16[768,512]{1,0:T(8,128)(2,1)S(1)}, bf16[768,512]{1,0:T(8,128)(2,1)S(1)}, u32[]{:S(2)}, u32[]{:S(2)}) %collective-permute-start.2) | collective-permute-done | bytes 786464 | tf_op jit(solution)/shard_map/ppermute | solution.py:22
  106.1 3.6 %multiply_convert_fusion = (bf16[1536,256]{1,0:T(8,128)(2,1)S(1)}, bf16[1536,256]{1,0:T(8,128)(2,1)}, bf16[1536,256]{1,0:T(8,128)(2,1)}) fusion(f32[1536,256]{1,0:T(8,128)S(1)} %fusion.25, bf16[1536,2048]{1,0:T(8,128)(2,1)S(1)} %constant_dynamic-update-slice_fusion.4, bf16[1,2048,256]{2,1,0:T(8,128)(2,1)S(1)} %copy-done.2), kind=kOutput, calls=%fused_computation.19 | convolution fusion | flops 1615724544 | bytes 11272192 | tf_op jit(solution)/shard_map/dot_general | solution.py:344
  109.7 9.3 %all-to-all-done = bf16[32,48,2048]{2,1,0:T(8,128)(2,1)} async-done(((bf16[32,48,2048]{2,1,0:T(8,128)(2,1)}), bf16[32,48,2048]{2,1,0:T(8,128)(2,1)}, u32[]{:S(2)}, u32[]{:S(2)}) %all-to-all-start) | async-done | bytes 6291488 | tf_op jit(solution)/shard_map/all_to_all | solution.py:26
  119.0 10.1 %shard_map.190 = (bf16[1536,512]{1,0:T(8,128)(2,1)}, bf16[1536,128]{1,0:T(8,128)(2,1)}, bf16[1536,128]{1,0:T(8,128)(2,1)}, bf16[1536,128]{1,0:T(8,128)(2,1)}, bf...) custom-call(bf16[1536,2048]{1,0:T(8,128)(2,1)} %bitcast.5.cot_ref, ...), custom_call_target="tpu_custom_call" | custom-call | tf_op jit(solution)/shard_map/pallas_call | solution.py:296
  130.6 9.7 %all-to-all-start.3 = ((bf16[32,48,512]{2,1,0:T(8,128)(2,1)}), bf16[32,48,512]{2,1,0:T(8,128)(2,1)}, u32[]{:S(2)}, u32[]{:S(2)}) async-start(bf16[32,48,512]{2,1,0:T(8,128)(2,1)} %bitcast.65), calls=%async_computation.3 | async-start | bytes 3145728 | tf_op jit(solution)/shard_map/all_to_all | solution.py:26
  141.8 2.7 collective-permute-start.8
  146.4 13.0 %collective-permute-done.8 = bf16[1536,128]{1,0:T(8,128)(2,1)S(1)} collective-permute-done((bf16[1536,128]{1,0:T(8,128)(2,1)}, bf16[1536,128]{1,0:T(8,128)(2,1)S(1)}, u32[]{:S(2)}, u32[]{:S(2)}) %collective-permute-start.8) | collective-permute-done | bytes 393248 | tf_op jit(solution)/shard_map/ppermute | solution.py:22
  163.7 4.9 %shard_map.191 = (bf16[1536,256]{1,0:T(8,128)(2,1)}, bf16[1536,128]{1,0:T(8,128)(2,1)}, bf16[1536,128]{1,0:T(8,128)(2,1)}, bf16[1536,128]{1,0:T(8,128)(2,1)}, bf16[1536,128]{1,0:T(8,128)(2,1)}) custom-call(bf16[1536,512]{1,0:T(8,128)(2,1)} %get-tuple-element.68.both_ref, bf16[1536,128]{1,0:T(8,128)(2,1)} %copy-done.17, bf16[1536,128]{1,0:T(8,128)(2,1)} %copy-done.18, ...), custom_call_target="tpu_custom_call" | custom-call | tf_op jit(solution)/shard_map/pallas_call | solution.py:296
  168.8 4.7 %collective-permute-start.22 = (f32[2,256]{1,0:T(2,128)S(1)}, f32[2,256]{1,0:T(2,128)S(1)}, u32[]{:S(2)}, u32[]{:S(2)}) collective-permute-start(f32[2,256]{1,0:T(2,128)S(1)} %slice.53), channel_id=1, source_target_pairs={{0,4},{4,8},{8,12},{12,16},{16,20},{20,24},{24,28},{28,32},{32,36}... | collective-permute-start | bytes 6152 | tf_op jit(solution)/shard_map/ppermute | solution.py:17
  173.5 3.0 %collective-permute-start.15 = (bf16[1536,128]{1,0:T(8,128)(2,1)}, bf16[1536,128]{1,0:T(8,128)(2,1)}, u32[]{:S(2)}, u32[]{:S(2)}) collective-permute-start(bf16[1536,128]{1,0:T(8,128)(2,1)} %get-tuple-element.66), channel_id=1, source_target_pairs={{0,3},{1,0},{2,1},{3,2},{4,7},{5,4},{6,5},{7,6},{8,11},{9,8},{10,9... | collective-permute-start | bytes 1179656 | tf_op jit(solution)/shard_map/ppermute | solution.py:22
  177.2 3.2 %shard_map.192 = bf16[1536,256]{1,0:T(8,128)(2,1)} custom-call(bf16[1536,256]{1,0:T(8,128)(2,1)} %get-tuple-element.55.own_ref, bf16[1536,128]{1,0:T(8,128)(2,1)} %copy-done.16, bf16[1536,128]{1,0:T(8,128)(2,1)} %collective-permute-done.9.b_next_ref), custom_call_target="tpu_custom_call" | custom-call | tf_op jit(solution)/shard_map/pallas_call | solution.py:296
  180.5 6.9 %all-to-all-start.2 = ((bf16[32,48,256]{2,1,0:T(8,128)(2,1)}), bf16[32,48,256]{2,1,0:T(8,128)(2,1)}, u32[]{:S(2)}, u32[]{:S(2)}) async-start(bf16[32,48,256]{2,1,0:T(8,128)(2,1)} %bitcast.63), calls=%async_computation.2 | async-start | bytes 1572864 | tf_op jit(solution)/shard_map/all_to_all | solution.py:26
  188.8 11.5 %collective-permute-done.14 = bf16[1536,128]{1,0:T(8,128)(2,1)S(1)} collective-permute-done((bf16[1536,128]{1,0:T(8,128)(2,1)S(1)}, bf16[1536,128]{1,0:T(8,128)(2,1)S(1)}, u32[]{:S(2)}, u32[]{:S(2)}) %collective-permute-start.14) | collective-permute-done | bytes 393248 | tf_op jit(solution)/shard_map/ppermute | solution.py:22
  202.2 8.0 %all-to-all-start.4 = ((bf16[32,48,128]{2,1,0:T(8,128)(2,1)}), bf16[32,48,128]{2,1,0:T(8,128)(2,1)S(1)}, u32[]{:S(2)}, u32[]{:S(2)}) async-start(bf16[32,48,128]{2,1,0:T(8,128)(2,1)} %bitcast.18), calls=%async_computation.4 | async-start | bytes 786432 | tf_op jit(solution)/shard_map/all_to_all | solution.py:26
  213.0 2.7 collective-permute-start.20
  218.0 2.7 collective-permute-start.11
  222.4 10.8 %collective-permute-done.10.refs_1_ = bf16[384,256]{1,0:T(8,128)(2,1)} collective-permute-done((bf16[384,256]{1,0:T(8,128)(2,1)}, bf16[384,256]{1,0:T(8,128)(2,1)}, u32[]{:S(2)}, u32[]{:S(2)}) %collective-permute-start.10) | collective-permute-done | bytes 196640 | tf_op jit(solution)/shard_map/ppermute | solution.py:22
  233.3 2.7 collective-permute-start.17
  237.6 5.9 %convolution_bitcast_fusion = f32[1,256,2048]{2,1,0:T(8,128)} fusion(bf16[1536,256]{1,0:T(8,128)(2,1)S(1)} %get-tuple-element.70, bf16[1536,2048]{1,0:T(8,128)(2,1)} %bitcast.5.cot_ref), kind=kOutput, calls=%fused_computation.14 | convolution fusion | flops 1610612736 | bytes 9175040 | tf_op jit(solution)/shard_map/rf,rd->fd/dot_general | solution.py:400
  244.4 4.0 %collective-permute-done.16.refs_5_ = bf16[384,128]{1,0:T(8,128)(2,1)S(1)} collective-permute-done((bf16[384,128]{1,0:T(8,128)(2,1)S(1)}, bf16[384,128]{1,0:T(8,128)(2,1)S(1)}, u32[]{:S(2)}, u32[]{:S(2)}) %collective-permute-start.16) | collective-permute-done | bytes 98336 | tf_op jit(solution)/shard_map/ppermute | solution.py:22
  249.0 5.0 %shard_map.193 = bf16[384,2048]{1,0:T(8,128)(2,1)} custom-call(s32[1]{0:T(128)} %bitcast.lane_ref, bf16[384,256]{1,0:T(8,128)(2,1)} %convolution_convert_fusion.2.refs_0_, bf16[384,256]{1,0:T(8,128)(2,1)} %collective-permute-done.10.refs_1_, bf16[384,256]{1,0:T(8,128)(2,1)} %collective-permute-done.11.refs_2_, ...), custom_call_target="tpu_custom_call" | custom-call | tf_op jit(solution)/shard_map/pallas_call | solution.py:97
  254.0 3.3 %convolution_convert_fusion = bf16[2048,256]{1,0:T(8,128)(2,1)} fusion(bf16[384,2048]{1,0:T(8,128)(2,1)} %shard_map.193, f32[384,256]{1,0:T(8,128)S(1)} %fusion.8, bf16[384,256]{1,0:T(8,128)(2,1)S(1)} %copy-done.23), kind=kOutput, calls=%fused_computation.15 | convolution fusion | flops 403472384 | bytes 3211264 | tf_op jit(solution)/shard_map/td,tc->dc/dot_general | solution.py:419
  257.3 8.0 %fusion.29 = f32[2048,512]{1,0:T(8,128)} fusion(bf16[1536,2048]{1,0:T(8,128)(2,1)} %copy-done.4, bf16[1536,512]{1,0:T(8,128)(2,1)S(1)} %copy-done.8), kind=kOutput, calls=%fused_computation.76 | convolution fusion | flops 3221225472 | bytes 12058624 | tf_op jit(solution)/shard_map/rd,rf->df/dot_general | solution.py:423
  265.3 8.6 %all-to-all-start.5 = ((bf16[32,64,256]{2,1,0:T(8,128)(2,1)}), bf16[32,64,256]{2,1,0:T(8,128)(2,1)}, u32[]{:S(2)}, u32[]{:S(2)}) async-start(bf16[32,64,256]{2,1,0:T(8,128)(2,1)} %bitcast.69), calls=%async_computation.5 | async-start | bytes 2097152 | tf_op jit(solution)/shard_map/all_to_all | solution.py:26
  279.9 8.0 %collective-permute-done.23 = f32[2,256]{1,0:T(2,128)S(1)} collective-permute-done((f32[2,256]{1,0:T(2,128)S(1)}, f32[2,256]{1,0:T(2,128)S(1)}, u32[]{:S(2)}, u32[]{:S(2)}) %collective-permute-start.23) | collective-permute-done | bytes 2080 | tf_op jit(solution)/shard_map/ppermute | solution.py:17
  (124 shorter events, 50.2 us)
Async XLA Ops:
  0.6 273.3 %copy-start = (bf16[2048,256]{1,0:T(8,128)(2,1)S(1)}, bf16[2048,256]{1,0:T(8,128)(2,1)}, u32[]{:S(2)}) copy-start(bf16[2048,256]{1,0:T(8,128)(2,1)} %param.21) | copy-start | bytes 3145732
  6.2 31.8 %all-to-all-start.1 = ((bf16[32,48,512]{2,1,0:T(8,128)(2,1)}), bf16[32,48,512]{2,1,0:T(8,128)(2,1)S(1)}, u32[]{:S(2)}, u32[]{:S(2)}) async-start(bf16[32,48,512]{2,1,0:T(8,128)(2,1)} %bitcast.66), calls=%async_computation.1 | async-start | bytes 3145728 | tf_op jit(solution)/shard_map/all_to_all | solution.py:26
  39.1 79.9 %all-to-all-start = ((bf16[32,48,2048]{2,1,0:T(8,128)(2,1)}), bf16[32,48,2048]{2,1,0:T(8,128)(2,1)}, u32[]{:S(2)}, u32[]{:S(2)}) async-start(bf16[32,48,2048]{2,1,0:T(8,128)(2,1)} %bitcast.59), calls=%async_computation | async-start | bytes 12582912 | tf_op jit(solution)/shard_map/all_to_all | solution.py:26
  45.7 37.1 %collective-permute-start = (bf16[1536,512]{1,0:T(8,128)(2,1)}, bf16[1536,512]{1,0:T(8,128)(2,1)}, u32[]{:S(2)}, u32[]{:S(2)}) collective-permute-start(bf16[1536,512]{1,0:T(8,128)(2,1)} %bitcast.60), channel_id=1, source_target_pairs={{0,1},{1,2},{2,3},{3,0},{4,5},{5,6},{6,7},{7,4},{8,9},{9,10},{10,1... | collective-permute-start | bytes 4718600 | tf_op jit(solution)/shard_map/ppermute | solution.py:22
  47.0 37.1 %collective-permute-start.1 = (bf16[1536,512]{1,0:T(8,128)(2,1)}, bf16[1536,512]{1,0:T(8,128)(2,1)}, u32[]{:S(2)}, u32[]{:S(2)}) collective-permute-start(bf16[1536,512]{1,0:T(8,128)(2,1)} %bitcast.61), channel_id=1, source_target_pairs={{0,3},{1,0},{2,1},{3,2},{4,7},{5,4},{6,5},{7,6},{8,11},{9,8},{10,9... | collective-permute-start | bytes 4718600 | tf_op jit(solution)/shard_map/ppermute | solution.py:22
  84.0 19.2 %collective-permute-start.2 = (bf16[768,512]{1,0:T(8,128)(2,1)S(1)}, bf16[768,512]{1,0:T(8,128)(2,1)S(1)}, u32[]{:S(2)}, u32[]{:S(2)}) collective-permute-start(bf16[768,512]{1,0:T(8,128)(2,1)S(1)} %slice.51), channel_id=1, source_target_pairs={{0,1},{1,2},{2,3},{3,0},{4,5},{5,6},{6,7},{7,4},{8,9},{9,10},{10,1... | collective-permute-start | bytes 2359304 | tf_op jit(solution)/shard_map/ppermute | solution.py:22
  85.3 18.1 %collective-permute-start.3 = (bf16[768,512]{1,0:T(8,128)(2,1)S(1)}, bf16[768,512]{1,0:T(8,128)(2,1)S(1)}, u32[]{:S(2)}, u32[]{:S(2)}) collective-permute-start(bf16[768,512]{1,0:T(8,128)(2,1)S(1)} %slice.52), channel_id=1, source_target_pairs={{0,3},{1,0},{2,1},{3,2},{4,7},{5,4},{6,5},{7,6},{8,11},{9,8},{10,9... | collective-permute-start | bytes 2359304 | tf_op jit(solution)/shard_map/ppermute | solution.py:22
  129.1 15.4 %collective-permute-start.6 = (bf16[1536,128]{1,0:T(8,128)(2,1)}, bf16[1536,128]{1,0:T(8,128)(2,1)}, u32[]{:S(2)}, u32[]{:S(2)}) collective-permute-start(bf16[1536,128]{1,0:T(8,128)(2,1)} %get-tuple-element.57), channel_id=1, source_target_pairs={{0,1},{1,2},{2,3},{3,0},{4,5},{5,6},{6,7},{7,4},{8,9},{9,10},{10,1... | collective-permute-start | bytes 1179656 | tf_op jit(solution)/shard_map/ppermute | solution.py:22
  130.6 28.8 %copy-start.21 = (bf16[1536,128]{1,0:T(8,128)(2,1)S(1)}, bf16[1536,128]{1,0:T(8,128)(2,1)}, u32[]{:S(2)}) copy-start(bf16[1536,128]{1,0:T(8,128)(2,1)} %get-tuple-element.58) | copy-start | bytes 1179652
  130.6 49.9 %all-to-all-start.3 = ((bf16[32,48,512]{2,1,0:T(8,128)(2,1)}), bf16[32,48,512]{2,1,0:T(8,128)(2,1)}, u32[]{:S(2)}, u32[]{:S(2)}) async-start(bf16[32,48,512]{2,1,0:T(8,128)(2,1)} %bitcast.65), calls=%async_computation.3 | async-start | bytes 3145728 | tf_op jit(solution)/shard_map/all_to_all | solution.py:26
  140.3 22.5 %collective-permute-start.4 = (bf16[1536,128]{1,0:T(8,128)(2,1)}, bf16[1536,128]{1,0:T(8,128)(2,1)S(1)}, u32[]{:S(2)}, u32[]{:S(2)}) collective-permute-start(bf16[1536,128]{1,0:T(8,128)(2,1)} %get-tuple-element.51), channel_id=1, source_target_pairs={{0,3},{1,0},{2,1},{3,2},{4,7},{5,4},{6,5},{7,6},{8,11},{9,8},{10,9... | collective-permute-start | bytes 1179656 | tf_op jit(solution)/shard_map/ppermute | solution.py:22
  141.8 21.0 %collective-permute-start.5 = (bf16[1536,128]{1,0:T(8,128)(2,1)}, bf16[1536,128]{1,0:T(8,128)(2,1)S(1)}, u32[]{:S(2)}, u32[]{:S(2)}) collective-permute-start(bf16[1536,128]{1,0:T(8,128)(2,1)} %get-tuple-element.52), channel_id=1, source_target_pairs={{0,1},{1,2},{2,3},{3,0},{4,5},{5,6},{6,7},{7,4},{8,9},{9,10},{10,1... | collective-permute-start | bytes 1179656 | tf_op jit(solution)/shard_map/ppermute | solution.py:22
  141.8 17.5 %collective-permute-start.8 = (bf16[1536,128]{1,0:T(8,128)(2,1)}, bf16[1536,128]{1,0:T(8,128)(2,1)S(1)}, u32[]{:S(2)}, u32[]{:S(2)}) collective-permute-start(bf16[1536,128]{1,0:T(8,128)(2,1)} %get-tuple-element.59), channel_id=1, source_target_pairs={{0,3},{1,0},{2,1},{3,2},{4,7},{5,4},{6,5},{7,6},{8,11},{9,8},{10,9... | collective-permute-start | bytes 1179656 | tf_op jit(solution)/shard_map/ppermute | solution.py:22
  146.4 30.1 %collective-permute-start.7 = (bf16[1536,128]{1,0:T(8,128)(2,1)}, bf16[1536,128]{1,0:T(8,128)(2,1)S(1)}, u32[]{:S(2)}, u32[]{:S(2)}) collective-permute-start(bf16[1536,128]{1,0:T(8,128)(2,1)} %add_convert_fusion.3), channel_id=1, source_target_pairs={{0,1},{1,2},{2,3},{3,0},{4,5},{5,6},{6,7},{7,4},{8,9},{9,10},{10,1... | collective-permute-start | bytes 1179656 | tf_op jit(solution)/shard_map/ppermute | solution.py:22
  160.2 16.3 %collective-permute-start.9 = (bf16[1536,128]{1,0:T(8,128)(2,1)}, bf16[1536,128]{1,0:T(8,128)(2,1)}, u32[]{:S(2)}, u32[]{:S(2)}) collective-permute-start(bf16[1536,128]{1,0:T(8,128)(2,1)} %add_convert_fusion.2), channel_id=1, source_target_pairs={{0,3},{1,0},{2,1},{3,2},{4,7},{5,4},{6,5},{7,6},{8,11},{9,8},{10,9... | collective-permute-start | bytes 1179656 | tf_op jit(solution)/shard_map/ppermute | solution.py:22
  168.6 18.8 %collective-permute-start.13 = (bf16[1536,128]{1,0:T(8,128)(2,1)}, bf16[1536,128]{1,0:T(8,128)(2,1)}, u32[]{:S(2)}, u32[]{:S(2)}) collective-permute-start(bf16[1536,128]{1,0:T(8,128)(2,1)} %get-tuple-element.65), channel_id=1, source_target_pairs={{0,1},{1,2},{2,3},{3,0},{4,5},{5,6},{6,7},{7,4},{8,9},{9,10},{10,1... | collective-permute-start | bytes 1179656 | tf_op jit(solution)/shard_map/ppermute | solution.py:22
  168.8 19.9 %collective-permute-start.22 = (f32[2,256]{1,0:T(2,128)S(1)}, f32[2,256]{1,0:T(2,128)S(1)}, u32[]{:S(2)}, u32[]{:S(2)}) collective-permute-start(f32[2,256]{1,0:T(2,128)S(1)} %slice.53), channel_id=1, source_target_pairs={{0,4},{4,8},{8,12},{12,16},{16,20},{20,24},{24,28},{28,32},{32,36}... | collective-permute-start | bytes 6152 | tf_op jit(solution)/shard_map/ppermute | solution.py:17
  173.5 15.3 %collective-permute-start.15 = (bf16[1536,128]{1,0:T(8,128)(2,1)}, bf16[1536,128]{1,0:T(8,128)(2,1)}, u32[]{:S(2)}, u32[]{:S(2)}) collective-permute-start(bf16[1536,128]{1,0:T(8,128)(2,1)} %get-tuple-element.66), channel_id=1, source_target_pairs={{0,3},{1,0},{2,1},{3,2},{4,7},{5,4},{6,5},{7,6},{8,11},{9,8},{10,9... | collective-permute-start | bytes 1179656 | tf_op jit(solution)/shard_map/ppermute | solution.py:22
  180.5 21.7 %all-to-all-start.2 = ((bf16[32,48,256]{2,1,0:T(8,128)(2,1)}), bf16[32,48,256]{2,1,0:T(8,128)(2,1)}, u32[]{:S(2)}, u32[]{:S(2)}) async-start(bf16[32,48,256]{2,1,0:T(8,128)(2,1)} %bitcast.63), calls=%async_computation.2 | async-start | bytes 1572864 | tf_op jit(solution)/shard_map/all_to_all | solution.py:26
  188.5 11.8 %collective-permute-start.14 = (bf16[1536,128]{1,0:T(8,128)(2,1)S(1)}, bf16[1536,128]{1,0:T(8,128)(2,1)S(1)}, u32[]{:S(2)}, u32[]{:S(2)}) collective-permute-start(bf16[1536,128]{1,0:T(8,128)(2,1)S(1)} %add_convert_fusion.1), channel_id=1, source_target_pairs={{0,1},{1,2},{2,3},{3,0},{4,5},{5,6},{6,7},{7,4},{8,9},{9,10},{10,1... | collective-permute-start | bytes 1179656 | tf_op jit(solution)/shard_map/ppermute | solution.py:22
  202.2 18.4 %all-to-all-start.4 = ((bf16[32,48,128]{2,1,0:T(8,128)(2,1)}), bf16[32,48,128]{2,1,0:T(8,128)(2,1)S(1)}, u32[]{:S(2)}, u32[]{:S(2)}) async-start(bf16[32,48,128]{2,1,0:T(8,128)(2,1)} %bitcast.18), calls=%async_computation.4 | async-start | bytes 786432 | tf_op jit(solution)/shard_map/all_to_all | solution.py:26
  212.9 23.0 %collective-permute-start.19 = (bf16[384,512]{1,0:T(8,128)(2,1)S(1)}, bf16[384,512]{1,0:T(8,128)(2,1)}, u32[]{:S(2)}, u32[]{:S(2)}) collective-permute-start(bf16[384,512]{1,0:T(8,128)(2,1)S(1)} %convolution_convert_fusion.1.refs_8_), channel_id=1, source_target_pairs={{0,1},{1,2},{2,3},{3,0},{4,5},{5,6},{6,7},{7,4},{8,9},{9,10},{10,1... | collective-permute-start | bytes 1179656 | tf_op jit(solution)/shard_map/ppermute | solution.py:22
  213.0 30.5 %collective-permute-start.20 = (bf16[384,512]{1,0:T(8,128)(2,1)S(1)}, bf16[384,512]{1,0:T(8,128)(2,1)}, u32[]{:S(2)}, u32[]{:S(2)}) collective-permute-start(bf16[384,512]{1,0:T(8,128)(2,1)S(1)} %convolution_convert_fusion.1.refs_8_), channel_id=1, source_target_pairs={{0,3},{1,0},{2,1},{3,2},{4,7},{5,4},{6,5},{7,6},{8,11},{9,8},{10,9... | collective-permute-start | bytes 1179656 | tf_op jit(solution)/shard_map/ppermute | solution.py:22
  217.9 15.2 %collective-permute-start.10 = (bf16[384,256]{1,0:T(8,128)(2,1)}, bf16[384,256]{1,0:T(8,128)(2,1)}, u32[]{:S(2)}, u32[]{:S(2)}) collective-permute-start(bf16[384,256]{1,0:T(8,128)(2,1)} %convolution_convert_fusion.2.refs_0_), channel_id=1, source_target_pairs={{0,1},{1,2},{2,3},{3,0},{4,5},{5,6},{6,7},{7,4},{8,9},{9,10},{10,1... | collective-permute-start | bytes 589832 | tf_op jit(solution)/shard_map/ppermute | solution.py:22
  218.0 15.2 %collective-permute-start.11 = (bf16[384,256]{1,0:T(8,128)(2,1)}, bf16[384,256]{1,0:T(8,128)(2,1)}, u32[]{:S(2)}, u32[]{:S(2)}) collective-permute-start(bf16[384,256]{1,0:T(8,128)(2,1)} %convolution_convert_fusion.2.refs_0_), channel_id=1, source_target_pairs={{0,3},{1,0},{2,1},{3,2},{4,7},{5,4},{6,5},{7,6},{8,11},{9,8},{10,9... | collective-permute-start | bytes 589832 | tf_op jit(solution)/shard_map/ppermute | solution.py:22
  220.6 12.6 %collective-permute-start.12 = (bf16[384,256]{1,0:T(8,128)(2,1)}, bf16[384,256]{1,0:T(8,128)(2,1)}, u32[]{:S(2)}, u32[]{:S(2)}) collective-permute-start(bf16[384,256]{1,0:T(8,128)(2,1)} %convolution_convert_fusion.2.refs_0_), channel_id=1, source_target_pairs={{0,2},{1,3},{2,0},{3,1},{4,6},{5,7},{6,4},{7,5},{8,10},{9,11},{10,... | collective-permute-start | bytes 589832 | tf_op jit(solution)/shard_map/ppermute | solution.py:22
  233.2 11.2 %collective-permute-start.21 = (bf16[384,512]{1,0:T(8,128)(2,1)S(1)}, bf16[384,512]{1,0:T(8,128)(2,1)S(1)}, u32[]{:S(2)}, u32[]{:S(2)}) collective-permute-start(bf16[384,512]{1,0:T(8,128)(2,1)S(1)} %convolution_convert_fusion.1.refs_8_), channel_id=1, source_target_pairs={{0,2},{1,3},{2,0},{3,1},{4,6},{5,7},{6,4},{7,5},{8,10},{9,11},{10,... | collective-permute-start | bytes 1179656 | tf_op jit(solution)/shard_map/ppermute | solution.py:22
  233.2 15.1 %collective-permute-start.16 = (bf16[384,128]{1,0:T(8,128)(2,1)S(1)}, bf16[384,128]{1,0:T(8,128)(2,1)S(1)}, u32[]{:S(2)}, u32[]{:S(2)}) collective-permute-start(bf16[384,128]{1,0:T(8,128)(2,1)S(1)} %convolution_convert_fusion.3.refs_4_), channel_id=1, source_target_pairs={{0,1},{1,2},{2,3},{3,0},{4,5},{5,6},{6,7},{7,4},{8,9},{9,10},{10,1... | collective-permute-start | bytes 294920 | tf_op jit(solution)/shard_map/ppermute | solution.py:22
  233.3 15.0 %collective-permute-start.17 = (bf16[384,128]{1,0:T(8,128)(2,1)S(1)}, bf16[384,128]{1,0:T(8,128)(2,1)S(1)}, u32[]{:S(2)}, u32[]{:S(2)}) collective-permute-start(bf16[384,128]{1,0:T(8,128)(2,1)S(1)} %convolution_convert_fusion.3.refs_4_), channel_id=1, source_target_pairs={{0,3},{1,0},{2,1},{3,2},{4,7},{5,4},{6,5},{7,6},{8,11},{9,8},{10,9... | collective-permute-start | bytes 294920 | tf_op jit(solution)/shard_map/ppermute | solution.py:22
  235.9 13.0 %collective-permute-start.18 = (bf16[384,128]{1,0:T(8,128)(2,1)S(1)}, bf16[384,128]{1,0:T(8,128)(2,1)}, u32[]{:S(2)}, u32[]{:S(2)}) collective-permute-start(bf16[384,128]{1,0:T(8,128)(2,1)S(1)} %convolution_convert_fusion.3.refs_4_), channel_id=1, source_target_pairs={{0,2},{1,3},{2,0},{3,1},{4,6},{5,7},{6,4},{7,5},{8,10},{9,11},{10,... | collective-permute-start | bytes 294920 | tf_op jit(solution)/shard_map/ppermute | solution.py:22
  265.3 25.7 %all-to-all-start.5 = ((bf16[32,64,256]{2,1,0:T(8,128)(2,1)}), bf16[32,64,256]{2,1,0:T(8,128)(2,1)}, u32[]{:S(2)}, u32[]{:S(2)}) async-start(bf16[32,64,256]{2,1,0:T(8,128)(2,1)} %bitcast.69), calls=%async_computation.5 | async-start | bytes 2097152 | tf_op jit(solution)/shard_map/all_to_all | solution.py:26
  275.2 12.7 %collective-permute-start.23 = (f32[2,256]{1,0:T(2,128)S(1)}, f32[2,256]{1,0:T(2,128)S(1)}, u32[]{:S(2)}, u32[]{:S(2)}) collective-permute-start(f32[2,256]{1,0:T(2,128)S(1)} %slice.56), channel_id=1, source_target_pairs={{4,0},{8,4},{12,8},{16,12},{20,16},{24,20},{28,24},{32,28},{36,32}... | collective-permute-start | bytes 6152 | tf_op jit(solution)/shard_map/ppermute | solution.py:17
  (25 other events, 182.0 us)
